TPU v7x, 256 devices: a whole 4x4x8 slice. The times are simulated.
256 devices in a mesh: ep: 128 (over z, y, x), tp: 2 (over core).
Axes of the slice: x: 4, y: 4, z: 8, core: 2. Of those that a mesh axis runs over, the one named last changes fastest.
Arguments:
- tokens: bfloat16 [6144, 2048], P('ep', 'tp'), may hold values from -12 to 12
- conv_state: bfloat16 [6144, 3, 1024], P('ep', None, 'tp'), may hold values from -6 to 6
- hidden_state: float32 [6144, 1024], P('ep', 'tp'), may hold values from -6 to 6
- mixer_gain: float32 [2048], replicated, may hold values from 0.1 to 1.9
- branch_weight: bfloat16 [2048, 1024], P(None, 'tp'), may hold values from -0.125 to 0.125
- gelu_weight: bfloat16 [2048, 1024], P(None, 'tp'), may hold values from -0.125 to 0.125
- conv_kernel: float32 [4, 1024], P(None, 'tp'), may hold values from -3 to 3
- recur_blocks: bfloat16 [16, 64, 64], P('tp'), may hold values from -0.75 to 0.75
- input_blocks: bfloat16 [16, 64, 64], P('tp'), may hold values from -0.75 to 0.75
- decay_rate: float32 [1024], P('tp'), may hold values from 0.002 to 0.1
- output_weight: bfloat16 [1024, 2048], P(None, 'tp'), may hold values from -0.1875 to 0.1875
- expert_gain: float32 [2048], replicated, may hold values from 0.1 to 1.9
- expert_ids: int32 [6144, 2], P('ep'), may hold values from 0 to 127, as said below
- group_prob: float32 [6144], P('ep'), may hold values from 0.25 to 1
- expert_logit: float32 [6144, 2], P('ep'), may hold values from -4 to 4
- expert_gate: bfloat16 [128, 2048, 512], P('ep', None, 'tp'), may hold values from -0.125 to 0.125
- expert_up: bfloat16 [128, 2048, 512], P('ep', None, 'tp'), may hold values from -0.125 to 0.125
- expert_down: bfloat16 [128, 512, 2048], P('ep', 'tp'), may hold values from -0.25 to 0.25
Outputs:
- layer_out: bfloat16 [6144, 2048], P('ep', 'tp')
- new_hidden: float32 [6144, 1024], P('ep', 'tp')
Inputs may be any that keep to these rules, and one draw needn't show every extreme that they name: `expert_ids`: the two experts of a row are different and lie in one group of 32 consecutive experts. Within the rows of one index of ep no expert is named more than 2 times, and one expert is named exactly 2 times by the rows of every index of ep.
All inputs are finite; a program needn't handle non-finite values.
Results may differ from a plain program's by a relative error of at most 0.012.
Values may be sent and summed in bfloat16 or wider, within the bound.
No kernel may reach another device: no remote copies, remote signals or barrier semaphores. Data moves between devices by JAX's collectives and lax.ppermute only.
A program may use at most 64 MiB of HBM per device.

v0:
```python
import jax
import jax.numpy as jnp
from jax import lax
from jax.sharding import PartitionSpec as P

EPSILON = 1e-06
RATE_SCALE = 8.0


def copy_for_each(array, axis):
    copies = jnp.broadcast_to(array, (lax.axis_size(axis), *array.shape))
    return lax.all_to_all(copies, axis, split_axis=0, concat_axis=0, tiled=True)


def in_order(tiles, dim):
    lengths = list(tiles.shape[1:])
    lengths[dim] *= tiles.shape[0]
    return jnp.moveaxis(tiles, 0, dim).reshape(lengths)


def collect(array, axis, dim):
    tiles = copy_for_each(array, axis)
    return in_order(tiles, dim)


def split_up(array, dim, devices):
    before, after = (array.shape[:dim], array.shape[dim + 1 :])
    return jnp.moveaxis(array.reshape(*before, devices, -1, *after), dim, 0)


def sent_and_summed(array, axis, dim):
    devices = lax.axis_size(axis)
    tiles = lax.all_to_all(split_up(array, dim, devices), axis, 0, 0, tiled=True)
    return jnp.sum(tiles.astype(jnp.float32), axis=0)


def of_everyone(array, axis):
    return copy_for_each(array, axis).sum(axis=0)


def normalize(values, gain_row):
    squares = jnp.mean(values * values, axis=-1, keepdims=True)
    return values * lax.rsqrt(squares + EPSILON) * gain_row


def local(
    tokens,
    conv_state,
    hidden_state,
    mixer_gain,
    branch_weight,
    gelu_weight,
    conv_kernel,
    recur_blocks,
    input_blocks,
    decay_rate,
    output_weight,
    expert_gain,
    expert_ids,
    group_prob,
    expert_logit,
    expert_gate,
    expert_up,
    expert_down,
):
    whole_tokens = collect(tokens, "tp", 1)
    normed = normalize(whole_tokens.astype(jnp.float32), mixer_gain).astype(jnp.bfloat16)
    branch = jnp.dot(normed, branch_weight, preferred_element_type=jnp.float32).astype(jnp.bfloat16)
    gelu_input = jnp.dot(normed, gelu_weight, preferred_element_type=jnp.float32).astype(
        jnp.bfloat16
    )
    window = jnp.concatenate([conv_state, branch[:, None, :]], axis=1).astype(jnp.float32)
    convolved = jnp.sum(window * conv_kernel[None], axis=1).astype(jnp.bfloat16)
    sequences, channels = convolved.shape
    blocks, block_size = (recur_blocks.shape[0], recur_blocks.shape[1])
    grouped = convolved.reshape(sequences, blocks, block_size)
    recur_pre = jnp.einsum(
        "tnc,ncd->tnd", grouped, recur_blocks, preferred_element_type=jnp.float32
    ).reshape(sequences, channels)
    input_pre = jnp.einsum(
        "tnc,ncd->tnd", grouped, input_blocks, preferred_element_type=jnp.float32
    ).reshape(sequences, channels)
    recur_gate = jax.nn.sigmoid(recur_pre)
    input_gate = jax.nn.sigmoid(input_pre)
    log_decay = -RATE_SCALE * recur_gate * decay_rate
    new_hidden = jnp.exp(log_decay) * hidden_state + jnp.sqrt(-jnp.expm1(2.0 * log_decay)) * (
        input_gate * convolved.astype(jnp.float32)
    )
    mixed_rows = (
        new_hidden * jax.nn.gelu(gelu_input.astype(jnp.float32), approximate=True)
    ).astype(jnp.bfloat16)
    mixed_whole = collect(mixed_rows, "tp", 1)
    residual = (
        tokens.astype(jnp.float32)
        + jnp.dot(mixed_whole, output_weight, preferred_element_type=jnp.float32)
    ).astype(jnp.bfloat16)
    experts = lax.axis_size("ep")
    top_count = expert_ids.shape[1]
    capacity = 2 * max(1, sequences // experts)
    flat_ids = expert_ids.reshape(-1)
    onehot_ids = (flat_ids[:, None] == jnp.arange(experts, dtype=jnp.int32)[None, :]).astype(
        jnp.int32
    )
    earlier = jnp.cumsum(onehot_ids, axis=0) - onehot_ids
    ranking = jnp.sum(earlier * onehot_ids, axis=1)
    slot_index = flat_ids * capacity + ranking
    placing = (
        jnp.arange(experts * capacity, dtype=jnp.int32)[:, None] == slot_index[None, :]
    ).astype(jnp.float32)
    placing = jnp.sum(placing.reshape(experts * capacity, sequences, top_count), axis=2).astype(
        jnp.bfloat16
    )
    values = residual.astype(jnp.float32)
    half_width = values.shape[1]
    square_total = of_everyone(jnp.sum(values * values, axis=1), "tp")
    gain_part = lax.dynamic_slice_in_dim(
        expert_gain, lax.axis_index("tp") * half_width, half_width, 0
    )
    scaling = lax.rsqrt(square_total / (half_width * lax.axis_size("tp")) + EPSILON)
    moe_input = (values * scaling[:, None] * gain_part[None, :]).astype(jnp.bfloat16)
    outgoing = jnp.dot(placing, moe_input, preferred_element_type=jnp.float32).astype(jnp.bfloat16)
    outgoing = outgoing.reshape(experts, capacity, half_width)
    received = collect(
        lax.all_to_all(outgoing, "ep", split_axis=0, concat_axis=0, tiled=True), "tp", 2
    )
    sources, slot_count, features = received.shape
    flat_rows = received.reshape(sources * slot_count, features)
    gate_part = jnp.dot(flat_rows, expert_gate[0], preferred_element_type=jnp.float32)
    upper_part = jnp.dot(flat_rows, expert_up[0], preferred_element_type=jnp.float32)
    hidden_units = (jax.nn.silu(gate_part) * upper_part).astype(jnp.bfloat16)
    partial_value = jnp.dot(
        hidden_units, expert_down[0], preferred_element_type=jnp.float32
    ).reshape(sources, slot_count, features)
    summed = sent_and_summed(partial_value.astype(jnp.bfloat16), "tp", 2).astype(jnp.bfloat16)
    returned = lax.all_to_all(summed, "ep", split_axis=0, concat_axis=0, tiled=True)
    out_width = returned.shape[2]
    picked = jnp.take(returned.reshape(experts * capacity, out_width), slot_index, axis=0).reshape(
        sequences, top_count, out_width
    )
    logit_exp = jnp.exp(expert_logit)
    weights = group_prob[:, None] * logit_exp / jnp.sum(logit_exp, axis=1, keepdims=True)
    layer_out = (
        residual.astype(jnp.float32)
        + jnp.sum(weights[:, :, None] * picked.astype(jnp.float32), axis=1)
    ).astype(jnp.bfloat16)
    return (layer_out, new_hidden)


def solution(mesh):
    return jax.shard_map(
        local,
        mesh=mesh,
        in_specs=(
            P("ep", "tp"),
            P("ep", None, "tp"),
            P("ep", "tp"),
            P(),
            P(None, "tp"),
            P(None, "tp"),
            P(None, "tp"),
            P("tp", None, None),
            P("tp", None, None),
            P("tp"),
            P(None, "tp"),
            P(),
            P("ep", None),
            P("ep"),
            P("ep", None),
            P("ep", None, "tp"),
            P("ep", None, "tp"),
            P("ep", "tp", None),
        ),
        out_specs=(P("ep", "tp"), P("ep", "tp")),
        check_vma=False,
    )
```

profile of v0, /device:TPU:1, one launch (start us, length us, event | category | flops | bytes accessed | tf_op | source)
XLA Modules:
  0.0 105.2 jit_solution(16739360342778136177)
XLA Ops:
  0.7 1.1 %broadcast_in_dim.20 = bf16[2,48,1024]{2,1,0:T(8,128)(2,1)S(1)} broadcast(bf16[48,1024]{1,0:T(8,128)(2,1)} %param.18), dimensions={1,2} | broadcast | bytes 294912 | tf_op jit(solution)/shard_map/broadcast_in_dim | solution.py:11
  1.7 6.9 %all_to_all.36 = bf16[2,48,1024]{2,1,0:T(8,128)(2,1)S(1)} all-to-all(bf16[2,48,1024]{2,1,0:T(8,128)(2,1)S(1)} %broadcast_in_dim.20), channel_id=1, replica_groups=mesh['ep'=128,'tp'=2] {'tp'}, dimensions={0} | all-to-all | bytes 393216 | tf_op jit(solution)/shard_map/all_to_all | solution.py:12
  8.7 0.1 fusion.17
  8.9 0.5 fusion.12
  9.4 0.1 copy-done.6
  9.6 0.1 convert_element_type.90
  9.7 0.2 fusion.8
  10.0 0.1 div.37
  10.1 0.2 fusion.4
  10.4 0.1 div.39
  10.5 0.1 multiply_add_fusion
  10.6 2.2 %fusion.27 = bf16[48,512]{1,0:T(8,128)(2,1)S(1)} fusion(f32[48,512]{1,0:T(8,128)S(1)} %multiply_add_fusion, bf16[2048,512]{1,0:T(8,128)(2,1)} %param.23, f32[48,2048]{1,0:T(8,128)S(1)} %bitcast.57, f32[2048]{0:T(1024)S(1)} %copy-done.8, f32[48]{0:T(128)S(1)} %add_rsqrt_fusion.1), kind=kOutput, calls=%fused_computation.47 | convolution fusion | flops 101253120 | bytes 2646208 | tf_op jit(solution)/shard_map/dot_general | solution.py:69
  12.8 3.8 %all_to_all.37 = bf16[2,48,512]{2,1,0:T(8,128)(2,1)S(1)} all-to-all(bf16[2,48,512]{2,1,0:T(8,128)(2,1)S(1)} %broadcast_in_dim.22), channel_id=1, replica_groups=mesh['ep'=128,'tp'=2] {'tp'}, dimensions={0} | all-to-all | bytes 196608 | tf_op jit(solution)/shard_map/all_to_all | solution.py:12
  16.7 0.6 multiply_reduce_fusion.2
  17.2 0.6 broadcast_in_dim.41
  17.8 3.5 %all-to-all-start.2 = ((f32[2,1,48]{2,1,0:T(1,128)}), f32[2,1,48]{2,1,0:T(1,128)S(1)}, u32[]{:S(2)}, u32[]{:S(2)}) async-start(f32[2,1,48]{2,1,0:T(1,128)} %broadcast_in_dim.41), calls=%async_computation.2 | async-start | bytes 2048 | tf_op jit(solution)/shard_map/all_to_all | solution.py:12
  21.4 1.0 all-to-all-done.2
  22.4 0.1 copy.100
  22.4 0.1 reshape.126
  22.7 0.1 reduce_window_sum.11
  22.8 0.2 select_reduce_fusion
  23.0 0.1 reduce_sum.92
  23.2 0.1 convert_reduce_fusion
  23.3 0.3 convolution_convert_fusion.1
  23.7 0.2 reshape.127
  23.9 32.4 %all_to_all.38 = bf16[128,2,1024]{2,1,0:T(2,128)(2,1)S(1)} all-to-all(bf16[128,2,1024]{2,1,0:T(2,128)(2,1)S(1)} %reshape.127), channel_id=1, replica_groups=mesh['ep'=128,'tp'=2] {'ep'}, dimensions={0} | all-to-all | bytes 1048576 | tf_op jit(solution)/shard_map/all_to_all | solution.py:124
  56.3 0.5 broadcast_in_dim.42
  56.9 7.0 %all_to_all.39 = bf16[2,128,2,1024]{3,2,1,0:T(2,128)(2,1)S(1)} all-to-all(bf16[2,128,2,1024]{3,2,1,0:T(2,128)(2,1)S(1)} %broadcast_in_dim.42), channel_id=1, replica_groups=mesh['ep'=128,'tp'=2] {'tp'}, dimensions={0} | all-to-all | bytes 2097152 | tf_op jit(solution)/shard_map/all_to_all | solution.py:12
  63.8 1.6 %copy.104 = bf16[128,2,2,1024]{3,2,1,0:T(2,128)(2,1)S(1)} copy(bf16[128,2,2,1024]{3,1,0,2:T(2,128)(2,1)S(1)} %bitcast.52) | data formatting | bytes 2097152 | tf_op jit(solution)/shard_map/transpose | solution.py:18
  65.5 0.3 copy.114
  65.8 0.5 fusion.15
  66.2 0.5 copy-done.15
  66.7 1.1 %fusion = bf16[256,256]{1,0:T(8,128)(2,1)} fusion(bf16[256,2048]{1,0:T(8,128)(2,1)S(1)} %bitcast.51, bf16[1,2048,256]{2,1,0:T(8,128)(2,1)S(1)} %copy-done.15, f32[256,256]{1,0:T(8,128)S(1)} %fusion.15), kind=kOutput, calls=%fused_computation.4 | convolution fusion | flops 268828672 | bytes 2490368 | tf_op jit(solution)/shard_map/dot_general | solution.py:129
  67.8 1.0 dot_general.37
  68.8 0.4 convolution_convert_fusion
  69.3 4.6 %all_to_all.40 = bf16[2,128,2,1024]{3,1,2,0:T(8,128)(2,1)S(1)} all-to-all(bf16[2,128,2,1024]{3,1,2,0:T(8,128)(2,1)S(1)} %bitcast.55), channel_id=1, replica_groups=mesh['ep'=128,'tp'=2] {'tp'}, dimensions={0} | all-to-all | bytes 2097152 | tf_op jit(solution)/shard_map/all_to_all | solution.py:33
  73.9 1.1 %reduce_sum.96 = bf16[128,2,1024]{2,0,1:T(8,128)(2,1)} reduce(bf16[2,128,2,1024]{3,1,2,0:T(8,128)(2,1)S(1)} %all_to_all.40, bf16[]{:T(256)} %constant.55.clone.1), dimensions={0}, to_apply=%region_8.9 | reduce | flops 262144 | bytes 1572866 | tf_op jit(solution)/shard_map/reduce_sum | solution.py:34
  75.0 2.4 %copy.108 = bf16[128,2,1024]{2,1,0:T(2,128)(2,1)} copy(bf16[128,2,1024]{2,0,1:T(8,128)(2,1)} %reduce_sum.96) | data formatting | bytes 1048576 | tf_op jit(solution)/shard_map/reduce_sum | solution.py:34
  77.4 6.2 %all-to-all-start.6 = ((bf16[128,2,1024]{2,1,0:T(2,128)(2,1)}), bf16[128,2,1024]{2,1,0:T(2,128)(2,1)S(1)}, u32[]{:S(2)}, u32[]{:S(2)}) async-start(bf16[128,2,1024]{2,1,0:T(2,128)(2,1)} %copy.108), calls=%async_computation.6 | async-start | bytes 1048576 | tf_op jit(solution)/shard_map/all_to_all | solution.py:135
  83.6 0.1 copy.109
  83.7 0.1 mul.191
  83.8 0.1 copy.102
  84.0 0.1 copy.99
  84.1 18.7 %all-to-all-done.6 = bf16[128,2,1024]{2,1,0:T(2,128)(2,1)S(1)} async-done(((bf16[128,2,1024]{2,1,0:T(2,128)(2,1)}), bf16[128,2,1024]{2,1,0:T(2,128)(2,1)S(1)}, u32[]{:S(2)}, u32[]{:S(2)}) %all-to-all-start.6) | async-done | bytes 524320 | tf_op jit(solution)/shard_map/all_to_all | solution.py:135
  102.8 0.2 reshape.129
  103.0 0.8 gather_fusion
  103.8 0.7 multiply_reduce_fusion
  104.5 0.7 add_convert_fusion
  (56 shorter events, 0.8 us)
Async XLA Ops:
  0.6 16.0 %copy-start = (bf16[1024,1024]{1,0:T(8,128)(2,1)S(1)}, bf16[1024,1024]{1,0:T(8,128)(2,1)}, u32[]{:S(2)}) copy-start(bf16[1024,1024]{1,0:T(8,128)(2,1)} %param.28) | copy-start | bytes 6291460
  0.6 8.2 %copy-start.8 = (f32[2048]{0:T(1024)S(1)}, f32[2048]{0:T(1024)}, u32[]{:S(2)}) copy-start(f32[2048]{0:T(1024)} %param.21) | copy-start | bytes 24580
  0.7 8.2 %copy-start.1 = (bf16[2048,512]{1,0:T(8,128)(2,1)S(1)}, bf16[2048,512]{1,0:T(8,128)(2,1)}, u32[]{:S(2)}) copy-start(bf16[2048,512]{1,0:T(8,128)(2,1)} %param.22) | copy-start | bytes 6291460
  8.6 0.9 copy-start.6
  8.6 0.9 copy-start.10
  8.6 1.0 copy-start.16
  8.9 1.2 %copy-start.17 = (bf16[8,64,64]{2,1,0:T(8,128)(2,1)S(1)}, bf16[8,64,64]{2,1,0:T(8,128)(2,1)}, u32[]{:S(2)}) copy-start(bf16[8,64,64]{2,1,0:T(8,128)(2,1)} %param.26) | copy-start | bytes 196612
  9.5 1.0 copy-start.12
  9.5 1.0 copy-start.7
  10.3 6.4 %copy-start.5 = (bf16[48,1024]{1,0:T(8,128)(2,1)S(1)}, bf16[48,1024]{1,0:T(8,128)(2,1)}, u32[]{:S(2)}) copy-start(bf16[48,1024]{1,0:T(8,128)(2,1)} %param.18) | copy-start | bytes 294916
  10.6 6.6 %copy-start.4 = (f32[48,512]{1,0:T(8,128)}, f32[48,512]{1,0:T(8,128)S(1)}, u32[]{:S(2)}) copy-start(f32[48,512]{1,0:T(8,128)S(1)} %multiply_add_fusion) | copy-start | bytes 294916
  12.8 9.6 %copy-start.9 = (s32[48,2]{0,1:T(2,128)S(1)}, s32[48,2]{0,1:T(2,128)}, u32[]{:S(2)}) copy-start(s32[48,2]{0,1:T(2,128)} %param.30) | copy-start | bytes 1156
  12.8 10.5 %copy-start.11 = (f32[2048]{0:T(1024)S(1)}, f32[2048]{0:T(1024)}, u32[]{:S(2)}) copy-start(f32[2048]{0:T(1024)} %param.29) | copy-start | bytes 24580
  17.8 4.5 %all-to-all-start.2 = ((f32[2,1,48]{2,1,0:T(1,128)}), f32[2,1,48]{2,1,0:T(1,128)S(1)}, u32[]{:S(2)}, u32[]{:S(2)}) async-start(f32[2,1,48]{2,1,0:T(1,128)} %broadcast_in_dim.41), calls=%async_computation.2 | async-start | bytes 2048 | tf_op jit(solution)/shard_map/all_to_all | solution.py:12
  63.8 1.9 %copy-start.2 = (bf16[1,2048,256]{2,1,0:T(8,128)(2,1)S(1)}, bf16[1,2048,256]{2,1,0:T(8,128)(2,1)}, u32[]{:S(2)}) copy-start(bf16[1,2048,256]{2,1,0:T(8,128)(2,1)} %param.33) | copy-start | bytes 3145732
  65.5 1.2 %copy-start.15 = (bf16[1,2048,256]{2,1,0:T(8,128)(2,1)S(1)}, bf16[1,2048,256]{2,1,0:T(8,128)(2,1)}, u32[]{:S(2)}) copy-start(bf16[1,2048,256]{2,1,0:T(8,128)(2,1)} %param.34) | copy-start | bytes 3145732
  66.7 2.1 %copy-start.3 = (bf16[1,256,2048]{2,1,0:T(8,128)(2,1)S(1)}, bf16[1,256,2048]{2,1,0:T(8,128)(2,1)}, u32[]{:S(2)}) copy-start(bf16[1,256,2048]{2,1,0:T(8,128)(2,1)} %param.35) | copy-start | bytes 3145732
  73.9 10.0 %copy-start.13 = (f32[48,2]{0,1:T(2,128)S(1)}, f32[48,2]{0,1:T(2,128)}, u32[]{:S(2)}) copy-start(f32[48,2]{0,1:T(2,128)} %param.32) | copy-start | bytes 1156
  73.9 10.1 %copy-start.14 = (f32[48]{0:T(128)S(1)}, f32[48]{0:T(128)}, u32[]{:S(2)}) copy-start(f32[48]{0:T(128)} %param.31) | copy-start | bytes 580
  77.4 25.4 %all-to-all-start.6 = ((bf16[128,2,1024]{2,1,0:T(2,128)(2,1)}), bf16[128,2,1024]{2,1,0:T(2,128)(2,1)S(1)}, u32[]{:S(2)}, u32[]{:S(2)}) async-start(bf16[128,2,1024]{2,1,0:T(2,128)(2,1)} %copy.108), calls=%async_computation.6 | async-start | bytes 1048576 | tf_op jit(solution)/shard_map/all_to_all | solution.py:135
where the time goes:
time: 106 us; the launch traced here: 105 us
  blocking collectives  54.7 us (52%)
  waiting for transfers between devices  19.6 us (18%)
  local copies, waits for them, and re-layouts  10.8 us (10%)
  starting transfers between devices  9.71 us (9%)
  matrix products  6 us (6%)
  other arithmetic  3.35 us (3%)
  between operations  1.06 us (1%)
    all_to_all x1, blocking collectives, local(): lax.all_to_all(outgoing, 'ep', split_axis=0, concat_axis=0, tiled=True)  32.4 us
    all_to_all x1, waiting for transfers between devices, local(): lax.all_to_all(summed, 'ep', split_axis=0, concat_axis=0, tiled=True)  18.7 us
    all_to_all x3, blocking collectives, copy_for_each(): return lax.all_to_all(copies, axis, split_axis=0, concat_axis=0, tiled=True)  17.6 us
    all_to_all x1, starting transfers between devices, local(): lax.all_to_all(summed, 'ep', split_axis=0, concat_axis=0, tiled=True)  6.17 us
    all_to_all x1, blocking collectives, sent_and_summed(): lax.all_to_all(split_up(array, dim, devices), axis, 0, 0, tiled=True)  4.58 us
    all_to_all x1, starting transfers between devices, copy_for_each(): return lax.all_to_all(copies, axis, split_axis=0, concat_axis=0, tiled=True)  3.54 us
    reduce_sum x1, local copies, waits for them, and re-layouts, sent_and_summed(): return jnp.sum(tiles.astype(jnp.float32), axis=0)  2.39 us
    broadcast_in_dim x4, local copies, waits for them, and re-layouts, copy_for_each(): copies = jnp.broadcast_to(array, (lax.axis_size(axis), *array.shape))  2.18 us
  transfers between devices with their start and end apart: 2, of which 2 were waited for; matrix products, arithmetic and copies ran while one was open for 0% of the time, Pallas kernels for 0%

commit v1 on v0

v1 whole, which is shorter than its diff:
```python
import jax
import jax.numpy as jnp
from jax import lax
from jax.sharding import PartitionSpec as P

EPSILON = 1e-06
RATE_SCALE = 8.0


def swap(array):
    return lax.ppermute(array, "tp", [(0, 1), (1, 0)])


def whole_row(own, first):
    other = swap(own)
    return jnp.concatenate(
        [jnp.where(first, own, other), jnp.where(first, other, own)], axis=1
    )


def normalize(values, gain_row):
    squares = jnp.mean(values * values, axis=-1, keepdims=True)
    return values * lax.rsqrt(squares + EPSILON) * gain_row


def local(
    tokens,
    conv_state,
    hidden_state,
    mixer_gain,
    branch_weight,
    gelu_weight,
    conv_kernel,
    recur_blocks,
    input_blocks,
    decay_rate,
    output_weight,
    expert_gain,
    expert_ids,
    group_prob,
    expert_logit,
    expert_gate,
    expert_up,
    expert_down,
):
    first = lax.axis_index("tp") == 0
    experts = lax.axis_size("ep")
    cores = lax.axis_size("tp")
    bf16 = jnp.bfloat16
    whole_tokens = whole_row(tokens, first)
    gates = (expert_gate[0], swap(expert_gate[0]))
    uppers = (expert_up[0], swap(expert_up[0]))
    downs = (expert_down[0], swap(expert_down[0]))

    normed = normalize(whole_tokens.astype(jnp.float32), mixer_gain).astype(bf16)
    branch = jnp.dot(normed, branch_weight, preferred_element_type=jnp.float32).astype(bf16)
    gelu_input = jnp.dot(normed, gelu_weight, preferred_element_type=jnp.float32).astype(bf16)
    taps = conv_kernel.shape[0]
    mixed_taps = branch.astype(jnp.float32) * conv_kernel[taps - 1]
    for tap in range(taps - 1):
        mixed_taps = mixed_taps + conv_state[:, tap].astype(jnp.float32) * conv_kernel[tap]
    convolved = mixed_taps.astype(bf16)
    sequences, channels = convolved.shape
    blocks, block_size = (recur_blocks.shape[0], recur_blocks.shape[1])
    grouped = convolved.reshape(sequences, blocks, block_size)
    recur_pre = jnp.einsum(
        "tnc,ncd->tnd", grouped, recur_blocks, preferred_element_type=jnp.float32
    ).reshape(sequences, channels)
    input_pre = jnp.einsum(
        "tnc,ncd->tnd", grouped, input_blocks, preferred_element_type=jnp.float32
    ).reshape(sequences, channels)
    recur_gate = jax.nn.sigmoid(recur_pre)
    input_gate = jax.nn.sigmoid(input_pre)
    log_decay = -RATE_SCALE * recur_gate * decay_rate
    new_hidden = jnp.exp(log_decay) * hidden_state + jnp.sqrt(-jnp.expm1(2.0 * log_decay)) * (
        input_gate * convolved.astype(jnp.float32)
    )
    mixed_rows = (
        new_hidden * jax.nn.gelu(gelu_input.astype(jnp.float32), approximate=True)
    ).astype(bf16)
    mixed_whole = whole_row(mixed_rows, first)
    residual = (
        tokens.astype(jnp.float32)
        + jnp.dot(mixed_whole, output_weight, preferred_element_type=jnp.float32)
    ).astype(bf16)

    flat_ids = expert_ids.reshape(-1)
    places = jnp.arange(flat_ids.shape[0], dtype=jnp.int32)
    same = (flat_ids[:, None] == flat_ids[None, :]) & (places[None, :] < places[:, None])
    ranking = jnp.sum(same.astype(jnp.int32), axis=1)
    slots = (ranking * experts + flat_ids).reshape(expert_ids.shape)
    slot_list = jnp.arange(cores * experts, dtype=jnp.int32)
    placing = jnp.any(slot_list[:, None, None] == slots[None], axis=2).astype(bf16)
    outgoing = jnp.dot(placing, residual, preferred_element_type=jnp.float32).astype(bf16)
    received = lax.all_to_all(outgoing, ("tp", "ep"), split_axis=0, concat_axis=0, tiled=True)

    half_width = received.shape[1]
    halves = received.reshape(cores, experts, half_width)
    parts = [halves[side].astype(jnp.float32) for side in range(cores)]
    squares = sum(jnp.sum(part * part, axis=1, keepdims=True) for part in parts)
    scaling = lax.rsqrt(squares / (half_width * cores) + EPSILON)
    rows = jnp.concatenate(parts, axis=1) * scaling * expert_gain[None, :]
    rows = rows.astype(bf16)
    results = []
    for gate_matrix, upper_matrix, down_matrix in zip(gates, uppers, downs):
        gate_part = jnp.dot(rows, gate_matrix, preferred_element_type=jnp.float32)
        upper_part = jnp.dot(rows, upper_matrix, preferred_element_type=jnp.float32)
        hidden_units = (jax.nn.silu(gate_part) * upper_part).astype(bf16)
        results.append((hidden_units, down_matrix))
    answers = []
    for side in range(cores):
        span = slice(side * half_width, (side + 1) * half_width)
        total = sum(
            jnp.dot(hidden_units, down_matrix[:, span], preferred_element_type=jnp.float32)
            for hidden_units, down_matrix in results
        )
        answers.append(total.astype(bf16))
    answers = jnp.concatenate(answers, axis=0)
    returned = lax.all_to_all(answers, ("tp", "ep"), split_axis=0, concat_axis=0, tiled=True)

    logit_exp = jnp.exp(expert_logit)
    weights = group_prob[:, None] * logit_exp / jnp.sum(logit_exp, axis=1, keepdims=True)
    picking = jnp.sum(
        jnp.where(slots[:, :, None] == slot_list[None, None, :], weights[:, :, None], 0.0), axis=1
    )
    high = picking.astype(bf16)
    low = (picking - high.astype(jnp.float32)).astype(bf16)
    chosen = jnp.dot(high, returned, preferred_element_type=jnp.float32) + jnp.dot(
        low, returned, preferred_element_type=jnp.float32
    )
    layer_out = (residual.astype(jnp.float32) + chosen).astype(bf16)
    return (layer_out, new_hidden)


def solution(mesh):
    return jax.shard_map(
        local,
        mesh=mesh,
        in_specs=(
            P("ep", "tp"),
            P("ep", None, "tp"),
            P("ep", "tp"),
            P(),
            P(None, "tp"),
            P(None, "tp"),
            P(None, "tp"),
            P("tp", None, None),
            P("tp", None, None),
            P("tp"),
            P(None, "tp"),
            P(),
            P("ep", None),
            P("ep"),
            P("ep", None),
            P("ep", None, "tp"),
            P("ep", None, "tp"),
            P("ep", "tp", None),
        ),
        out_specs=(P("ep", "tp"), P("ep", "tp")),
        check_vma=False,
    )
```

time: 106 us -> 101 us (0.953)
  blocking collectives: 54.7 us -> 0 us
  waiting for transfers between devices: 19.6 us -> 38.5 us
  starting transfers between devices: 9.71 us -> 26.8 us
  matrix products: 6 us -> 13.4 us
  other arithmetic: 3.35 us -> 6.6 us
  local copies, waits for them, and re-layouts: 10.8 us -> 14 us
    all_to_all x5 -> x0, blocking collectives: 54.7 us -> none  [the longest x1 32.4 us: local(): lax.all_to_all(outgoing, 'ep', split_axis=0, concat_axis=0, tiled=True)]
    all_to_all x2, waiting for transfers between devices: 19.6 us -> 37.4 us  [the longest x1 20.1 us: local(): lax.all_to_all(answers, ('tp', 'ep'), split_axis=0, concat_axis=0, tiled=...]
    unnamed x38 -> x32, local copies, waits for them, and re-layouts: 1.03 us -> 11.9 us
    all_to_all x2, starting transfers between devices: 9.71 us -> 20.5 us  [the longest x1 13.6 us: local(): lax.all_to_all(outgoing, ('tp', 'ep'), split_axis=0, concat_axis=0, tiled...]
    ppermute x0 -> x5, starting transfers between devices: none -> 6.24 us  [swap(): return lax.ppermute(array, 'tp', [(0, 1), (1, 0)])]
    dot_general x4 -> x11, matrix products: 2.33 us -> 8.23 us  [the longest x4 3.02 us: local(): jnp.dot(hidden_units, down_matrix[:, span], preferred_element_type=jnp.fl...]
    reduce_sum x3 -> x0, local copies, waits for them, and re-layouts: 2.59 us -> none  [the longest x1 2.39 us: sent_and_summed(): return jnp.sum(tiles.astype(jnp.float32), axis=0)]
    broadcast_in_dim x4 -> x0, local copies, waits for them, and re-layouts: 2.18 us -> none  [copy_for_each(): copies = jnp.broadcast_to(array, (lax.axis_size(axis), *array.shape))]
  transfers between devices with their start and end apart: 2 -> 7, of which waited for: 2 -> 3; matrix products, arithmetic and copies ran while one was open for 0% -> 13% of each run, Pallas kernels for 0% -> 0%
where the time goes in v1:
time: 101 us; the launch traced here: 100 us
  waiting for transfers between devices  38.5 us (38%)
  starting transfers between devices  26.8 us (27%)
  local copies, waits for them, and re-layouts  14 us (14%)
  matrix products  13.4 us (13%)
  other arithmetic  6.6 us (7%)
  between operations  1.08 us (1%)
    all_to_all x1, waiting for transfers between devices, local(): lax.all_to_all(answers, ('tp', 'ep'), split_axis=0, concat_axis=0, tiled=...  20.1 us
    all_to_all x1, waiting for transfers between devices, local(): lax.all_to_all(outgoing, ('tp', 'ep'), split_axis=0, concat_axis=0, tiled...  17.3 us
    all_to_all x1, starting transfers between devices, local(): lax.all_to_all(outgoing, ('tp', 'ep'), split_axis=0, concat_axis=0, tiled...  13.6 us
    unnamed x32, local copies, waits for them, and re-layouts  11.9 us
    all_to_all x1, starting transfers between devices, local(): lax.all_to_all(answers, ('tp', 'ep'), split_axis=0, concat_axis=0, tiled=...  6.92 us
    ppermute x5, starting transfers between devices, swap(): return lax.ppermute(array, 'tp', [(0, 1), (1, 0)])  6.24 us
    dot_general x4, matrix products, local(): jnp.dot(hidden_units, down_matrix[:, span], preferred_element_type=jnp.fl...  3.02 us
    dot_general x1, matrix products, local(): jnp.dot(normed, gelu_weight, preferred_element_type=jnp.float32)  2.17 us
  transfers between devices with their start and end apart: 7, of which 3 were waited for; matrix products, arithmetic and copies ran while one was open for 13% of the time, Pallas kernels for 0%

profile of v1, /device:TPU:1, one launch (start us, length us, event | category | flops | bytes accessed | tf_op | source)
XLA Modules:
  0.0 100.3 jit_solution(1170708060861310892)
XLA Ops:
  0.7 3.3 %collective-permute-start = (bf16[48,1024]{1,0:T(8,128)(2,1)}, bf16[48,1024]{1,0:T(8,128)(2,1)S(1)}, u32[]{:S(2)}, u32[]{:S(2)}) collective-permute-start(bf16[48,1024]{1,0:T(8,128)(2,1)} %param.18), channel_id=1, source_target_pairs={{0,1},{1,0},{2,3},{3,2},{4,5},{5,4},{6,7},{7,6},{8,9},{9,8},{10,11... | collective-permute-start | bytes 294920 | tf_op jit(solution)/shard_map/ppermute | solution.py:11
  3.9 0.9 fusion.64
  4.8 0.7 broadcast_multiply_fusion
  5.5 0.8 copy.69
  6.2 0.1 eq.45
  6.4 0.2 convert_reduce_fusion
  6.6 0.1 mul.204
  6.8 0.7 add.104
  7.5 0.9 broadcast_select_fusion.1
  8.4 0.1 fusion.33
  8.5 2.2 %fusion.21 = bf16[48,512]{1,0:T(8,128)(2,1)S(1)} fusion(bf16[2048,512]{1,0:T(8,128)(2,1)} %param.22, f32[512]{0:T(512)S(1)} %bitcast.69, bf16[48,3,512]{2,0,1:T(8,128)(2,1)} %param.19, f32[512]{0:T(512)S(1)} %bitcast.70, f32[512]{0:T(512)S(1)} %bitcast.68, f32[512]{0:T(512)S(1)} %bitcast.67, f32[2048]{0:T(1024)} %param.21, f32[48]{0:T(128)S(1)} %add_rsqrt_fusion.1, ...), kind=kOutput, calls=%fused_computation.31 | convolution fusion | flops 101670912 | bytes 2506944 | tf_op jit(solution)/shard_map/dot_general | solution.py:56
  10.7 0.1 reshape.85
  10.9 0.2 fusion.11
  11.3 0.2 fusion.7
  11.8 2.2 %fusion.47 = bf16[48,512]{1,0:T(8,128)(2,1)S(1)} fusion(f32[48,512]{1,0:T(8,128)S(1)} %multiply_add_fusion, bf16[2048,512]{1,0:T(8,128)(2,1)} %param.23, f32[2048]{0:T(1024)S(1)} %copy-done.6, f32[48]{0:T(128)S(1)} %add_rsqrt_fusion.1, bf16[48,1024]{1,0:T(8,128)(2,1)S(1)} %get-tuple-element.5, bf16[48,1024]{1,0:T(8,128)(2,1)S(1)} %get-tuple-element.4), kind=kOutput, calls=%fused_computation.69 | convolution fusion | flops 101646336 | bytes 2449600 | tf_op jit(solution)/shard_map/dot_general | solution.py:57
  14.0 0.1 collective-permute-start.1
  14.2 1.1 %collective-permute-done.1 = bf16[48,512]{1,0:T(8,128)(2,1)S(1)} collective-permute-done((bf16[48,512]{1,0:T(8,128)(2,1)S(1)}, bf16[48,512]{1,0:T(8,128)(2,1)S(1)}, u32[]{:S(2)}, u32[]{:S(2)}) %collective-permute-start.1) | collective-permute-done | bytes 49184 | tf_op jit(solution)/shard_map/ppermute | solution.py:11
  15.3 0.5 fusion.12
  15.8 0.3 fusion
  16.1 0.5 broadcast.66
  16.7 1.0 %reduce = bf16[256,1024]{1,0:T(8,128)(2,1)S(1)} reduce(bf16[256,1,1024]{2,0,1:T(8,128)(2,1)S(1)} %fusion, bf16[]{:T(256)} %broadcast.66), dimensions={1}, to_apply=%copy.71.reduce_sub_computation | reduce | bytes 1048578 | tf_op jit(solution)/shard_map/all_to_all | solution.py:95
  17.7 1.2 %reshape.91 = bf16[256,2,512]{2,1,0:T(2,128)(2,1)} reshape(bf16[256,1024]{1,0:T(8,128)(2,1)S(1)} %reduce) | data formatting | bytes 1048576
  18.9 13.6 %all-to-all-start = ((bf16[256,2,512]{2,1,0:T(2,128)(2,1)}), bf16[256,2,512]{2,1,0:T(2,128)(2,1)}, u32[]{:S(2)}, u32[]{:S(2)}) async-start(bf16[256,2,512]{2,1,0:T(2,128)(2,1)} %reshape.91), calls=%async_computation | async-start | bytes 1048576 | tf_op jit(solution)/shard_map/all_to_all | solution.py:95
  32.5 2.3 %collective-permute-start.2 = (bf16[2048,256]{1,0:T(8,128)(2,1)}, bf16[2048,256]{1,0:T(8,128)(2,1)}, u32[]{:S(2)}, u32[]{:S(2)}) collective-permute-start(bf16[2048,256]{1,0:T(8,128)(2,1)} %bitcast.66), channel_id=1, source_target_pairs={{0,1},{1,0},{2,3},{3,2},{4,5},{5,4},{6,7},{7,6},{8,9},{9,8},{10,11... | collective-permute-start | bytes 3145736 | tf_op jit(solution)/shard_map/ppermute | solution.py:11
  34.9 0.4 collective-permute-start.4
  35.3 17.3 %all-to-all-done = bf16[256,2,512]{2,1,0:T(2,128)(2,1)} async-done(((bf16[256,2,512]{2,1,0:T(2,128)(2,1)}), bf16[256,2,512]{2,1,0:T(2,128)(2,1)}, u32[]{:S(2)}, u32[]{:S(2)}) %all-to-all-start) | async-done | bytes 524320 | tf_op jit(solution)/shard_map/all_to_all | solution.py:95
  52.6 3.6 %reshape.92 = bf16[256,1,1024]{2,1,0:T(2,128)(2,1)S(1)} reshape(bf16[256,2,512]{2,1,0:T(2,128)(2,1)} %all-to-all-done) | data formatting | bytes 1048576
  56.2 1.1 %fusion.63 = (bf16[128,1,1024]{2,1,0:T(2,128)(2,1)S(1)}, f32[128,1,1024]{2,1,0:T(1,128)S(1)}) fusion(bf16[256,1,1024]{2,1,0:T(2,128)(2,1)S(1)} %reshape.92), kind=kLoop, calls=%fused_computation.103 | loop fusion | flops 131072 | bytes 1310720 | tf_op jit(solution)/shard_map/slice | solution.py:99
  57.4 0.2 multiply_reduce_fusion
  57.8 0.2 copy-done.7
  58.0 0.2 fusion.23
  58.1 0.5 copy-done.2
  58.6 0.3 fusion.59
  59.0 0.3 fusion.14
  59.3 0.6 copy-done.1
  59.9 0.2 fusion.28
  60.2 0.2 fusion.25
  60.4 1.5 %fusion.65 = f32[128,256]{1,0:T(8,128)S(1)} fusion(bf16[128,2048]{1,0:T(8,128)(2,1)S(1)} %fusion.23, bf16[2048,256]{1,0:T(8,128)(2,1)} %collective-permute-done.2), kind=kOutput, calls=%fused_computation.105 | convolution fusion | flops 134217728 | bytes 1703936 | tf_op jit(solution)/shard_map/dot_general | solution.py:106
  62.0 1.5 %multiply_convert_fusion = bf16[128,256]{1,0:T(8,128)(2,1)S(1)} fusion(f32[128,256]{1,0:T(8,128)S(1)} %fusion.65, bf16[128,2048]{1,0:T(8,128)(2,1)S(1)} %fusion.23, bf16[2048,256]{1,0:T(8,128)(2,1)} %collective-permute-done.3), kind=kOutput, calls=%fused_computation.60 | convolution fusion | flops 134414336 | bytes 1769472 | tf_op jit(solution)/shard_map/dot_general | solution.py:107
  63.5 1.3 %fusion.1 = bf16[128,1024]{1,0:T(8,128)(2,1)S(1)} fusion(f32[128,1024]{1,0:T(8,128)S(1)} %fusion.28, bf16[128,256]{1,0:T(8,128)(2,1)S(1)} %multiply_convert_fusion, bf16[256,2048]{1,0:T(8,128)(2,1)} %collective-permute-done.4), kind=kOutput, calls=%fused_computation.4 | convolution fusion | flops 67371008 | bytes 1376256 | tf_op jit(solution)/shard_map/dot_general | solution.py:114
  64.8 1.3 %fusion.2 = bf16[128,1024]{1,0:T(8,128)(2,1)S(1)} fusion(f32[128,1024]{1,0:T(8,128)S(1)} %fusion.25, bf16[128,256]{1,0:T(8,128)(2,1)S(1)} %multiply_convert_fusion, bf16[256,2048]{1,0:T(8,128)(2,1)} %collective-permute-done.4), kind=kOutput, calls=%fused_computation.5 | convolution fusion | flops 67371008 | bytes 1376256 | tf_op jit(solution)/shard_map/dot_general | solution.py:114
  66.2 1.0 %reduce.1 = bf16[256,1024]{1,0:T(8,128)(2,1)S(1)} reduce(bf16[256,1,1024]{2,0,1:T(8,128)(2,1)S(1)} %maximum_bitcast_fusion, bf16[]{:T(256)} %broadcast.66), dimensions={1}, to_apply=%copy.73.reduce_sub_computation | reduce | bytes 1048578 | tf_op jit(solution)/shard_map/all_to_all | solution.py:119
  67.2 1.2 %reshape.93 = bf16[256,2,512]{2,1,0:T(2,128)(2,1)} reshape(bf16[256,1024]{1,0:T(8,128)(2,1)S(1)} %reduce.1) | data formatting | bytes 1048576
  68.4 6.9 %all-to-all-start.1 = ((bf16[256,2,512]{2,1,0:T(2,128)(2,1)}), bf16[256,2,512]{2,1,0:T(2,128)(2,1)}, u32[]{:S(2)}, u32[]{:S(2)}) async-start(bf16[256,2,512]{2,1,0:T(2,128)(2,1)} %reshape.93), calls=%async_computation.1 | async-start | bytes 1048576 | tf_op jit(solution)/shard_map/all_to_all | solution.py:119
  75.5 20.1 %all-to-all-done.1 = bf16[256,2,512]{2,1,0:T(2,128)(2,1)} async-done(((bf16[256,2,512]{2,1,0:T(2,128)(2,1)}), bf16[256,2,512]{2,1,0:T(2,128)(2,1)}, u32[]{:S(2)}, u32[]{:S(2)}) %all-to-all-start.1) | async-done | bytes 524320 | tf_op jit(solution)/shard_map/all_to_all | solution.py:119
  95.5 3.6 %reshape.94 = bf16[256,1,1024]{2,1,0:T(2,128)(2,1)S(1)} reshape(bf16[256,2,512]{2,1,0:T(2,128)(2,1)} %all-to-all-done.1) | data formatting | bytes 1048576
  99.2 0.3 fusion.31
  99.4 0.9 fusion.13
  (45 shorter events, 1.2 us)
Async XLA Ops:
  0.6 14.7 %copy-start = (bf16[1024,1024]{1,0:T(8,128)(2,1)S(1)}, bf16[1024,1024]{1,0:T(8,128)(2,1)}, u32[]{:S(2)}) copy-start(bf16[1024,1024]{1,0:T(8,128)(2,1)} %param.28) | copy-start | bytes 6291460
  0.6 10.2 %copy-start.11 = (bf16[8,64,64]{2,1,0:T(8,128)(2,1)S(1)}, bf16[8,64,64]{2,1,0:T(8,128)(2,1)}, u32[]{:S(2)}) copy-start(bf16[8,64,64]{2,1,0:T(8,128)(2,1)} %param.25) | copy-start | bytes 196612
  0.7 6.8 %collective-permute-start = (bf16[48,1024]{1,0:T(8,128)(2,1)}, bf16[48,1024]{1,0:T(8,128)(2,1)S(1)}, u32[]{:S(2)}, u32[]{:S(2)}) collective-permute-start(bf16[48,1024]{1,0:T(8,128)(2,1)} %param.18), channel_id=1, source_target_pairs={{0,1},{1,0},{2,3},{3,2},{4,5},{5,4},{6,7},{7,6},{8,9},{9,8},{10,11... | collective-permute-start | bytes 294920 | tf_op jit(solution)/shard_map/ppermute | solution.py:11
  8.5 2.7 %copy-start.12 = (bf16[8,64,64]{2,1,0:T(8,128)(2,1)S(1)}, bf16[8,64,64]{2,1,0:T(8,128)(2,1)}, u32[]{:S(2)}) copy-start(bf16[8,64,64]{2,1,0:T(8,128)(2,1)} %param.26) | copy-start | bytes 196612
  10.7 0.9 copy-start.5
  10.7 1.0 %copy-start.6 = (f32[2048]{0:T(1024)S(1)}, f32[2048]{0:T(1024)}, u32[]{:S(2)}) copy-start(f32[2048]{0:T(1024)} %param.21) | copy-start | bytes 24580
  11.5 3.8 %copy-start.3 = (bf16[48,1024]{1,0:T(8,128)(2,1)S(1)}, bf16[48,1024]{1,0:T(8,128)(2,1)}, u32[]{:S(2)}) copy-start(bf16[48,1024]{1,0:T(8,128)(2,1)} %param.18) | copy-start | bytes 294916
  11.8 4.0 %copy-start.4 = (f32[48,512]{1,0:T(8,128)}, f32[48,512]{1,0:T(8,128)S(1)}, u32[]{:S(2)}) copy-start(f32[48,512]{1,0:T(8,128)S(1)} %multiply_add_fusion) | copy-start | bytes 294916
  14.0 1.3 %collective-permute-start.1 = (bf16[48,512]{1,0:T(8,128)(2,1)S(1)}, bf16[48,512]{1,0:T(8,128)(2,1)S(1)}, u32[]{:S(2)}, u32[]{:S(2)}) collective-permute-start(bf16[48,512]{1,0:T(8,128)(2,1)S(1)} %fusion.47), channel_id=1, source_target_pairs={{0,1},{1,0},{2,3},{3,2},{4,5},{5,4},{6,7},{7,6},{8,9},{9,8},{10,11... | collective-permute-start | bytes 147464 | tf_op jit(solution)/shard_map/ppermute | solution.py:11
  18.9 33.7 %all-to-all-start = ((bf16[256,2,512]{2,1,0:T(2,128)(2,1)}), bf16[256,2,512]{2,1,0:T(2,128)(2,1)}, u32[]{:S(2)}, u32[]{:S(2)}) async-start(bf16[256,2,512]{2,1,0:T(2,128)(2,1)} %reshape.91), calls=%async_computation | async-start | bytes 1048576 | tf_op jit(solution)/shard_map/all_to_all | solution.py:95
  32.5 27.9 %collective-permute-start.2 = (bf16[2048,256]{1,0:T(8,128)(2,1)}, bf16[2048,256]{1,0:T(8,128)(2,1)}, u32[]{:S(2)}, u32[]{:S(2)}) collective-permute-start(bf16[2048,256]{1,0:T(8,128)(2,1)} %bitcast.66), channel_id=1, source_target_pairs={{0,1},{1,0},{2,3},{3,2},{4,5},{5,4},{6,7},{7,6},{8,9},{9,8},{10,11... | collective-permute-start | bytes 3145736 | tf_op jit(solution)/shard_map/ppermute | solution.py:11
  34.8 27.2 %collective-permute-start.3 = (bf16[2048,256]{1,0:T(8,128)(2,1)}, bf16[2048,256]{1,0:T(8,128)(2,1)}, u32[]{:S(2)}, u32[]{:S(2)}) collective-permute-start(bf16[2048,256]{1,0:T(8,128)(2,1)} %bitcast.71), channel_id=1, source_target_pairs={{0,1},{1,0},{2,3},{3,2},{4,5},{5,4},{6,7},{7,6},{8,9},{9,8},{10,11... | collective-permute-start | bytes 3145736 | tf_op jit(solution)/shard_map/ppermute | solution.py:11
  34.9 28.6 %collective-permute-start.4 = (bf16[256,2048]{1,0:T(8,128)(2,1)}, bf16[256,2048]{1,0:T(8,128)(2,1)}, u32[]{:S(2)}, u32[]{:S(2)}) collective-permute-start(bf16[256,2048]{1,0:T(8,128)(2,1)} %bitcast.63), channel_id=1, source_target_pairs={{0,1},{1,0},{2,3},{3,2},{4,5},{5,4},{6,7},{7,6},{8,9},{9,8},{10,11... | collective-permute-start | bytes 3145736 | tf_op jit(solution)/shard_map/ppermute | solution.py:11
  57.3 0.7 copy-start.7
  57.4 1.2 %copy-start.2 = (bf16[1,2048,256]{2,1,0:T(8,128)(2,1)S(1)}, bf16[1,2048,256]{2,1,0:T(8,128)(2,1)}, u32[]{:S(2)}) copy-start(bf16[1,2048,256]{2,1,0:T(8,128)(2,1)} %param.33) | copy-start | bytes 3145732
  57.6 1.4 %copy-start.10 = (bf16[1,2048,256]{2,1,0:T(8,128)(2,1)S(1)}, bf16[1,2048,256]{2,1,0:T(8,128)(2,1)}, u32[]{:S(2)}) copy-start(bf16[1,2048,256]{2,1,0:T(8,128)(2,1)} %param.34) | copy-start | bytes 3145732
  58.6 1.3 %copy-start.1 = (bf16[1,256,2048]{2,1,0:T(8,128)(2,1)S(1)}, bf16[1,256,2048]{2,1,0:T(8,128)(2,1)}, u32[]{:S(2)}) copy-start(bf16[1,256,2048]{2,1,0:T(8,128)(2,1)} %param.35) | copy-start | bytes 3145732
  66.1 9.2 %copy-start.8 = (f32[48,2]{0,1:T(2,128)S(1)}, f32[48,2]{0,1:T(2,128)}, u32[]{:S(2)}) copy-start(f32[48,2]{0,1:T(2,128)} %param.32) | copy-start | bytes 1156
  66.1 9.2 %copy-start.9 = (f32[48]{0:T(128)S(1)}, f32[48]{0:T(128)}, u32[]{:S(2)}) copy-start(f32[48]{0:T(128)} %param.31) | copy-start | bytes 580
  68.4 27.2 %all-to-all-start.1 = ((bf16[256,2,512]{2,1,0:T(2,128)(2,1)}), bf16[256,2,512]{2,1,0:T(2,128)(2,1)}, u32[]{:S(2)}, u32[]{:S(2)}) async-start(bf16[256,2,512]{2,1,0:T(2,128)(2,1)} %reshape.93), calls=%async_computation.1 | async-start | bytes 1048576 | tf_op jit(solution)/shard_map/all_to_all | solution.py:119

commit v2 on v1

v2 whole, which is shorter than its diff:
```python
import jax
import jax.numpy as jnp
from jax import lax
from jax.experimental import pallas as pl
from jax.experimental.pallas import tpu as pltpu
from jax.sharding import PartitionSpec as P

EPSILON = 1e-06
RATE_SCALE = 8.0
BF16 = jnp.bfloat16
F32 = jnp.float32


def swap(array):
    return lax.ppermute(array, "tp", [(0, 1), (1, 0)])


def iota(shape, dim):
    return lax.broadcasted_iota(jnp.int32, shape, dim)


def mm(left, right):
    return jnp.dot(left, right, preferred_element_type=F32)


def call(body, outs, smem=0):
    def run(*operands):
        specs = [
            pl.BlockSpec(memory_space=pltpu.SMEM if at < smem else pltpu.VMEM)
            for at in range(len(operands))
        ]
        return pl.pallas_call(
            body,
            out_shape=tuple(jax.ShapeDtypeStruct(shape, kind) for shape, kind in outs),
            in_specs=specs,
            out_specs=tuple(pl.BlockSpec(memory_space=pltpu.VMEM) for _ in outs),
            scratch_shapes=getattr(body, "scratch", ()),
            name=body.__name__,
            compiler_params=pltpu.CompilerParams(vmem_limit_bytes=body.room << 20),
        )(*operands)

    return run


def block_diagonal(blocks):
    count, size, _ = blocks.shape
    width = count * size
    tiled = (iota((size, width), 1) % size == iota((size, width), 0)).astype(BF16)
    spread = mm(blocks.reshape(width, size), tiled)
    keep = iota((width, width), 0) // size == iota((width, width), 1) // size
    return jnp.where(keep, spread, 0.0).astype(BF16)


def prepare(recur_ref, input_ref, ids_ref, prob_ref, logit_ref, rd_ref, id_ref, place_ref, pick_ref):
    rd_ref[...] = block_diagonal(recur_ref[...])
    id_ref[...] = block_diagonal(input_ref[...])
    ids = ids_ref[...]
    sequences, top_count = ids.shape
    experts = 128
    lane = iota((sequences, experts), 1)
    onehots = [(ids[:, k : k + 1] == lane).astype(F32) for k in range(top_count)]
    before = (iota((sequences, sequences), 1) < iota((sequences, sequences), 0)).astype(BF16)
    earlier = mm(before, sum(onehots).astype(BF16))
    ranks = [jnp.sum(earlier * one, axis=1, keepdims=True).astype(jnp.int32) for one in onehots]
    logit_exp = jnp.exp(logit_ref[...])
    diagonal = iota((sequences, sequences), 0) == iota((sequences, sequences), 1)
    prob = jnp.sum(jnp.where(diagonal, prob_ref[...], 0.0), axis=1, keepdims=True)
    weights = prob * logit_exp / jnp.sum(logit_exp, axis=1, keepdims=True)
    columns = 4 * experts
    column = iota((sequences, columns), 1)
    for half in range(2):
        place = jnp.zeros((sequences, columns), F32)
        pick = jnp.zeros((sequences, columns), F32)
        for k in range(top_count):
            row = (ranks[k] * experts + ids[:, k : k + 1]) * 2 + half
            here = column == row
            place = jnp.where(here, 1.0, place)
            pick = jnp.where(here, weights[:, k : k + 1], pick)
        span = slice(half * sequences, (half + 1) * sequences)
        place_ref[span, :] = place.astype(BF16)
        high = pick.astype(BF16)
        pick_ref[span, :] = high
        low_span = slice((2 + half) * sequences, (3 + half) * sequences)
        pick_ref[low_span, :] = (pick - high.astype(F32)).astype(BF16)


def expm1(values):
    series = values * (
        1.0
        + values
        * (1 / 2 + values * (1 / 6 + values * (1 / 24 + values * (1 / 120 + values * (1 / 720)))))
    )
    return jnp.where(jnp.abs(values) < 0.25, series, jnp.exp(values) - 1.0)


def mixer(
    core_ref, own_ref, other_ref, gain_ref, branch_ref, gelu_ref, state_ref, taps_ref,
    hidden_ref, rd_ref, id_ref, rate_ref, new_ref, mixed_ref,
):
    core = core_ref[0]
    own = own_ref[...].astype(F32)
    other = other_ref[...].astype(F32)
    half = own.shape[1]
    squares = jnp.sum(own * own + other * other, axis=1, keepdims=True)
    scaling = lax.rsqrt(squares / (2 * half) + EPSILON)
    left, right = gain_ref[:, :half], gain_ref[:, half:]
    own = (own * scaling * jnp.where(core == 0, left, right)).astype(BF16)
    other = (other * scaling * jnp.where(core == 0, right, left)).astype(BF16)
    own_rows = pl.ds(pl.multiple_of(core * half, half), half)
    other_rows = pl.ds(pl.multiple_of((1 - core) * half, half), half)
    branch = (mm(own, branch_ref[own_rows, :]) + mm(other, branch_ref[other_rows, :])).astype(BF16)
    gelu_input = (mm(own, gelu_ref[own_rows, :]) + mm(other, gelu_ref[other_rows, :])).astype(BF16)
    taps = taps_ref.shape[0]
    convolved = branch.astype(F32) * taps_ref[taps - 1 : taps, :]
    for tap in range(taps - 1):
        convolved = convolved + state_ref[:, tap, :].astype(F32) * taps_ref[tap : tap + 1, :]
    convolved = convolved.astype(BF16)
    recur_gate = jax.nn.sigmoid(mm(convolved, rd_ref[...]))
    input_gate = jax.nn.sigmoid(mm(convolved, id_ref[...]))
    log_decay = -RATE_SCALE * recur_gate * rate_ref[...]
    new_hidden = jnp.exp(log_decay) * hidden_ref[...] + jnp.sqrt(-expm1(2.0 * log_decay)) * (
        input_gate * convolved.astype(F32)
    )
    new_ref[...] = new_hidden
    mixed_ref[...] = (new_hidden * jax.nn.gelu(gelu_input.astype(F32), approximate=True)).astype(BF16)


def project(core_ref, tokens_ref, own_ref, other_ref, weight_ref, place_ref, residual_ref, out_ref):
    core = core_ref[0]
    half = own_ref.shape[1]
    own_rows = pl.ds(pl.multiple_of(core * half, half), half)
    other_rows = pl.ds(pl.multiple_of((1 - core) * half, half), half)
    product = mm(own_ref[...], weight_ref[own_rows, :]) + mm(other_ref[...], weight_ref[other_rows, :])
    residual = (tokens_ref[...].astype(F32) + product).astype(BF16)
    residual_ref[...] = residual
    width = residual.shape[1] // 2
    stacked = jnp.concatenate([residual[:, :width], residual[:, width:]], axis=0)
    out_ref[...] = lax.dot_general(
        place_ref[...], stacked, (((0,), (0,)), ((), ())), preferred_element_type=F32
    ).astype(BF16)


def experts_of(
    rows_ref, gain_ref, gate_a, gate_b, up_a, up_b, down_a, down_b, out_ref, scratch_ref
):
    total, width = rows_ref.shape
    slots = total // 4
    pieces = width // 128
    for piece in range(pieces):
        scratch_ref[piece] = rows_ref[:, piece * 128 : (piece + 1) * 128].astype(F32)

    def of_quarter(q):
        return pl.ds((q // 2) * 2 * slots + q % 2, slots, 2)

    quarters = [
        jnp.concatenate([scratch_ref[piece, of_quarter(q), :] for piece in range(pieces)], axis=1)
        for q in range(4)
    ]
    squares = sum(jnp.sum(part * part, axis=1, keepdims=True) for part in quarters)
    scaling = lax.rsqrt(squares / (4 * width) + EPSILON)
    quarters = [
        (part * scaling * gain_ref[:, q * width : (q + 1) * width]).astype(BF16)
        for q, part in enumerate(quarters)
    ]
    rows = jnp.concatenate(quarters, axis=1)
    hidden = []
    for gate_ref, up_ref in ((gate_a, up_a), (gate_b, up_b)):
        gate = mm(rows, gate_ref[...])
        up = mm(rows, up_ref[...])
        hidden.append((jax.nn.silu(gate) * up).astype(BF16))
    for q in range(4):
        span = slice(q * width, (q + 1) * width)
        answer = mm(hidden[0], down_a[:, span]) + mm(hidden[1], down_b[:, span])
        for piece in range(pieces):
            scratch_ref[piece, of_quarter(q), :] = answer[:, piece * 128 : (piece + 1) * 128]
    for piece in range(pieces):
        out_ref[:, piece * 128 : (piece + 1) * 128] = scratch_ref[piece].astype(BF16)


experts_of.scratch = (pltpu.VMEM((4, 512, 128), F32),)


def combine(returned_ref, pick_ref, residual_ref, out_ref):
    found = mm(pick_ref[...], returned_ref[...])
    sequences, width = residual_ref.shape
    width = width // 2
    for half in range(2):
        span = slice(half * width, (half + 1) * width)
        high = found[half * sequences : (half + 1) * sequences]
        low = found[(2 + half) * sequences : (3 + half) * sequences]
        out_ref[:, span] = (residual_ref[:, span].astype(F32) + (high + low)).astype(BF16)


prepare.room, mixer.room, project.room, experts_of.room, combine.room = 8, 16, 8, 20, 8


def exchange(rows):
    total, width = rows.shape
    messages = rows.reshape(total // 2, 2, width)
    arrived = lax.all_to_all(messages, ("tp", "ep"), split_axis=0, concat_axis=0, tiled=True)
    return arrived.reshape(total, width)


def local(
    tokens,
    conv_state,
    hidden_state,
    mixer_gain,
    branch_weight,
    gelu_weight,
    conv_kernel,
    recur_blocks,
    input_blocks,
    decay_rate,
    output_weight,
    expert_gain,
    expert_ids,
    group_prob,
    expert_logit,
    expert_gate,
    expert_up,
    expert_down,
):
    core = lax.axis_index("tp").astype(jnp.int32).reshape(1)
    sequences, half = tokens.shape
    channels = hidden_state.shape[1]
    messages = 2 * lax.axis_size("ep") * lax.axis_size("tp")
    width = half // 2

    other_tokens = swap(tokens)
    recur_full, input_full, place, pick = call(
        prepare,
        (
            ((channels, channels), BF16),
            ((channels, channels), BF16),
            ((2 * sequences, messages), BF16),
            ((4 * sequences, messages), BF16),
        ),
    )(recur_blocks, input_blocks, expert_ids, group_prob[None, :], expert_logit)
    new_hidden, mixed = call(
        mixer, (((sequences, channels), F32), ((sequences, channels), BF16)), smem=1
    )(
        core, tokens, other_tokens, mixer_gain[None, :], branch_weight, gelu_weight,
        conv_state, conv_kernel, hidden_state, recur_full, input_full, decay_rate[None, :],
    )
    other_mixed = swap(mixed)
    residual, outgoing = call(
        project, (((sequences, half), BF16), ((messages, width), BF16)), smem=1
    )(core, tokens, mixed, other_mixed, output_weight, place)
    other_gate, other_up, other_down = swap(expert_gate[0]), swap(expert_up[0]), swap(expert_down[0])
    received = exchange(outgoing)
    (answers,) = call(experts_of, (((messages, width), BF16),))(
        received, expert_gain[None, :], expert_gate[0], other_gate, expert_up[0], other_up,
        expert_down[0], other_down,
    )
    returned = exchange(answers)
    (layer_out,) = call(combine, (((sequences, half), BF16),))(returned, pick, residual)
    return (layer_out, new_hidden)


def solution(mesh):
    return jax.shard_map(
        local,
        mesh=mesh,
        in_specs=(
            P("ep", "tp"),
            P("ep", None, "tp"),
            P("ep", "tp"),
            P(),
            P(None, "tp"),
            P(None, "tp"),
            P(None, "tp"),
            P("tp", None, None),
            P("tp", None, None),
            P("tp"),
            P(None, "tp"),
            P(),
            P("ep", None),
            P("ep"),
            P("ep", None),
            P("ep", None, "tp"),
            P("ep", None, "tp"),
            P("ep", "tp", None),
        ),
        out_specs=(P("ep", "tp"), P("ep", "tp")),
        check_vma=False,
    )
```

time: 101 us -> 87 us (0.86)
  blocking collectives: 0 us -> 59.7 us
  waiting for transfers between devices: 38.5 us -> 0.21 us
  starting transfers between devices: 26.8 us -> 4.31 us
  matrix products: 13.4 us -> 0 us
  Pallas kernels: 0 us -> 7.63 us
  other arithmetic: 6.6 us -> 0 us
    all_to_all x0 -> x2, blocking collectives: none -> 59.7 us  [exchange(): lax.all_to_all(messages, ('tp', 'ep'), split_axis=0, concat_axis=0, tiled...]
    all_to_all x2 -> x0, waiting for transfers between devices: 37.4 us -> none  [the longest x1 20.1 us: local(): lax.all_to_all(answers, ('tp', 'ep'), split_axis=0, concat_axis=0, tiled=...]
    all_to_all x2 -> x0, starting transfers between devices: 20.5 us -> none  [the longest x1 13.6 us: local(): lax.all_to_all(outgoing, ('tp', 'ep'), split_axis=0, concat_axis=0, tiled...]
    dot_general x16 -> x0, matrix products: 13.4 us -> none  [the longest x4 3.02 us: local(): jnp.dot(hidden_units, down_matrix[:, span], preferred_element_type=jnp.fl...]
    pallas_call x0 -> x5, Pallas kernels: none -> 7.63 us  [run(): pl.pallas_call(body, out_shape=tuple((jax.ShapeDtypeStruct(shape, kind) f...]
    all_to_all x3 -> x0, other arithmetic: 2.1 us -> none  [the longest x2 1.07 us: local(): lax.all_to_all(answers, ('tp', 'ep'), split_axis=0, concat_axis=0, tiled=...]
    ppermute x5, starting transfers between devices: 6.24 us -> 4.31 us  [swap(): return lax.ppermute(array, 'tp', [(0, 1), (1, 0)])]
    reshape x1 -> x4, local copies, waits for them, and re-layouts: 0.12 us -> 1.83 us  [the longest x2 1.44 us: exchange(): return arrived.reshape(total, width)]
  transfers between devices with their start and end apart: 7 -> 5, of which waited for: 3 -> 1; matrix products, arithmetic and copies ran while one was open for 13% -> 5% of each run, Pallas kernels for 0% -> 2%
where the time goes in v2:
time: 87 us; the launch traced here: 86.5 us
  blocking collectives  59.7 us (69%)
  local copies, waits for them, and re-layouts  13.9 us (16%)
  Pallas kernels  7.63 us (9%)
  starting transfers between devices  4.31 us (5%)
    all_to_all x2, blocking collectives, exchange(): lax.all_to_all(messages, ('tp', 'ep'), split_axis=0, concat_axis=0, tiled...  59.7 us
    unnamed x31, local copies, waits for them, and re-layouts  12.1 us
    pallas_call x5, Pallas kernels, run(): pl.pallas_call(body, out_shape=tuple((jax.ShapeDtypeStruct(shape, kind) f...  7.63 us
    ppermute x5, starting transfers between devices, swap(): return lax.ppermute(array, 'tp', [(0, 1), (1, 0)])  4.31 us
  transfers between devices with their start and end apart: 5, of which 1 were waited for; matrix products, arithmetic and copies ran while one was open for 5% of the time, Pallas kernels for 2%

profile of v2, /device:TPU:1, one launch (start us, length us, event | category | flops | bytes accessed | tf_op | source)
XLA Modules:
  0.0 86.5 jit_solution(10303351947262406090)
XLA Ops:
  0.6 3.3 %collective-permute-start = (bf16[48,1024]{1,0:T(8,128)(2,1)}, bf16[48,1024]{1,0:T(8,128)(2,1)S(1)}, u32[]{:S(2)}, u32[]{:S(2)}) collective-permute-start(bf16[48,1024]{1,0:T(8,128)(2,1)} %tokens_ref.1), channel_id=1, source_target_pairs={{0,1},{1,0},{2,3},{3,2},{4,5},{5,4},{6,7},{7,6},{8,9},{9,8},{10,11... | collective-permute-start | bytes 294920 | tf_op jit(solution)/shard_map/ppermute | solution.py:15
  3.9 0.8 copy.20.ids_ref
  4.7 0.8 copy.21.logit_ref
  5.4 1.0 %copy.22.state_ref = bf16[48,3,512]{2,1,0:T(4,128)(2,1)S(1)} copy(bf16[48,3,512]{2,0,1:T(8,128)(2,1)} %param.19) | data formatting | bytes 294912 | tf_op args[1]
  6.5 0.0 copy-start.6
  6.5 0.9 %copy-done.6 = bf16[8,64,64]{2,1,0:T(8,128)(2,1)S(1)} copy-done((bf16[8,64,64]{2,1,0:T(8,128)(2,1)S(1)}, bf16[8,64,64]{2,1,0:T(8,128)(2,1)}, u32[]{:S(2)}) %copy-start.6) | copy-done | bytes 65560
  7.4 0.0 copy-start.7
  7.4 0.9 %copy-done.7 = bf16[8,64,64]{2,1,0:T(8,128)(2,1)S(1)} copy-done((bf16[8,64,64]{2,1,0:T(8,128)(2,1)S(1)}, bf16[8,64,64]{2,1,0:T(8,128)(2,1)}, u32[]{:S(2)}) %copy-start.7) | copy-done | bytes 65560
  8.3 0.0 copy-start.13
  8.3 0.7 copy-done.13
  9.0 0.6 prepare.1
  9.6 0.0 collective-permute-done.other_ref
  9.6 0.0 copy-start
  9.6 1.6 %copy-done = bf16[2048,512]{1,0:T(8,128)(2,1)S(1)} copy-done((bf16[2048,512]{1,0:T(8,128)(2,1)S(1)}, bf16[2048,512]{1,0:T(8,128)(2,1)}, u32[]{:S(2)}) %copy-start) | copy-done | bytes 2097176
  11.2 0.0 copy-start.1
  11.2 1.6 %copy-done.1 = bf16[2048,512]{1,0:T(8,128)(2,1)S(1)} copy-done((bf16[2048,512]{1,0:T(8,128)(2,1)S(1)}, bf16[2048,512]{1,0:T(8,128)(2,1)}, u32[]{:S(2)}) %copy-start.1) | copy-done | bytes 2097176
  12.8 0.0 copy-start.5
  12.8 0.9 %copy-done.5 = bf16[48,1024]{1,0:T(8,128)(2,1)S(1)} copy-done((bf16[48,1024]{1,0:T(8,128)(2,1)S(1)}, bf16[48,1024]{1,0:T(8,128)(2,1)}, u32[]{:S(2)}) %copy-start.5) | copy-done | bytes 98328
  13.7 0.0 copy-start.8
  13.7 0.9 %copy-done.8 = f32[48,512]{1,0:T(8,128)S(1)} copy-done((f32[48,512]{1,0:T(8,128)S(1)}, f32[48,512]{1,0:T(8,128)}, u32[]{:S(2)}) %copy-start.8) | copy-done | bytes 98328
  14.6 0.0 copy-start.9
  14.6 0.7 copy-done.9
  15.3 0.0 copy-start.10
  15.3 0.7 copy-done.10
  16.0 0.7 copy-done.12
  16.7 1.8 %mixer.1 = (f32[48,512]{1,0:T(8,128)}, bf16[48,512]{1,0:T(8,128)(2,1)S(1)}) custom-call(s32[1]{0:T(128)} %bitcast.core_ref, bf16[48,1024]{1,0:T(8,128)(2,1)S(1)} %copy-done.5, bf16[48,1024]{1,0:T(8,128)(2,1)S(1)} %collective-permute-done.other_ref, f32[1,2048]{1,0:T(1,128)S(1)} %bitcast.12, bf16[2048,512]{1,0:T(8,128)(2,1)S(1)} %copy-done, ...), custom_call_target="tpu_custom_call" | custom-call | tf_op jit(solution)/shard_map/mixer/pallas_call | solution.py:32
  18.5 0.0 collective-permute-start.1
  18.5 0.0 copy-done.3
  18.5 0.5 collective-permute-start.2
  19.0 0.0 copy-done.4
  19.0 0.1 collective-permute-start.3
  19.1 0.4 collective-permute-start.4
  19.5 0.2 collective-permute-done.1.other_ref
  19.7 0.0 copy-done.2
  19.7 0.7 project.1
  20.5 0.0 copy-start.11
  20.5 0.2 reshape.20
  20.7 33.5 %all_to_all.10 = bf16[256,2,512]{2,1,0:T(2,128)(2,1)} all-to-all(bf16[256,2,512]{2,1,0:T(2,128)(2,1)S(1)} %reshape.20), channel_id=1, replica_groups=mesh['ep'=128,'tp'=2] {'tp','ep'}, dimensions={0} | all-to-all | bytes 1048576 | tf_op jit(solution)/shard_map/all_to_all | solution.py:200
  54.2 1.2 %reshape.21.rows_ref = bf16[512,512]{1,0:T(8,128)(2,1)S(1)} reshape(bf16[256,2,512]{2,1,0:T(2,128)(2,1)} %all_to_all.10) | data formatting | bytes 1048576 | tf_op jit(solution)/shard_map/reshape | solution.py:201
  55.4 0.0 collective-permute-done.2.gate_b
  55.5 0.0 collective-permute-done.3.up_b
  55.5 0.0 collective-permute-done.4.down_b
  55.5 0.0 copy-done.11
  55.5 3.5 %experts_of.1 = bf16[512,512]{1,0:T(8,128)(2,1)S(1)} custom-call(bf16[512,512]{1,0:T(8,128)(2,1)S(1)} %reshape.21.rows_ref, f32[1,2048]{1,0:T(1,128)S(1)} %bitcast.13, bf16[2048,256]{1,0:T(8,128)(2,1)S(1)} %bitcast.9, bf16[2048,256]{1,0:T(8,128)(2,1)} %collective-permute-done.2.gate_b, bf16[2048,256]{1,0:T(8,128)(2,1)S(1)} %bitcast.11, ...), custom_call_target="tpu_custom_call" | custom-call | tf_op jit(solution)/shard_map/experts_of/pallas_call | solution.py:32
  59.0 0.2 reshape.22
  59.2 26.2 %all_to_all.11 = bf16[256,2,512]{2,1,0:T(2,128)(2,1)S(1)} all-to-all(bf16[256,2,512]{2,1,0:T(2,128)(2,1)S(1)} %reshape.22), channel_id=1, replica_groups=mesh['ep'=128,'tp'=2] {'tp','ep'}, dimensions={0} | all-to-all | bytes 1048576 | tf_op jit(solution)/shard_map/all_to_all | solution.py:200
  85.4 0.2 reshape.23.returned_ref
  85.6 0.9 %combine.1 = bf16[48,1024]{1,0:T(8,128)(2,1)} custom-call(bf16[512,512]{1,0:T(8,128)(2,1)S(1)} %reshape.23.returned_ref, bf16[192,512]{1,0:T(8,128)(2,1)S(1)} %get-tuple-element.15.pick_ref, bf16[48,1024]{1,0:T(8,128)(2,1)S(1)} %get-tuple-element.16.residual_ref), custom_call_target="tpu_custom_call" | custom-call | tf_op jit(solution)/shard_map/combine/pallas_call | solution.py:32
  (4 shorter events, 0.0 us)
Async XLA Ops:
  0.6 9.0 %collective-permute-start = (bf16[48,1024]{1,0:T(8,128)(2,1)}, bf16[48,1024]{1,0:T(8,128)(2,1)S(1)}, u32[]{:S(2)}, u32[]{:S(2)}) collective-permute-start(bf16[48,1024]{1,0:T(8,128)(2,1)} %tokens_ref.1), channel_id=1, source_target_pairs={{0,1},{1,0},{2,3},{3,2},{4,5},{5,4},{6,7},{7,6},{8,9},{9,8},{10,11... | collective-permute-start | bytes 294920 | tf_op jit(solution)/shard_map/ppermute | solution.py:15
  6.5 0.9 %copy-start.6 = (bf16[8,64,64]{2,1,0:T(8,128)(2,1)S(1)}, bf16[8,64,64]{2,1,0:T(8,128)(2,1)}, u32[]{:S(2)}) copy-start(bf16[8,64,64]{2,1,0:T(8,128)(2,1)} %recur_ref.1) | copy-start | bytes 196612
  7.4 0.9 %copy-start.7 = (bf16[8,64,64]{2,1,0:T(8,128)(2,1)S(1)}, bf16[8,64,64]{2,1,0:T(8,128)(2,1)}, u32[]{:S(2)}) copy-start(bf16[8,64,64]{2,1,0:T(8,128)(2,1)} %input_ref.1) | copy-start | bytes 196612
  8.3 0.7 copy-start.13
  9.6 1.6 %copy-start = (bf16[2048,512]{1,0:T(8,128)(2,1)S(1)}, bf16[2048,512]{1,0:T(8,128)(2,1)}, u32[]{:S(2)}) copy-start(bf16[2048,512]{1,0:T(8,128)(2,1)} %branch_ref.1) | copy-start | bytes 6291460
  11.2 1.6 %copy-start.1 = (bf16[2048,512]{1,0:T(8,128)(2,1)S(1)}, bf16[2048,512]{1,0:T(8,128)(2,1)}, u32[]{:S(2)}) copy-start(bf16[2048,512]{1,0:T(8,128)(2,1)} %gelu_ref.1) | copy-start | bytes 6291460
  12.8 0.9 %copy-start.5 = (bf16[48,1024]{1,0:T(8,128)(2,1)S(1)}, bf16[48,1024]{1,0:T(8,128)(2,1)}, u32[]{:S(2)}) copy-start(bf16[48,1024]{1,0:T(8,128)(2,1)} %tokens_ref.1) | copy-start | bytes 294916
  13.7 0.9 %copy-start.8 = (f32[48,512]{1,0:T(8,128)S(1)}, f32[48,512]{1,0:T(8,128)}, u32[]{:S(2)}) copy-start(f32[48,512]{1,0:T(8,128)} %hidden_ref.1) | copy-start | bytes 294916
  14.6 0.7 copy-start.9
  15.3 0.7 copy-start.10
  16.0 0.7 copy-start.12
  16.7 1.8 %copy-start.3 = (bf16[1,2048,256]{2,1,0:T(8,128)(2,1)S(1)}, bf16[1,2048,256]{2,1,0:T(8,128)(2,1)}, u32[]{:S(2)}) copy-start(bf16[1,2048,256]{2,1,0:T(8,128)(2,1)} %param.33) | copy-start | bytes 3145732
  16.7 2.3 %copy-start.4 = (bf16[1,2048,256]{2,1,0:T(8,128)(2,1)S(1)}, bf16[1,2048,256]{2,1,0:T(8,128)(2,1)}, u32[]{:S(2)}) copy-start(bf16[1,2048,256]{2,1,0:T(8,128)(2,1)} %param.34) | copy-start | bytes 3145732
  16.7 3.0 %copy-start.2 = (bf16[1024,1024]{1,0:T(8,128)(2,1)S(1)}, bf16[1024,1024]{1,0:T(8,128)(2,1)}, u32[]{:S(2)}) copy-start(bf16[1024,1024]{1,0:T(8,128)(2,1)} %weight_ref.1) | copy-start | bytes 6291460
  18.5 1.2 %collective-permute-start.1 = (bf16[48,512]{1,0:T(8,128)(2,1)S(1)}, bf16[48,512]{1,0:T(8,128)(2,1)S(1)}, u32[]{:S(2)}, u32[]{:S(2)}) collective-permute-start(bf16[48,512]{1,0:T(8,128)(2,1)S(1)} %get-tuple-element.12.own_ref), channel_id=1, source_target_pairs={{0,1},{1,0},{2,3},{3,2},{4,5},{5,4},{6,7},{7,6},{8,9},{9,8},{10,11... | collective-permute-start | bytes 147464 | tf_op jit(solution)/shard_map/ppermute | solution.py:15
  18.5 36.9 %collective-permute-start.2 = (bf16[2048,256]{1,0:T(8,128)(2,1)S(1)}, bf16[2048,256]{1,0:T(8,128)(2,1)}, u32[]{:S(2)}, u32[]{:S(2)}) collective-permute-start(bf16[2048,256]{1,0:T(8,128)(2,1)S(1)} %bitcast.8), channel_id=1, source_target_pairs={{0,1},{1,0},{2,3},{3,2},{4,5},{5,4},{6,7},{7,6},{8,9},{9,8},{10,11... | collective-permute-start | bytes 3145736 | tf_op jit(solution)/shard_map/ppermute | solution.py:15
  19.0 36.5 %collective-permute-start.3 = (bf16[2048,256]{1,0:T(8,128)(2,1)S(1)}, bf16[2048,256]{1,0:T(8,128)(2,1)}, u32[]{:S(2)}, u32[]{:S(2)}) collective-permute-start(bf16[2048,256]{1,0:T(8,128)(2,1)S(1)} %bitcast.10), channel_id=1, source_target_pairs={{0,1},{1,0},{2,3},{3,2},{4,5},{5,4},{6,7},{7,6},{8,9},{9,8},{10,11... | collective-permute-start | bytes 3145736 | tf_op jit(solution)/shard_map/ppermute | solution.py:15
  19.1 36.4 %collective-permute-start.4 = (bf16[256,2048]{1,0:T(8,128)(2,1)}, bf16[256,2048]{1,0:T(8,128)(2,1)}, u32[]{:S(2)}, u32[]{:S(2)}) collective-permute-start(bf16[256,2048]{1,0:T(8,128)(2,1)} %bitcast.7.down_a), channel_id=1, source_target_pairs={{0,1},{1,0},{2,3},{3,2},{4,5},{5,4},{6,7},{7,6},{8,9},{9,8},{10,11... | collective-permute-start | bytes 3145736 | tf_op jit(solution)/shard_map/ppermute | solution.py:15
  20.5 35.0 %copy-start.11 = (f32[2048]{0:T(1024)S(1)}, f32[2048]{0:T(1024)}, u32[]{:S(2)}) copy-start(f32[2048]{0:T(1024)} %param.29) | copy-start | bytes 24580

commit v3 on v2

--- a/solution.py
+++ b/solution.py
@@ -23,23 +23,36 @@
     return jnp.dot(left, right, preferred_element_type=F32)
 
 
-def call(body, outs, smem=0):
-    def run(*operands):
-        specs = [
-            pl.BlockSpec(memory_space=pltpu.SMEM if at < smem else pltpu.VMEM)
-            for at in range(len(operands))
-        ]
-        return pl.pallas_call(
-            body,
-            out_shape=tuple(jax.ShapeDtypeStruct(shape, kind) for shape, kind in outs),
-            in_specs=specs,
-            out_specs=tuple(pl.BlockSpec(memory_space=pltpu.VMEM) for _ in outs),
-            scratch_shapes=getattr(body, "scratch", ()),
-            name=body.__name__,
-            compiler_params=pltpu.CompilerParams(vmem_limit_bytes=body.room << 20),
-        )(*operands)
-
-    return run
+def call(body, outs, spaces):
+    places = {"s": pltpu.SMEM, "v": pltpu.VMEM, "V": pltpu.VMEM, "h": pltpu.HBM}
+    run = pl.pallas_call(
+        body,
+        out_shape=tuple(jax.ShapeDtypeStruct(shape, kind) for shape, kind in outs),
+        in_specs=[pl.BlockSpec(memory_space=places[space]) for space in spaces],
+        out_specs=tuple(pl.BlockSpec(memory_space=pltpu.VMEM) for _ in outs),
+        scratch_shapes=getattr(body, "scratch", ()),
+        name=body.__name__,
+        compiler_params=pltpu.CompilerParams(vmem_limit_bytes=body.room << 20),
+    )
+
+    def placed(*operands):
+        return run(
+            *(
+                pltpu.with_memory_space_constraint(operand, places[space])
+                if space in "Vh"
+                else operand
+                for operand, space in zip(operands, spaces)
+            )
+        )
+
+    return placed
+
+
+def half_of(ref, core, other, dim):
+    size = ref.shape[dim] // 2
+    start = (1 - core if other else core) * size
+    span = pl.ds(pl.multiple_of(start, size), size)
+    return ref.at[span, :] if dim == 0 else ref.at[:, span]
 
 
 def block_diagonal(blocks):
@@ -51,31 +64,33 @@
     return jnp.where(keep, spread, 0.0).astype(BF16)
 
 
-def prepare(recur_ref, input_ref, ids_ref, prob_ref, logit_ref, rd_ref, id_ref, place_ref, pick_ref):
-    rd_ref[...] = block_diagonal(recur_ref[...])
-    id_ref[...] = block_diagonal(input_ref[...])
-    ids = ids_ref[...]
-    sequences, top_count = ids.shape
-    experts = 128
+def as_column(row):
+    size = row.shape[1]
+    diagonal = iota((size, size), 0) == iota((size, size), 1)
+    return jnp.sum(jnp.where(diagonal, row, 0.0), axis=1, keepdims=True)
+
+
+def route(ids_ref, prob_ref, logit_ref, place_ref, pick_ref):
+    top_count, sequences = ids_ref.shape
+    columns = place_ref.shape[1]
+    experts = columns // 4
+    rows = [ids_ref[k : k + 1, :].astype(F32) for k in range(top_count)]
+    ids = [as_column(row).astype(jnp.int32) for row in rows]
     lane = iota((sequences, experts), 1)
-    onehots = [(ids[:, k : k + 1] == lane).astype(F32) for k in range(top_count)]
+    onehots = [(one == lane).astype(F32) for one in ids]
     before = (iota((sequences, sequences), 1) < iota((sequences, sequences), 0)).astype(BF16)
     earlier = mm(before, sum(onehots).astype(BF16))
     ranks = [jnp.sum(earlier * one, axis=1, keepdims=True).astype(jnp.int32) for one in onehots]
-    logit_exp = jnp.exp(logit_ref[...])
-    diagonal = iota((sequences, sequences), 0) == iota((sequences, sequences), 1)
-    prob = jnp.sum(jnp.where(diagonal, prob_ref[...], 0.0), axis=1, keepdims=True)
-    weights = prob * logit_exp / jnp.sum(logit_exp, axis=1, keepdims=True)
-    columns = 4 * experts
+    logit_exp = [jnp.exp(logit_ref[k : k + 1, :]) for k in range(top_count)]
+    weights = [as_column(prob_ref[...] * one / sum(logit_exp)) for one in logit_exp]
     column = iota((sequences, columns), 1)
     for half in range(2):
         place = jnp.zeros((sequences, columns), F32)
         pick = jnp.zeros((sequences, columns), F32)
         for k in range(top_count):
-            row = (ranks[k] * experts + ids[:, k : k + 1]) * 2 + half
-            here = column == row
+            here = column == (ranks[k] * experts + ids[k]) * 2 + half
             place = jnp.where(here, 1.0, place)
-            pick = jnp.where(here, weights[:, k : k + 1], pick)
+            pick = jnp.where(here, weights[k], pick)
         span = slice(half * sequences, (half + 1) * sequences)
         place_ref[span, :] = place.astype(BF16)
         high = pick.astype(BF16)
@@ -84,6 +99,70 @@
         pick_ref[low_span, :] = (pick - high.astype(F32)).astype(BF16)
 
 
+def begin(
+    core_ref, tokens_hbm, gain_hbm, branch_hbm, gelu_hbm, recur_hbm, input_hbm, ids_hbm, prob_hbm,
+    logit_hbm, state_hbm, taps_hbm, hidden_hbm, rate_hbm,
+    tokens_ref, gain_ref, branch_ref, gelu_ref, state_ref, taps_ref, hidden_ref, rate_ref,
+    rd_ref, id_ref, place_ref, pick_ref, branch_part, gelu_part, squares_ref,
+    own_gain, own_branch, own_gelu, recur_ref, input_ref, ids_ref, prob_ref, logit_ref, sems,
+):
+    core = core_ref[0]
+    pairs = (
+        (tokens_hbm, tokens_ref),
+        (half_of(gain_hbm, core, False, 1), own_gain),
+        (half_of(branch_hbm, core, False, 0), own_branch),
+        (half_of(gelu_hbm, core, False, 0), own_gelu),
+        (ids_hbm, ids_ref),
+        (prob_hbm, prob_ref),
+        (logit_hbm, logit_ref),
+        (recur_hbm, recur_ref),
+        (input_hbm, input_ref),
+        (half_of(branch_hbm, core, True, 0), branch_ref),
+        (half_of(gelu_hbm, core, True, 0), gelu_ref),
+        (half_of(gain_hbm, core, True, 1), gain_ref),
+        (state_hbm, state_ref),
+        (taps_hbm, taps_ref),
+        (hidden_hbm, hidden_ref),
+        (rate_hbm, rate_ref),
+    )
+    copies = [
+        pltpu.make_async_copy(source, target, sems.at[at]) for at, (source, target) in enumerate(pairs)
+    ]
+    for copy in copies:
+        copy.start()
+    for copy in copies[4:7]:
+        copy.wait()
+    route(ids_ref, prob_ref, logit_ref, place_ref, pick_ref)
+    for copy in copies[7:9]:
+        copy.wait()
+    rd_ref[...] = block_diagonal(recur_ref[...])
+    id_ref[...] = block_diagonal(input_ref[...])
+    for copy in copies[:2]:
+        copy.wait()
+    own = tokens_ref[...].astype(F32)
+    squares_ref[...] = jnp.sum(own * own, axis=1, keepdims=True)
+    own = (own * own_gain[...]).astype(BF16)
+    copies[2].wait()
+    branch_part[...] = mm(own, own_branch[...])
+    copies[3].wait()
+    gelu_part[...] = mm(own, own_gelu[...])
+    for copy in copies[9:]:
+        copy.wait()
+
+
+begin.scratch = (
+    pltpu.VMEM((1, 1024), F32),
+    pltpu.VMEM((1024, 512), BF16),
+    pltpu.VMEM((1024, 512), BF16),
+    pltpu.VMEM((8, 64, 64), BF16),
+    pltpu.VMEM((8, 64, 64), BF16),
+    pltpu.VMEM((2, 48), jnp.int32),
+    pltpu.VMEM((1, 48), F32),
+    pltpu.VMEM((2, 48), F32),
+    pltpu.SemaphoreType.DMA((16,)),
+)
+
+
 def expm1(values):
     series = values * (
         1.0
@@ -94,26 +173,20 @@
 
 
 def mixer(
-    core_ref, own_ref, other_ref, gain_ref, branch_ref, gelu_ref, state_ref, taps_ref,
-    hidden_ref, rd_ref, id_ref, rate_ref, new_ref, mixed_ref,
+    other_ref, squares_ref, gain_ref, branch_ref, gelu_ref, branch_part, gelu_part, state_ref,
+    taps_ref, hidden_ref, rate_ref, rd_ref, id_ref, new_ref, mixed_ref,
 ):
-    core = core_ref[0]
-    own = own_ref[...].astype(F32)
     other = other_ref[...].astype(F32)
-    half = own.shape[1]
-    squares = jnp.sum(own * own + other * other, axis=1, keepdims=True)
+    half = other.shape[1]
+    squares = squares_ref[...] + jnp.sum(other * other, axis=1, keepdims=True)
     scaling = lax.rsqrt(squares / (2 * half) + EPSILON)
-    left, right = gain_ref[:, :half], gain_ref[:, half:]
-    own = (own * scaling * jnp.where(core == 0, left, right)).astype(BF16)
-    other = (other * scaling * jnp.where(core == 0, right, left)).astype(BF16)
-    own_rows = pl.ds(pl.multiple_of(core * half, half), half)
-    other_rows = pl.ds(pl.multiple_of((1 - core) * half, half), half)
-    branch = (mm(own, branch_ref[own_rows, :]) + mm(other, branch_ref[other_rows, :])).astype(BF16)
-    gelu_input = (mm(own, gelu_ref[own_rows, :]) + mm(other, gelu_ref[other_rows, :])).astype(BF16)
+    other = (other * gain_ref[...]).astype(BF16)
+    branch = ((branch_part[...] + mm(other, branch_ref[...])) * scaling).astype(BF16)
+    gelu_input = ((gelu_part[...] + mm(other, gelu_ref[...])) * scaling).astype(BF16)
     taps = taps_ref.shape[0]
     convolved = branch.astype(F32) * taps_ref[taps - 1 : taps, :]
     for tap in range(taps - 1):
-        convolved = convolved + state_ref[:, tap, :].astype(F32) * taps_ref[tap : tap + 1, :]
+        convolved = convolved + state_ref[tap].astype(F32) * taps_ref[tap : tap + 1, :]
     convolved = convolved.astype(BF16)
     recur_gate = jax.nn.sigmoid(mm(convolved, rd_ref[...]))
     input_gate = jax.nn.sigmoid(mm(convolved, id_ref[...]))
@@ -141,8 +214,15 @@
 
 
 def experts_of(
-    rows_ref, gain_ref, gate_a, gate_b, up_a, up_b, down_a, down_b, out_ref, scratch_ref
+    rows_ref, gain_ref, gate_a, up_a, down_a_hbm, gate_b_hbm, up_b_hbm, down_b_hbm, out_ref,
+    down_a, gate_b, up_b, down_b, scratch_ref, sems,
 ):
+    pairs = ((gate_b_hbm, gate_b), (up_b_hbm, up_b), (down_a_hbm, down_a), (down_b_hbm, down_b))
+    copies = [
+        pltpu.make_async_copy(source, target, sems.at[at]) for at, (source, target) in enumerate(pairs)
+    ]
+    for copy in copies:
+        copy.start()
     total, width = rows_ref.shape
     slots = total // 4
     pieces = width // 128
@@ -163,11 +243,13 @@
         for q, part in enumerate(quarters)
     ]
     rows = jnp.concatenate(quarters, axis=1)
-    hidden = []
-    for gate_ref, up_ref in ((gate_a, up_a), (gate_b, up_b)):
-        gate = mm(rows, gate_ref[...])
-        up = mm(rows, up_ref[...])
-        hidden.append((jax.nn.silu(gate) * up).astype(BF16))
+    hidden = [(jax.nn.silu(mm(rows, gate_a[...])) * mm(rows, up_a[...])).astype(BF16)]
+    copies[0].wait()
+    gate = jax.nn.silu(mm(rows, gate_b[...]))
+    copies[1].wait()
+    hidden.append((gate * mm(rows, up_b[...])).astype(BF16))
+    copies[2].wait()
+    copies[3].wait()
     for q in range(4):
         span = slice(q * width, (q + 1) * width)
         answer = mm(hidden[0], down_a[:, span]) + mm(hidden[1], down_b[:, span])
@@ -177,7 +259,14 @@
         out_ref[:, piece * 128 : (piece + 1) * 128] = scratch_ref[piece].astype(BF16)
 
 
-experts_of.scratch = (pltpu.VMEM((4, 512, 128), F32),)
+experts_of.scratch = (
+    pltpu.VMEM((256, 2048), BF16),
+    pltpu.VMEM((2048, 256), BF16),
+    pltpu.VMEM((2048, 256), BF16),
+    pltpu.VMEM((256, 2048), BF16),
+    pltpu.VMEM((4, 512, 128), F32),
+    pltpu.SemaphoreType.DMA((4,)),
+)
 
 
 def combine(returned_ref, pick_ref, residual_ref, out_ref):
@@ -191,7 +280,7 @@
         out_ref[:, span] = (residual_ref[:, span].astype(F32) + (high + low)).astype(BF16)
 
 
-prepare.room, mixer.room, project.room, experts_of.room, combine.room = 8, 16, 8, 20, 8
+begin.room, mixer.room, project.room, experts_of.room, combine.room = 8, 6, 6, 12, 6
 
 
 def exchange(rows):
@@ -228,33 +317,49 @@
     width = half // 2
 
     other_tokens = swap(tokens)
-    recur_full, input_full, place, pick = call(
-        prepare,
-        (
-            ((channels, channels), BF16),
-            ((channels, channels), BF16),
-            ((2 * sequences, messages), BF16),
-            ((4 * sequences, messages), BF16),
-        ),
-    )(recur_blocks, input_blocks, expert_ids, group_prob[None, :], expert_logit)
+    kinds = (
+        ((sequences, half), BF16),
+        ((1, half), F32),
+        ((half, channels), BF16),
+        ((half, channels), BF16),
+        ((3, sequences, channels), BF16),
+        ((4, channels), F32),
+        ((sequences, channels), F32),
+        ((1, channels), F32),
+        ((channels, channels), BF16),
+        ((channels, channels), BF16),
+        ((2 * sequences, messages), BF16),
+        ((4 * sequences, messages), BF16),
+        ((sequences, channels), F32),
+        ((sequences, channels), F32),
+        ((sequences, 1), F32),
+    )
+    (
+        own_tokens, gain, branch_rows, gelu_rows, state, taps, hidden, rate, recur_full, input_full,
+        place, pick, branch_part, gelu_part, squares,
+    ) = call(begin, kinds, "s" + "h" * 13)(
+        core, tokens, mixer_gain[None, :], branch_weight, gelu_weight, recur_blocks, input_blocks,
+        expert_ids.T, group_prob[None, :], expert_logit.T, jnp.transpose(conv_state, (1, 0, 2)),
+        conv_kernel, hidden_state, decay_rate[None, :],
+    )
     new_hidden, mixed = call(
-        mixer, (((sequences, channels), F32), ((sequences, channels), BF16)), smem=1
+        mixer, (((sequences, channels), F32), ((sequences, channels), BF16)), "v" * 13
     )(
-        core, tokens, other_tokens, mixer_gain[None, :], branch_weight, gelu_weight,
-        conv_state, conv_kernel, hidden_state, recur_full, input_full, decay_rate[None, :],
+        other_tokens, squares, gain, branch_rows, gelu_rows, branch_part, gelu_part, state, taps,
+        hidden, rate, recur_full, input_full,
     )
     other_mixed = swap(mixed)
     residual, outgoing = call(
-        project, (((sequences, half), BF16), ((messages, width), BF16)), smem=1
-    )(core, tokens, mixed, other_mixed, output_weight, place)
+        project, (((sequences, half), BF16), ((messages, width), BF16)), "s" + "v" * 5
+    )(core, own_tokens, mixed, other_mixed, output_weight, place)
     other_gate, other_up, other_down = swap(expert_gate[0]), swap(expert_up[0]), swap(expert_down[0])
     received = exchange(outgoing)
-    (answers,) = call(experts_of, (((messages, width), BF16),))(
-        received, expert_gain[None, :], expert_gate[0], other_gate, expert_up[0], other_up,
-        expert_down[0], other_down,
+    (answers,) = call(experts_of, (((messages, width), BF16),), "vvvvhhhh")(
+        received, expert_gain[None, :], expert_gate[0], expert_up[0], expert_down[0], other_gate,
+        other_up, other_down,
     )
     returned = exchange(answers)
-    (layer_out,) = call(combine, (((sequences, half), BF16),))(returned, pick, residual)
+    (layer_out,) = call(combine, (((sequences, half), BF16),), "vvv")(returned, pick, residual)
     return (layer_out, new_hidden)
 
 

time: 87 us -> 76.4 us (0.88)
  local copies, waits for them, and re-layouts: 13.9 us -> 1.86 us
  Pallas kernels: 7.63 us -> 9.41 us
    unnamed x31 -> x8, local copies, waits for them, and re-layouts: 12.1 us -> 0.02 us
    pallas_call x5, Pallas kernels: 7.63 us -> 9.41 us  [placed(): run(*(pltpu.with_memory_space_constraint(operand, places[space]) if space...]
  transfers between devices with their start and end apart: 5 -> 5, of which waited for: 1 -> 1; matrix products, arithmetic and copies ran while one was open for 5% -> 2% of each run, Pallas kernels for 2% -> 5%
where the time goes in v3:
time: 76.4 us; the launch traced here: 76.2 us
  blocking collectives  59.7 us (78%)
  Pallas kernels  9.41 us (12%)
  starting transfers between devices  4.31 us (6%)
  local copies, waits for them, and re-layouts  1.86 us (2%)
    all_to_all x2, blocking collectives, exchange(): lax.all_to_all(messages, ('tp', 'ep'), split_axis=0, concat_axis=0, tiled...  59.7 us
    pallas_call x5, Pallas kernels, placed(): run(*(pltpu.with_memory_space_constraint(operand, places[space]) if space...  9.41 us
    ppermute x5, starting transfers between devices, swap(): return lax.ppermute(array, 'tp', [(0, 1), (1, 0)])  4.31 us
  transfers between devices with their start and end apart: 5, of which 1 were waited for; matrix products, arithmetic and copies ran while one was open for 2% of the time, Pallas kernels for 5%

profile of v3, /device:TPU:1, one launch (start us, length us, event | category | flops | bytes accessed | tf_op | source)
XLA Modules:
  0.0 76.2 jit_solution(7543342738671943463)
XLA Ops:
  0.6 3.3 %collective-permute-start = (bf16[48,1024]{1,0:T(8,128)(2,1)}, bf16[48,1024]{1,0:T(8,128)(2,1)S(1)}, u32[]{:S(2)}, u32[]{:S(2)}) collective-permute-start(bf16[48,1024]{1,0:T(8,128)(2,1)} %tokens_hbm.1), channel_id=1, source_target_pairs={{0,1},{1,0},{2,3},{3,2},{4,5},{5,4},{6,7},{7,6},{8,9},{9,8},{10,11... | collective-permute-start | bytes 294920 | tf_op jit(solution)/shard_map/ppermute | solution.py:15
  3.9 0.0 copy-start.2
  3.9 3.2 %begin.1 = (bf16[48,1024]{1,0:T(8,128)(2,1)S(1)}, f32[1,1024]{1,0:T(1,128)S(1)}, bf16[1024,512]{1,0:T(8,128)(2,1)S(1)}, bf16[1024,512]{1,0:T(8,128)(2,1)S(1)}, b...) custom-call(s32[1]{0:T(128)} %bitcast.core_ref, ...), custom_call_target="tpu_custom_call" | custom-call | tf_op jit(solution)/shard_map/begin/pallas_call | solution.py:39
  7.1 0.0 copy-start.1
  7.1 0.0 copy-start
  7.1 0.0 collective-permute-done.other_ref
  7.1 1.4 %mixer.1 = (f32[48,512]{1,0:T(8,128)}, bf16[48,512]{1,0:T(8,128)(2,1)S(1)}) custom-call(bf16[48,1024]{1,0:T(8,128)(2,1)S(1)} %collective-permute-done.other_ref, f32[48,1]{1,0:T(8,128)S(1)} %get-tuple-element.22.squares_ref, f32[1,1024]{1,0:T(1,128)S(1)} %get-tuple-element.23.gain_ref, bf16[1024,512]{1,0:T(8,128)(2,1)S(1)} %get-tuple-element.24.branch_ref, ...), custom_call_target="tpu_custom_call" | custom-call | tf_op jit(solution)/shard_map/mixer/pallas_call | solution.py:39
  8.5 0.0 collective-permute-start.1
  8.6 0.0 copy-done.1
  8.6 0.5 collective-permute-start.2
  9.0 0.0 copy-done.2
  9.0 0.1 collective-permute-start.3
  9.1 0.4 collective-permute-start.4
  9.5 0.2 collective-permute-done.1.other_ref
  9.8 0.0 copy-done
  9.8 0.7 project.1
  10.5 0.0 copy-start.3
  10.5 0.2 reshape.20
  10.7 33.5 %all_to_all.10 = bf16[256,2,512]{2,1,0:T(2,128)(2,1)} all-to-all(bf16[256,2,512]{2,1,0:T(2,128)(2,1)S(1)} %reshape.20), channel_id=1, replica_groups=mesh['ep'=128,'tp'=2] {'tp','ep'}, dimensions={0} | all-to-all | bytes 1048576 | tf_op jit(solution)/shard_map/all_to_all | solution.py:289
  44.2 1.2 %reshape.21.rows_ref = bf16[512,512]{1,0:T(8,128)(2,1)S(1)} reshape(bf16[256,2,512]{2,1,0:T(2,128)(2,1)} %all_to_all.10) | data formatting | bytes 1048576 | tf_op jit(solution)/shard_map/reshape | solution.py:290
  45.5 0.0 collective-permute-done.2.gate_b_hbm
  45.5 0.0 collective-permute-done.3.up_b_hbm
  45.5 0.0 collective-permute-done.4.down_b_hbm
  45.5 0.0 copy-done.3
  45.5 3.2 %experts_of.1 = bf16[512,512]{1,0:T(8,128)(2,1)S(1)} custom-call(bf16[512,512]{1,0:T(8,128)(2,1)S(1)} %reshape.21.rows_ref, f32[1,2048]{1,0:T(1,128)S(1)} %bitcast.15, bf16[2048,256]{1,0:T(8,128)(2,1)S(1)} %bitcast.12, bf16[2048,256]{1,0:T(8,128)(2,1)S(1)} %bitcast.14, bf16[256,2048]{1,0:T(8,128)(2,1)} %bitcast.10.down_a_hbm, ...), custom_call_target="tpu_custom_call" | custom-call | tf_op jit(solution)/shard_map/experts_of/pallas_call | solution.py:39
  48.7 0.2 reshape.22
  48.9 26.2 %all_to_all.11 = bf16[256,2,512]{2,1,0:T(2,128)(2,1)S(1)} all-to-all(bf16[256,2,512]{2,1,0:T(2,128)(2,1)S(1)} %reshape.22), channel_id=1, replica_groups=mesh['ep'=128,'tp'=2] {'tp','ep'}, dimensions={0} | all-to-all | bytes 1048576 | tf_op jit(solution)/shard_map/all_to_all | solution.py:289
  75.1 0.2 reshape.23.returned_ref
  75.3 0.9 %combine.1 = bf16[48,1024]{1,0:T(8,128)(2,1)} custom-call(bf16[512,512]{1,0:T(8,128)(2,1)S(1)} %reshape.23.returned_ref, bf16[192,512]{1,0:T(8,128)(2,1)S(1)} %get-tuple-element.37.pick_ref, bf16[48,1024]{1,0:T(8,128)(2,1)S(1)} %get-tuple-element.38.residual_ref), custom_call_target="tpu_custom_call" | custom-call | tf_op jit(solution)/shard_map/combine/pallas_call | solution.py:39
Async XLA Ops:
  0.6 6.5 %collective-permute-start = (bf16[48,1024]{1,0:T(8,128)(2,1)}, bf16[48,1024]{1,0:T(8,128)(2,1)S(1)}, u32[]{:S(2)}, u32[]{:S(2)}) collective-permute-start(bf16[48,1024]{1,0:T(8,128)(2,1)} %tokens_hbm.1), channel_id=1, source_target_pairs={{0,1},{1,0},{2,3},{3,2},{4,5},{5,4},{6,7},{7,6},{8,9},{9,8},{10,11... | collective-permute-start | bytes 294920 | tf_op jit(solution)/shard_map/ppermute | solution.py:15
  3.9 5.1 %copy-start.2 = (bf16[1,2048,256]{2,1,0:T(8,128)(2,1)S(1)}, bf16[1,2048,256]{2,1,0:T(8,128)(2,1)}, u32[]{:S(2)}) copy-start(bf16[1,2048,256]{2,1,0:T(8,128)(2,1)} %param.34) | copy-start | bytes 3145732
  7.1 1.5 %copy-start.1 = (bf16[1,2048,256]{2,1,0:T(8,128)(2,1)S(1)}, bf16[1,2048,256]{2,1,0:T(8,128)(2,1)}, u32[]{:S(2)}) copy-start(bf16[1,2048,256]{2,1,0:T(8,128)(2,1)} %param.33) | copy-start | bytes 3145732
  7.1 2.6 %copy-start = (bf16[1024,1024]{1,0:T(8,128)(2,1)S(1)}, bf16[1024,1024]{1,0:T(8,128)(2,1)}, u32[]{:S(2)}) copy-start(bf16[1024,1024]{1,0:T(8,128)(2,1)} %weight_ref.1) | copy-start | bytes 6291460
  8.5 1.2 %collective-permute-start.1 = (bf16[48,512]{1,0:T(8,128)(2,1)S(1)}, bf16[48,512]{1,0:T(8,128)(2,1)S(1)}, u32[]{:S(2)}, u32[]{:S(2)}) collective-permute-start(bf16[48,512]{1,0:T(8,128)(2,1)S(1)} %get-tuple-element.34.own_ref), channel_id=1, source_target_pairs={{0,1},{1,0},{2,3},{3,2},{4,5},{5,4},{6,7},{7,6},{8,9},{9,8},{10,11... | collective-permute-start | bytes 147464 | tf_op jit(solution)/shard_map/ppermute | solution.py:15
  8.6 36.9 %collective-permute-start.2 = (bf16[2048,256]{1,0:T(8,128)(2,1)S(1)}, bf16[2048,256]{1,0:T(8,128)(2,1)}, u32[]{:S(2)}, u32[]{:S(2)}) collective-permute-start(bf16[2048,256]{1,0:T(8,128)(2,1)S(1)} %bitcast.11), channel_id=1, source_target_pairs={{0,1},{1,0},{2,3},{3,2},{4,5},{5,4},{6,7},{7,6},{8,9},{9,8},{10,11... | collective-permute-start | bytes 3145736 | tf_op jit(solution)/shard_map/ppermute | solution.py:15
  9.0 36.5 %collective-permute-start.3 = (bf16[2048,256]{1,0:T(8,128)(2,1)S(1)}, bf16[2048,256]{1,0:T(8,128)(2,1)}, u32[]{:S(2)}, u32[]{:S(2)}) collective-permute-start(bf16[2048,256]{1,0:T(8,128)(2,1)S(1)} %bitcast.13), channel_id=1, source_target_pairs={{0,1},{1,0},{2,3},{3,2},{4,5},{5,4},{6,7},{7,6},{8,9},{9,8},{10,11... | collective-permute-start | bytes 3145736 | tf_op jit(solution)/shard_map/ppermute | solution.py:15
  9.1 36.4 %collective-permute-start.4 = (bf16[256,2048]{1,0:T(8,128)(2,1)}, bf16[256,2048]{1,0:T(8,128)(2,1)}, u32[]{:S(2)}, u32[]{:S(2)}) collective-permute-start(bf16[256,2048]{1,0:T(8,128)(2,1)} %bitcast.10.down_a_hbm), channel_id=1, source_target_pairs={{0,1},{1,0},{2,3},{3,2},{4,5},{5,4},{6,7},{7,6},{8,9},{9,8},{10,11... | collective-permute-start | bytes 3145736 | tf_op jit(solution)/shard_map/ppermute | solution.py:15
  10.5 35.0 %copy-start.3 = (f32[2048]{0:T(1024)S(1)}, f32[2048]{0:T(1024)}, u32[]{:S(2)}) copy-start(f32[2048]{0:T(1024)} %param.29) | copy-start | bytes 24580

commit v4 on v3

--- a/solution.py
+++ b/solution.py
@@ -31,7 +31,6 @@
         in_specs=[pl.BlockSpec(memory_space=places[space]) for space in spaces],
         out_specs=tuple(pl.BlockSpec(memory_space=pltpu.VMEM) for _ in outs),
         scratch_shapes=getattr(body, "scratch", ()),
-        name=body.__name__,
         compiler_params=pltpu.CompilerParams(vmem_limit_bytes=body.room << 20),
     )
 
@@ -208,26 +207,21 @@
     residual_ref[...] = residual
     width = residual.shape[1] // 2
     stacked = jnp.concatenate([residual[:, :width], residual[:, width:]], axis=0)
-    out_ref[...] = lax.dot_general(
+    outgoing = lax.dot_general(
         place_ref[...], stacked, (((0,), (0,)), ((), ())), preferred_element_type=F32
-    ).astype(BF16)
+    )
+    out_ref[...] = outgoing.astype(BF16).reshape(out_ref.shape)
 
 
 def experts_of(
-    rows_ref, gain_ref, gate_a, up_a, down_a_hbm, gate_b_hbm, up_b_hbm, down_b_hbm, out_ref,
-    down_a, gate_b, up_b, down_b, scratch_ref, sems,
+    rows_ref, gain_ref, gate_a, up_a, down_a, gate_b, up_b, down_b, out_ref, scratch_ref
 ):
-    pairs = ((gate_b_hbm, gate_b), (up_b_hbm, up_b), (down_a_hbm, down_a), (down_b_hbm, down_b))
-    copies = [
-        pltpu.make_async_copy(source, target, sems.at[at]) for at, (source, target) in enumerate(pairs)
-    ]
-    for copy in copies:
-        copy.start()
-    total, width = rows_ref.shape
-    slots = total // 4
+    messages, _, width = rows_ref.shape
+    slots = messages // 2
     pieces = width // 128
+    flat = rows_ref[...].reshape(2 * messages, width)
     for piece in range(pieces):
-        scratch_ref[piece] = rows_ref[:, piece * 128 : (piece + 1) * 128].astype(F32)
+        scratch_ref[piece] = flat[:, piece * 128 : (piece + 1) * 128].astype(F32)
 
     def of_quarter(q):
         return pl.ds((q // 2) * 2 * slots + q % 2, slots, 2)
@@ -243,34 +237,25 @@
         for q, part in enumerate(quarters)
     ]
     rows = jnp.concatenate(quarters, axis=1)
-    hidden = [(jax.nn.silu(mm(rows, gate_a[...])) * mm(rows, up_a[...])).astype(BF16)]
-    copies[0].wait()
-    gate = jax.nn.silu(mm(rows, gate_b[...]))
-    copies[1].wait()
-    hidden.append((gate * mm(rows, up_b[...])).astype(BF16))
-    copies[2].wait()
-    copies[3].wait()
+    hidden = [
+        (jax.nn.silu(mm(rows, gate[...])) * mm(rows, up[...])).astype(BF16)
+        for gate, up in ((gate_a, up_a), (gate_b, up_b))
+    ]
     for q in range(4):
         span = slice(q * width, (q + 1) * width)
         answer = mm(hidden[0], down_a[:, span]) + mm(hidden[1], down_b[:, span])
         for piece in range(pieces):
             scratch_ref[piece, of_quarter(q), :] = answer[:, piece * 128 : (piece + 1) * 128]
-    for piece in range(pieces):
-        out_ref[:, piece * 128 : (piece + 1) * 128] = scratch_ref[piece].astype(BF16)
-
-
-experts_of.scratch = (
-    pltpu.VMEM((256, 2048), BF16),
-    pltpu.VMEM((2048, 256), BF16),
-    pltpu.VMEM((2048, 256), BF16),
-    pltpu.VMEM((256, 2048), BF16),
-    pltpu.VMEM((4, 512, 128), F32),
-    pltpu.SemaphoreType.DMA((4,)),
-)
+    answers = jnp.concatenate([scratch_ref[piece].astype(BF16) for piece in range(pieces)], axis=1)
+    out_ref[...] = answers.reshape(out_ref.shape)
+
+
+experts_of.scratch = (pltpu.VMEM((4, 512, 128), F32),)
 
 
 def combine(returned_ref, pick_ref, residual_ref, out_ref):
-    found = mm(pick_ref[...], returned_ref[...])
+    messages, _, width = returned_ref.shape
+    found = mm(pick_ref[...], returned_ref[...].reshape(2 * messages, width))
     sequences, width = residual_ref.shape
     width = width // 2
     for half in range(2):
@@ -283,11 +268,8 @@
 begin.room, mixer.room, project.room, experts_of.room, combine.room = 8, 6, 6, 12, 6
 
 
-def exchange(rows):
-    total, width = rows.shape
-    messages = rows.reshape(total // 2, 2, width)
-    arrived = lax.all_to_all(messages, ("tp", "ep"), split_axis=0, concat_axis=0, tiled=True)
-    return arrived.reshape(total, width)
+def exchange(messages):
+    return lax.all_to_all(messages, ("tp", "ep"), split_axis=0, concat_axis=0, tiled=True)
 
 
 def local(
@@ -350,11 +332,16 @@
     )
     other_mixed = swap(mixed)
     residual, outgoing = call(
-        project, (((sequences, half), BF16), ((messages, width), BF16)), "s" + "v" * 5
+        project, (((sequences, half), BF16), ((messages // 2, 2, width), BF16)), "s" + "v" * 5
     )(core, own_tokens, mixed, other_mixed, output_weight, place)
-    other_gate, other_up, other_down = swap(expert_gate[0]), swap(expert_up[0]), swap(expert_down[0])
+    other_gate = swap(expert_gate[0])
+    other_up = swap(expert_up[0])
+    other_down = swap(expert_down[0])
+    outgoing, other_gate, other_up, other_down = lax.optimization_barrier(
+        (outgoing, other_gate, other_up, other_down)
+    )
     received = exchange(outgoing)
-    (answers,) = call(experts_of, (((messages, width), BF16),), "vvvvhhhh")(
+    (answers,) = call(experts_of, (((messages // 2, 2, width), BF16),), "VvVVVVVV")(
         received, expert_gain[None, :], expert_gate[0], expert_up[0], expert_down[0], other_gate,
         other_up, other_down,
     )

time: 76.4 us -> 75.8 us (level)
  waiting for transfers between devices: 0.21 us -> 2.82 us
  local copies, waits for them, and re-layouts: 1.86 us -> 0.02 us
  Pallas kernels: 9.41 us -> 8.01 us
    ppermute x5, waiting for transfers between devices: 0.21 us -> 2.82 us  [swap(): return lax.ppermute(array, 'tp', [(0, 1), (1, 0)])]
    reshape x4 -> x0, local copies, waits for them, and re-layouts: 1.83 us -> none  [the longest x2 1.44 us: exchange(): return arrived.reshape(total, width)]
    pallas_call x5, Pallas kernels: 9.41 us -> 8.01 us  [placed(): run(*(pltpu.with_memory_space_constraint(operand, places[space]) if space...]
  transfers between devices with their start and end apart: 5 -> 5, of which waited for: 1 -> 2; matrix products, arithmetic and copies ran while one was open for 2% -> 0% of each run, Pallas kernels for 5% -> 7%
where the time goes in v4:
time: 75.8 us; the launch traced here: 75.7 us
  blocking collectives  59.7 us (79%)
  Pallas kernels  8.01 us (11%)
  starting transfers between devices  4.36 us (6%)
  waiting for transfers between devices  2.82 us (4%)
    all_to_all x2, blocking collectives, exchange(): lax.all_to_all(messages, ('tp', 'ep'), split_axis=0, concat_axis=0, tiled...  59.7 us
    pallas_call x5, Pallas kernels, placed(): run(*(pltpu.with_memory_space_constraint(operand, places[space]) if space...  8.01 us
    ppermute x5, starting transfers between devices, swap(): return lax.ppermute(array, 'tp', [(0, 1), (1, 0)])  4.36 us
    ppermute x5, waiting for transfers between devices, swap(): return lax.ppermute(array, 'tp', [(0, 1), (1, 0)])  2.82 us
  transfers between devices with their start and end apart: 5, of which 2 were waited for; matrix products, arithmetic and copies ran while one was open for 0% of the time, Pallas kernels for 7%

profile of v4, /device:TPU:1, one launch (start us, length us, event | category | flops | bytes accessed | tf_op | source)
XLA Modules:
  0.0 75.7 jit_solution(11587675881927922179)
XLA Ops:
  0.6 3.3 %collective-permute-start.2 = (bf16[2048,256]{1,0:T(8,128)(2,1)}, bf16[2048,256]{1,0:T(8,128)(2,1)S(1)}, u32[]{:S(2)}, u32[]{:S(2)}) collective-permute-start(bf16[2048,256]{1,0:T(8,128)(2,1)} %bitcast.11), channel_id=1, source_target_pairs={{0,1},{1,0},{2,3},{3,2},{4,5},{5,4},{6,7},{7,6},{8,9},{9,8},{10,11... | collective-permute-start | bytes 3145736 | tf_op jit(solution)/shard_map/ppermute | solution.py:15
  3.9 0.1 collective-permute-start.3
  4.0 0.4 collective-permute-start.4
  4.4 0.1 collective-permute-start
  4.5 3.1 %shard_map.185 = (bf16[48,1024]{1,0:T(8,128)(2,1)S(1)}, f32[1,1024]{1,0:T(1,128)S(1)}, bf16[1024,512]{1,0:T(8,128)(2,1)S(1)}, bf16[1024,512]{1,0:T(8,128)(2,1)S(...) custom-call(s32[1]{0:T(128)} %bitcast.core_ref, ...), custom_call_target="tpu_custom_call" | custom-call | tf_op jit(solution)/shard_map/pallas_call | solution.py:38
  7.6 0.0 copy-start
  7.6 1.9 %collective-permute-done.other_ref = bf16[48,1024]{1,0:T(8,128)(2,1)S(1)} collective-permute-done((bf16[48,1024]{1,0:T(8,128)(2,1)}, bf16[48,1024]{1,0:T(8,128)(2,1)S(1)}, u32[]{:S(2)}, u32[]{:S(2)}) %collective-permute-start) | collective-permute-done | bytes 98336 | tf_op jit(solution)/shard_map/ppermute | solution.py:15
  9.6 1.4 %shard_map.186 = (f32[48,512]{1,0:T(8,128)}, bf16[48,512]{1,0:T(8,128)(2,1)S(1)}) custom-call(bf16[48,1024]{1,0:T(8,128)(2,1)S(1)} %collective-permute-done.other_ref, f32[48,1]{1,0:T(8,128)S(1)} %get-tuple-element.26.squares_ref, f32[1,1024]{1,0:T(1,128)S(1)} %get-tuple-element.27.gain_ref, bf16[1024,512]{1,0:T(8,128)(2,1)S(1)} %get-tuple-element.28.branch_ref, ...), custom_call_target="tpu_custom_call" | custom-call | tf_op jit(solution)/shard_map/pallas_call | solution.py:38
  10.9 0.0 copy-start.1
  10.9 0.0 copy-start.2
  10.9 0.0 copy-start.3
  10.9 0.0 copy-start.4
  11.0 0.5 collective-permute-start.1
  11.4 0.9 %collective-permute-done.1.other_ref = bf16[48,512]{1,0:T(8,128)(2,1)S(1)} collective-permute-done((bf16[48,512]{1,0:T(8,128)(2,1)S(1)}, bf16[48,512]{1,0:T(8,128)(2,1)S(1)}, u32[]{:S(2)}, u32[]{:S(2)}) %collective-permute-start.1) | collective-permute-done | bytes 49184 | tf_op jit(solution)/shard_map/ppermute | solution.py:15
  12.3 0.0 copy-done
  12.3 0.7 shard_map.187
  13.1 0.0 collective-permute-done.2.gate_b
  13.1 0.0 collective-permute-done.3.up_b
  13.1 0.0 collective-permute-done.4.down_b
  13.1 33.6 %all_to_all.10.rows_ref = bf16[256,2,512]{2,1,0:T(2,128)(2,1)S(1)} all-to-all(bf16[256,2,512]{2,1,0:T(2,128)(2,1)S(1)} %get-tuple-element.41), channel_id=1, replica_groups=mesh['ep'=128,'tp'=2] {'tp','ep'}, dimensions={0} | all-to-all | bytes 1048576 | tf_op jit(solution)/shard_map/all_to_all | solution.py:272
  46.7 0.0 copy-done.1
  46.7 0.0 copy-done.2
  46.7 0.0 copy-done.3
  46.7 0.0 copy-done.4
  46.7 1.9 %shard_map.188 = bf16[256,2,512]{2,1,0:T(2,128)(2,1)S(1)} custom-call(bf16[256,2,512]{2,1,0:T(2,128)(2,1)S(1)} %all_to_all.10.rows_ref, f32[1,2048]{1,0:T(1,128)S(1)} %bitcast.17, bf16[2048,256]{1,0:T(8,128)(2,1)S(1)} %bitcast.12, bf16[2048,256]{1,0:T(8,128)(2,1)S(1)} %bitcast.14, bf16[256,2048]{1,0:T(8,128)(2,1)S(1)} %bitcast.16, ...), custom_call_target="tpu_custom_call" | custom-call | tf_op jit(solution)/shard_map/pallas_call | solution.py:38
  48.6 26.1 %all_to_all.11.returned_ref = bf16[256,2,512]{2,1,0:T(2,128)(2,1)S(1)} all-to-all(bf16[256,2,512]{2,1,0:T(2,128)(2,1)S(1)} %shard_map.188), channel_id=1, replica_groups=mesh['ep'=128,'tp'=2] {'tp','ep'}, dimensions={0} | all-to-all | bytes 1048576 | tf_op jit(solution)/shard_map/all_to_all | solution.py:272
  74.7 0.9 %shard_map.189 = bf16[48,1024]{1,0:T(8,128)(2,1)} custom-call(bf16[256,2,512]{2,1,0:T(2,128)(2,1)S(1)} %all_to_all.11.returned_ref, bf16[192,512]{1,0:T(8,128)(2,1)S(1)} %get-tuple-element.45.pick_ref, bf16[48,1024]{1,0:T(8,128)(2,1)S(1)} %get-tuple-element.46.residual_ref), custom_call_target="tpu_custom_call" | custom-call | tf_op jit(solution)/shard_map/pallas_call | solution.py:38
Async XLA Ops:
  0.6 12.4 %collective-permute-start.2 = (bf16[2048,256]{1,0:T(8,128)(2,1)}, bf16[2048,256]{1,0:T(8,128)(2,1)S(1)}, u32[]{:S(2)}, u32[]{:S(2)}) collective-permute-start(bf16[2048,256]{1,0:T(8,128)(2,1)} %bitcast.11), channel_id=1, source_target_pairs={{0,1},{1,0},{2,3},{3,2},{4,5},{5,4},{6,7},{7,6},{8,9},{9,8},{10,11... | collective-permute-start | bytes 3145736 | tf_op jit(solution)/shard_map/ppermute | solution.py:15
  3.9 9.1 %collective-permute-start.3 = (bf16[2048,256]{1,0:T(8,128)(2,1)}, bf16[2048,256]{1,0:T(8,128)(2,1)S(1)}, u32[]{:S(2)}, u32[]{:S(2)}) collective-permute-start(bf16[2048,256]{1,0:T(8,128)(2,1)} %bitcast.13), channel_id=1, source_target_pairs={{0,1},{1,0},{2,3},{3,2},{4,5},{5,4},{6,7},{7,6},{8,9},{9,8},{10,11... | collective-permute-start | bytes 3145736 | tf_op jit(solution)/shard_map/ppermute | solution.py:15
  4.0 9.1 %collective-permute-start.4 = (bf16[256,2048]{1,0:T(8,128)(2,1)}, bf16[256,2048]{1,0:T(8,128)(2,1)S(1)}, u32[]{:S(2)}, u32[]{:S(2)}) collective-permute-start(bf16[256,2048]{1,0:T(8,128)(2,1)} %bitcast.15), channel_id=1, source_target_pairs={{0,1},{1,0},{2,3},{3,2},{4,5},{5,4},{6,7},{7,6},{8,9},{9,8},{10,11... | collective-permute-start | bytes 3145736 | tf_op jit(solution)/shard_map/ppermute | solution.py:15
  4.4 5.1 %collective-permute-start = (bf16[48,1024]{1,0:T(8,128)(2,1)}, bf16[48,1024]{1,0:T(8,128)(2,1)S(1)}, u32[]{:S(2)}, u32[]{:S(2)}) collective-permute-start(bf16[48,1024]{1,0:T(8,128)(2,1)} %tokens_hbm.1), channel_id=1, source_target_pairs={{0,1},{1,0},{2,3},{3,2},{4,5},{5,4},{6,7},{7,6},{8,9},{9,8},{10,11... | collective-permute-start | bytes 294920 | tf_op jit(solution)/shard_map/ppermute | solution.py:15
  7.6 4.7 %copy-start = (bf16[1024,1024]{1,0:T(8,128)(2,1)S(1)}, bf16[1024,1024]{1,0:T(8,128)(2,1)}, u32[]{:S(2)}) copy-start(bf16[1024,1024]{1,0:T(8,128)(2,1)} %weight_ref.1) | copy-start | bytes 6291460
  10.9 35.8 %copy-start.1 = (bf16[1,2048,256]{2,1,0:T(8,128)(2,1)S(1)}, bf16[1,2048,256]{2,1,0:T(8,128)(2,1)}, u32[]{:S(2)}) copy-start(bf16[1,2048,256]{2,1,0:T(8,128)(2,1)} %param.33) | copy-start | bytes 3145732
  10.9 35.8 %copy-start.2 = (bf16[1,2048,256]{2,1,0:T(8,128)(2,1)S(1)}, bf16[1,2048,256]{2,1,0:T(8,128)(2,1)}, u32[]{:S(2)}) copy-start(bf16[1,2048,256]{2,1,0:T(8,128)(2,1)} %param.34) | copy-start | bytes 3145732
  10.9 35.8 %copy-start.3 = (bf16[1,256,2048]{2,1,0:T(8,128)(2,1)S(1)}, bf16[1,256,2048]{2,1,0:T(8,128)(2,1)}, u32[]{:S(2)}) copy-start(bf16[1,256,2048]{2,1,0:T(8,128)(2,1)} %param.35) | copy-start | bytes 3145732
  10.9 35.8 %copy-start.4 = (f32[2048]{0:T(1024)S(1)}, f32[2048]{0:T(1024)}, u32[]{:S(2)}) copy-start(f32[2048]{0:T(1024)} %param.29) | copy-start | bytes 24580
  11.0 1.3 %collective-permute-start.1 = (bf16[48,512]{1,0:T(8,128)(2,1)S(1)}, bf16[48,512]{1,0:T(8,128)(2,1)S(1)}, u32[]{:S(2)}, u32[]{:S(2)}) collective-permute-start(bf16[48,512]{1,0:T(8,128)(2,1)S(1)} %get-tuple-element.38.own_ref), channel_id=1, source_target_pairs={{0,1},{1,0},{2,3},{3,2},{4,5},{5,4},{6,7},{7,6},{8,9},{9,8},{10,11... | collective-permute-start | bytes 147464 | tf_op jit(solution)/shard_map/ppermute | solution.py:15

commit v5 on v4

--- a/solution.py
+++ b/solution.py
@@ -32,6 +32,7 @@
         out_specs=tuple(pl.BlockSpec(memory_space=pltpu.VMEM) for _ in outs),
         scratch_shapes=getattr(body, "scratch", ()),
         compiler_params=pltpu.CompilerParams(vmem_limit_bytes=body.room << 20),
+        cost_estimate=pl.CostEstimate(flops=body.flops, bytes_accessed=0, transcendentals=0),
     )
 
     def placed(*operands):
@@ -47,20 +48,20 @@
     return placed
 
 
-def half_of(ref, core, other, dim):
-    size = ref.shape[dim] // 2
-    start = (1 - core if other else core) * size
-    span = pl.ds(pl.multiple_of(start, size), size)
-    return ref.at[span, :] if dim == 0 else ref.at[:, span]
-
-
 def block_diagonal(blocks):
     count, size, _ = blocks.shape
-    width = count * size
+    width = 2 * size
     tiled = (iota((size, width), 1) % size == iota((size, width), 0)).astype(BF16)
-    spread = mm(blocks.reshape(width, size), tiled)
-    keep = iota((width, width), 0) // size == iota((width, width), 1) // size
+    spread = mm(blocks.reshape(count * size, size), tiled)
+    shape = (count * size, width)
+    keep = (iota(shape, 0) // size) % 2 == iota(shape, 1) // size
     return jnp.where(keep, spread, 0.0).astype(BF16)
+
+
+def times_diagonal(rows, pairs_ref):
+    width = pairs_ref.shape[1]
+    spans = [slice(at, at + width) for at in range(0, rows.shape[1], width)]
+    return jnp.concatenate([mm(rows[:, span], pairs_ref[span, :]) for span in spans], axis=1)
 
 
 def as_column(row):
@@ -99,66 +100,37 @@
 
 
 def begin(
-    core_ref, tokens_hbm, gain_hbm, branch_hbm, gelu_hbm, recur_hbm, input_hbm, ids_hbm, prob_hbm,
-    logit_hbm, state_hbm, taps_hbm, hidden_hbm, rate_hbm,
-    tokens_ref, gain_ref, branch_ref, gelu_ref, state_ref, taps_ref, hidden_ref, rate_ref,
-    rd_ref, id_ref, place_ref, pick_ref, branch_part, gelu_part, squares_ref,
-    own_gain, own_branch, own_gelu, recur_ref, input_ref, ids_ref, prob_ref, logit_ref, sems,
+    recur_hbm, input_hbm, ids_hbm, prob_hbm, logit_hbm, rd_ref, id_ref, place_ref, pick_ref,
+    recur_ref, input_ref, ids_ref, prob_ref, logit_ref, sems,
 ):
-    core = core_ref[0]
     pairs = (
-        (tokens_hbm, tokens_ref),
-        (half_of(gain_hbm, core, False, 1), own_gain),
-        (half_of(branch_hbm, core, False, 0), own_branch),
-        (half_of(gelu_hbm, core, False, 0), own_gelu),
         (ids_hbm, ids_ref),
         (prob_hbm, prob_ref),
         (logit_hbm, logit_ref),
         (recur_hbm, recur_ref),
         (input_hbm, input_ref),
-        (half_of(branch_hbm, core, True, 0), branch_ref),
-        (half_of(gelu_hbm, core, True, 0), gelu_ref),
-        (half_of(gain_hbm, core, True, 1), gain_ref),
-        (state_hbm, state_ref),
-        (taps_hbm, taps_ref),
-        (hidden_hbm, hidden_ref),
-        (rate_hbm, rate_ref),
     )
     copies = [
         pltpu.make_async_copy(source, target, sems.at[at]) for at, (source, target) in enumerate(pairs)
     ]
     for copy in copies:
         copy.start()
-    for copy in copies[4:7]:
+    for copy in copies[:3]:
         copy.wait()
     route(ids_ref, prob_ref, logit_ref, place_ref, pick_ref)
-    for copy in copies[7:9]:
+    for copy in copies[3:]:
         copy.wait()
     rd_ref[...] = block_diagonal(recur_ref[...])
     id_ref[...] = block_diagonal(input_ref[...])
-    for copy in copies[:2]:
-        copy.wait()
-    own = tokens_ref[...].astype(F32)
-    squares_ref[...] = jnp.sum(own * own, axis=1, keepdims=True)
-    own = (own * own_gain[...]).astype(BF16)
-    copies[2].wait()
-    branch_part[...] = mm(own, own_branch[...])
-    copies[3].wait()
-    gelu_part[...] = mm(own, own_gelu[...])
-    for copy in copies[9:]:
-        copy.wait()
 
 
 begin.scratch = (
-    pltpu.VMEM((1, 1024), F32),
-    pltpu.VMEM((1024, 512), BF16),
-    pltpu.VMEM((1024, 512), BF16),
     pltpu.VMEM((8, 64, 64), BF16),
     pltpu.VMEM((8, 64, 64), BF16),
     pltpu.VMEM((2, 48), jnp.int32),
     pltpu.VMEM((1, 48), F32),
     pltpu.VMEM((2, 48), F32),
-    pltpu.SemaphoreType.DMA((16,)),
+    pltpu.SemaphoreType.DMA((5,)),
 )
 
 
@@ -172,23 +144,34 @@
 
 
 def mixer(
-    other_ref, squares_ref, gain_ref, branch_ref, gelu_ref, branch_part, gelu_part, state_ref,
-    taps_ref, hidden_ref, rate_ref, rd_ref, id_ref, new_ref, mixed_ref,
+    core_ref, own_ref, other_ref, gain_ref, branch_ref, gelu_ref, state_ref, taps_ref, hidden_ref,
+    rate_ref, rd_ref, id_ref, new_ref, mixed_ref,
 ):
+    core = core_ref[0]
+    own = own_ref[...].astype(F32)
     other = other_ref[...].astype(F32)
-    half = other.shape[1]
-    squares = squares_ref[...] + jnp.sum(other * other, axis=1, keepdims=True)
+    half = own.shape[1]
+    squares = jnp.sum(own * own + other * other, axis=1, keepdims=True)
     scaling = lax.rsqrt(squares / (2 * half) + EPSILON)
-    other = (other * gain_ref[...]).astype(BF16)
-    branch = ((branch_part[...] + mm(other, branch_ref[...])) * scaling).astype(BF16)
-    gelu_input = ((gelu_part[...] + mm(other, gelu_ref[...])) * scaling).astype(BF16)
+    left, right = gain_ref[:, :half], gain_ref[:, half:]
+    own = (own * jnp.where(core == 0, left, right)).astype(BF16)
+    other = (other * jnp.where(core == 0, right, left)).astype(BF16)
+    own_rows = pl.ds(pl.multiple_of(core * half, half), half)
+    other_rows = pl.ds(pl.multiple_of((1 - core) * half, half), half)
+
+    def product(weight_ref):
+        total = mm(own, weight_ref[own_rows, :]) + mm(other, weight_ref[other_rows, :])
+        return (total * scaling).astype(BF16)
+
+    branch = product(branch_ref)
+    gelu_input = product(gelu_ref)
     taps = taps_ref.shape[0]
     convolved = branch.astype(F32) * taps_ref[taps - 1 : taps, :]
     for tap in range(taps - 1):
         convolved = convolved + state_ref[tap].astype(F32) * taps_ref[tap : tap + 1, :]
     convolved = convolved.astype(BF16)
-    recur_gate = jax.nn.sigmoid(mm(convolved, rd_ref[...]))
-    input_gate = jax.nn.sigmoid(mm(convolved, id_ref[...]))
+    recur_gate = jax.nn.sigmoid(times_diagonal(convolved, rd_ref))
+    input_gate = jax.nn.sigmoid(times_diagonal(convolved, id_ref))
     log_decay = -RATE_SCALE * recur_gate * rate_ref[...]
     new_hidden = jnp.exp(log_decay) * hidden_ref[...] + jnp.sqrt(-expm1(2.0 * log_decay)) * (
         input_gate * convolved.astype(F32)
@@ -265,6 +248,11 @@
         out_ref[:, span] = (residual_ref[:, span].astype(F32) + (high + low)).astype(BF16)
 
 
+begin.flops = 20_000_000_000
+mixer.flops = 210_000_000
+project.flops = 150_000_000
+experts_of.flops = 810_000_000
+combine.flops = 100_000_000
 begin.room, mixer.room, project.room, experts_of.room, combine.room = 8, 6, 6, 12, 6
 
 
@@ -299,41 +287,27 @@
     width = half // 2
 
     other_tokens = swap(tokens)
-    kinds = (
-        ((sequences, half), BF16),
-        ((1, half), F32),
-        ((half, channels), BF16),
-        ((half, channels), BF16),
-        ((3, sequences, channels), BF16),
-        ((4, channels), F32),
-        ((sequences, channels), F32),
-        ((1, channels), F32),
-        ((channels, channels), BF16),
-        ((channels, channels), BF16),
-        ((2 * sequences, messages), BF16),
-        ((4 * sequences, messages), BF16),
-        ((sequences, channels), F32),
-        ((sequences, channels), F32),
-        ((sequences, 1), F32),
-    )
-    (
-        own_tokens, gain, branch_rows, gelu_rows, state, taps, hidden, rate, recur_full, input_full,
-        place, pick, branch_part, gelu_part, squares,
-    ) = call(begin, kinds, "s" + "h" * 13)(
-        core, tokens, mixer_gain[None, :], branch_weight, gelu_weight, recur_blocks, input_blocks,
-        expert_ids.T, group_prob[None, :], expert_logit.T, jnp.transpose(conv_state, (1, 0, 2)),
-        conv_kernel, hidden_state, decay_rate[None, :],
-    )
+    recur_pairs, input_pairs, place, pick = call(
+        begin,
+        (
+            ((channels, 128), BF16),
+            ((channels, 128), BF16),
+            ((2 * sequences, messages), BF16),
+            ((4 * sequences, messages), BF16),
+        ),
+        "h" * 5,
+    )(recur_blocks, input_blocks, expert_ids.T, group_prob[None, :], expert_logit.T)
     new_hidden, mixed = call(
-        mixer, (((sequences, channels), F32), ((sequences, channels), BF16)), "v" * 13
+        mixer, (((sequences, channels), F32), ((sequences, channels), BF16)), "s" + "V" * 11
     )(
-        other_tokens, squares, gain, branch_rows, gelu_rows, branch_part, gelu_part, state, taps,
-        hidden, rate, recur_full, input_full,
+        core, tokens, other_tokens, mixer_gain[None, :], branch_weight, gelu_weight,
+        jnp.transpose(conv_state, (1, 0, 2)), conv_kernel, hidden_state, decay_rate[None, :],
+        recur_pairs, input_pairs,
     )
     other_mixed = swap(mixed)
     residual, outgoing = call(
         project, (((sequences, half), BF16), ((messages // 2, 2, width), BF16)), "s" + "v" * 5
-    )(core, own_tokens, mixed, other_mixed, output_weight, place)
+    )(core, tokens, mixed, other_mixed, output_weight, place)
     other_gate = swap(expert_gate[0])
     other_up = swap(expert_up[0])
     other_down = swap(expert_down[0])
@@ -351,6 +325,7 @@
 
 
 def solution(mesh):
+
     return jax.shard_map(
         local,
         mesh=mesh,

time: 75.8 us -> 82.4 us (1.087)
  local copies, waits for them, and re-layouts: 0.02 us -> 6.97 us
  waiting for transfers between devices: 2.82 us -> 0.89 us
  Pallas kernels: 8.01 us -> 9.27 us
    unnamed x10 -> x38, local copies, waits for them, and re-layouts: 0.02 us -> 6.97 us
    ppermute x5, waiting for transfers between devices: 2.82 us -> 0.89 us  [swap(): return lax.ppermute(array, 'tp', [(0, 1), (1, 0)])]
    pallas_call x5, Pallas kernels: 8.01 us -> 9.27 us  [placed(): run(*(pltpu.with_memory_space_constraint(operand, places[space]) if space...]
  transfers between devices with their start and end apart: 5 -> 5, of which waited for: 2 -> 1; matrix products, arithmetic and copies ran while one was open for 0% -> 0% of each run, Pallas kernels for 7% -> 6%
where the time goes in v5:
time: 82.4 us; the launch traced here: 82 us
  blocking collectives  59.8 us (73%)
  Pallas kernels  9.27 us (11%)
  local copies, waits for them, and re-layouts  6.97 us (8%)
  starting transfers between devices  4.39 us (5%)
  waiting for transfers between devices  0.89 us (1%)
    all_to_all x2, blocking collectives, exchange(): lax.all_to_all(messages, ('tp', 'ep'), split_axis=0, concat_axis=0, tiled...  59.8 us
    pallas_call x5, Pallas kernels, placed(): run(*(pltpu.with_memory_space_constraint(operand, places[space]) if space...  9.27 us
    unnamed x38, local copies, waits for them, and re-layouts  6.97 us
    ppermute x5, starting transfers between devices, swap(): return lax.ppermute(array, 'tp', [(0, 1), (1, 0)])  4.39 us
  transfers between devices with their start and end apart: 5, of which 1 were waited for; matrix products, arithmetic and copies ran while one was open for 0% of the time, Pallas kernels for 6%

profile of v5, /device:TPU:1, one launch (start us, length us, event | category | flops | bytes accessed | tf_op | source)
XLA Modules:
  0.0 82.0 jit_solution(8039926838876319192)
XLA Ops:
  0.6 3.3 %collective-permute-start = (bf16[48,1024]{1,0:T(8,128)(2,1)}, bf16[48,1024]{1,0:T(8,128)(2,1)}, u32[]{:S(2)}, u32[]{:S(2)}) collective-permute-start(bf16[48,1024]{1,0:T(8,128)(2,1)} %tokens_ref.1), channel_id=1, source_target_pairs={{0,1},{1,0},{2,3},{3,2},{4,5},{5,4},{6,7},{7,6},{8,9},{9,8},{10,11... | collective-permute-start | bytes 294920 | tf_op jit(solution)/shard_map/ppermute | solution.py:15
  3.9 0.1 collective-permute-start.2
  4.0 0.4 collective-permute-start.3
  4.4 0.1 collective-permute-start.4
  4.5 0.0 copy-start
  4.5 0.0 copy-start.6
  4.5 0.0 copy-start.12
  4.5 0.0 copy-start.15
  4.5 0.0 copy-start.16
  4.6 1.5 %shard_map.185 = (bf16[512,128]{1,0:T(8,128)(2,1)S(1)}, bf16[512,128]{1,0:T(8,128)(2,1)S(1)}, bf16[96,512]{1,0:T(8,128)(2,1)S(1)}, bf16[192,512]{1,0:T(8,128)(2,1)S(1)}) custom-call(bf16[8,64,64]{2,1,0:T(8,128)(2,1)} %recur_hbm.1, bf16[8,64,64]{2,1,0:T(8,128)(2,1)} %input_hbm.1, s32[2,48]{1,0:T(2,128)} %bitcast.21, f32[1,48]{1,0:T(1,128)} %bitcast.23, ...), custom_call_target="tpu_custom_call" | custom-call | flops 20000000000 | tf_op jit(solution)/shard_map/pallas_call | solution.py:39
  6.1 0.0 copy-start.8
  6.1 0.6 copy-done.8
  6.7 0.0 copy-start.10
  6.7 0.7 copy-done.10
  7.4 0.0 copy-start.13
  7.4 0.6 copy-done.13
  8.0 0.0 collective-permute-done.other_ref
  8.0 0.0 copy-done
  8.0 0.0 copy-done.6
  8.0 0.0 copy-done.12
  8.0 0.0 copy-done.15
  8.1 0.0 copy-done.16
  8.1 0.0 copy-start.1
  8.1 1.6 %copy-done.1 = bf16[2048,512]{1,0:T(8,128)(2,1)S(1)} copy-done((bf16[2048,512]{1,0:T(8,128)(2,1)S(1)}, bf16[2048,512]{1,0:T(8,128)(2,1)}, u32[]{:S(2)}) %copy-start.1) | copy-done | bytes 2097176
  9.7 0.0 copy-start.7
  9.7 0.9 %copy-done.7 = bf16[48,3,512]{2,0,1:T(8,128)(2,1)S(1)} copy-done((bf16[48,3,512]{2,0,1:T(8,128)(2,1)S(1)}, bf16[48,3,512]{2,0,1:T(8,128)(2,1)}, u32[]{:S(2)}) %copy-start.7) | copy-done | bytes 147480
  10.6 0.0 copy-start.9
  10.6 0.9 %copy-done.9 = bf16[512,128]{1,0:T(8,128)(2,1)S(1)} copy-done((bf16[512,128]{1,0:T(8,128)(2,1)S(1)}, bf16[512,128]{1,0:T(8,128)(2,1)}, u32[]{:S(2)}) %copy-start.9) | copy-done | bytes 131096
  11.5 0.0 copy-start.11
  11.5 0.9 %copy-done.11 = bf16[512,128]{1,0:T(8,128)(2,1)S(1)} copy-done((bf16[512,128]{1,0:T(8,128)(2,1)S(1)}, bf16[512,128]{1,0:T(8,128)(2,1)}, u32[]{:S(2)}) %copy-start.11) | copy-done | bytes 131096
  12.4 0.7 copy-done.18
  13.1 2.7 %shard_map.186 = (f32[48,512]{1,0:T(8,128)}, bf16[48,512]{1,0:T(8,128)(2,1)S(1)}) custom-call(s32[1]{0:T(128)} %bitcast.core_ref, bf16[48,1024]{1,0:T(8,128)(2,1)S(1)} %copy-done.6, bf16[48,1024]{1,0:T(8,128)(2,1)} %collective-permute-done.other_ref, f32[1,2048]{1,0:T(1,128)S(1)} %bitcast.18, bf16[2048,512]{1,0:T(8,128)(2,1)S(1)} %copy-done, ...), custom_call_target="tpu_custom_call" | custom-call | flops 210000000 | tf_op jit(solution)/shard_map/pallas_call | solution.py:39
  15.8 0.5 collective-permute-start.1
  16.3 0.9 %collective-permute-done.1.other_ref = bf16[48,512]{1,0:T(8,128)(2,1)S(1)} collective-permute-done((bf16[48,512]{1,0:T(8,128)(2,1)S(1)}, bf16[48,512]{1,0:T(8,128)(2,1)S(1)}, u32[]{:S(2)}, u32[]{:S(2)}) %collective-permute-start.1) | collective-permute-done | bytes 49184 | tf_op jit(solution)/shard_map/ppermute | solution.py:15
  17.2 0.0 copy-done.2
  17.2 0.0 copy-done.14
  17.2 0.7 shard_map.187
  17.9 0.0 collective-permute-done.2.gate_b
  17.9 0.0 collective-permute-done.3.up_b
  17.9 0.0 collective-permute-done.4.down_b
  18.0 33.6 %all_to_all.10.rows_ref = bf16[256,2,512]{2,1,0:T(2,128)(2,1)S(1)} all-to-all(bf16[256,2,512]{2,1,0:T(2,128)(2,1)S(1)} %get-tuple-element.19), channel_id=1, replica_groups=mesh['ep'=128,'tp'=2] {'tp','ep'}, dimensions={0} | all-to-all | bytes 1048576 | tf_op jit(solution)/shard_map/all_to_all | solution.py:260
  51.6 0.0 copy-done.3
  51.6 0.0 copy-done.4
  51.6 0.0 copy-done.5
  51.6 0.0 copy-done.17
  51.6 3.4 %shard_map.188 = bf16[256,2,512]{2,1,0:T(2,128)(2,1)S(1)} custom-call(bf16[256,2,512]{2,1,0:T(2,128)(2,1)S(1)} %all_to_all.10.rows_ref, f32[1,2048]{1,0:T(1,128)S(1)} %bitcast.19, bf16[2048,256]{1,0:T(8,128)(2,1)S(1)} %bitcast.12, bf16[2048,256]{1,0:T(8,128)(2,1)S(1)} %bitcast.14, bf16[256,2048]{1,0:T(8,128)(2,1)S(1)} %bitcast.16, ...), custom_call_target="tpu_custom_call" | custom-call | flops 810000000 | tf_op jit(solution)/shard_map/pallas_call | solution.py:39
  55.0 26.2 %all_to_all.11.returned_ref = bf16[256,2,512]{2,1,0:T(2,128)(2,1)S(1)} all-to-all(bf16[256,2,512]{2,1,0:T(2,128)(2,1)S(1)} %shard_map.188), channel_id=1, replica_groups=mesh['ep'=128,'tp'=2] {'tp','ep'}, dimensions={0} | all-to-all | bytes 1048576 | tf_op jit(solution)/shard_map/all_to_all | solution.py:260
  81.1 0.9 %shard_map.189 = bf16[48,1024]{1,0:T(8,128)(2,1)} custom-call(bf16[256,2,512]{2,1,0:T(2,128)(2,1)S(1)} %all_to_all.11.returned_ref, bf16[192,512]{1,0:T(8,128)(2,1)S(1)} %get-tuple-element.23.pick_ref, bf16[48,1024]{1,0:T(8,128)(2,1)S(1)} %get-tuple-element.24.residual_ref), custom_call_target="tpu_custom_call" | custom-call | flops 100000000 | tf_op jit(solution)/shard_map/pallas_call | solution.py:39
  (7 shorter events, 0.0 us)
Async XLA Ops:
  0.6 7.4 %collective-permute-start = (bf16[48,1024]{1,0:T(8,128)(2,1)}, bf16[48,1024]{1,0:T(8,128)(2,1)}, u32[]{:S(2)}, u32[]{:S(2)}) collective-permute-start(bf16[48,1024]{1,0:T(8,128)(2,1)} %tokens_ref.1), channel_id=1, source_target_pairs={{0,1},{1,0},{2,3},{3,2},{4,5},{5,4},{6,7},{7,6},{8,9},{9,8},{10,11... | collective-permute-start | bytes 294920 | tf_op jit(solution)/shard_map/ppermute | solution.py:15
  3.9 14.0 %collective-permute-start.2 = (bf16[2048,256]{1,0:T(8,128)(2,1)}, bf16[2048,256]{1,0:T(8,128)(2,1)S(1)}, u32[]{:S(2)}, u32[]{:S(2)}) collective-permute-start(bf16[2048,256]{1,0:T(8,128)(2,1)} %bitcast.11), channel_id=1, source_target_pairs={{0,1},{1,0},{2,3},{3,2},{4,5},{5,4},{6,7},{7,6},{8,9},{9,8},{10,11... | collective-permute-start | bytes 3145736 | tf_op jit(solution)/shard_map/ppermute | solution.py:15
  4.0 13.9 %collective-permute-start.3 = (bf16[2048,256]{1,0:T(8,128)(2,1)}, bf16[2048,256]{1,0:T(8,128)(2,1)}, u32[]{:S(2)}, u32[]{:S(2)}) collective-permute-start(bf16[2048,256]{1,0:T(8,128)(2,1)} %bitcast.13), channel_id=1, source_target_pairs={{0,1},{1,0},{2,3},{3,2},{4,5},{5,4},{6,7},{7,6},{8,9},{9,8},{10,11... | collective-permute-start | bytes 3145736 | tf_op jit(solution)/shard_map/ppermute | solution.py:15
  4.4 13.5 %collective-permute-start.4 = (bf16[256,2048]{1,0:T(8,128)(2,1)}, bf16[256,2048]{1,0:T(8,128)(2,1)}, u32[]{:S(2)}, u32[]{:S(2)}) collective-permute-start(bf16[256,2048]{1,0:T(8,128)(2,1)} %bitcast.15), channel_id=1, source_target_pairs={{0,1},{1,0},{2,3},{3,2},{4,5},{5,4},{6,7},{7,6},{8,9},{9,8},{10,11... | collective-permute-start | bytes 3145736 | tf_op jit(solution)/shard_map/ppermute | solution.py:15
  4.5 3.5 %copy-start = (bf16[2048,512]{1,0:T(8,128)(2,1)S(1)}, bf16[2048,512]{1,0:T(8,128)(2,1)}, u32[]{:S(2)}) copy-start(bf16[2048,512]{1,0:T(8,128)(2,1)} %branch_ref.1) | copy-start | bytes 6291460
  4.5 3.5 %copy-start.6 = (bf16[48,1024]{1,0:T(8,128)(2,1)S(1)}, bf16[48,1024]{1,0:T(8,128)(2,1)}, u32[]{:S(2)}) copy-start(bf16[48,1024]{1,0:T(8,128)(2,1)} %tokens_ref.1) | copy-start | bytes 294916
  4.5 3.5 %copy-start.12 = (f32[48,512]{1,0:T(8,128)S(1)}, f32[48,512]{1,0:T(8,128)}, u32[]{:S(2)}) copy-start(f32[48,512]{1,0:T(8,128)} %hidden_ref.1) | copy-start | bytes 294916
  4.5 3.5 %copy-start.15 = (f32[2048]{0:T(1024)S(1)}, f32[2048]{0:T(1024)}, u32[]{:S(2)}) copy-start(f32[2048]{0:T(1024)} %param.21) | copy-start | bytes 24580
  4.5 3.5 %copy-start.16 = (f32[4,512]{1,0:T(4,128)S(1)}, f32[4,512]{1,0:T(4,128)}, u32[]{:S(2)}) copy-start(f32[4,512]{1,0:T(4,128)} %taps_ref.1) | copy-start | bytes 24580
  6.1 0.7 copy-start.8
  6.7 0.7 copy-start.10
  7.4 0.6 copy-start.13
  8.1 1.6 %copy-start.1 = (bf16[2048,512]{1,0:T(8,128)(2,1)S(1)}, bf16[2048,512]{1,0:T(8,128)(2,1)}, u32[]{:S(2)}) copy-start(bf16[2048,512]{1,0:T(8,128)(2,1)} %gelu_ref.1) | copy-start | bytes 6291460
  9.7 0.9 %copy-start.7 = (bf16[48,3,512]{2,0,1:T(8,128)(2,1)S(1)}, bf16[48,3,512]{2,0,1:T(8,128)(2,1)}, u32[]{:S(2)}) copy-start(bf16[48,3,512]{2,0,1:T(8,128)(2,1)} %param.19) | copy-start | bytes 442372
  10.6 0.9 %copy-start.9 = (bf16[512,128]{1,0:T(8,128)(2,1)S(1)}, bf16[512,128]{1,0:T(8,128)(2,1)}, u32[]{:S(2)}) copy-start(bf16[512,128]{1,0:T(8,128)(2,1)} %copy-done.8) | copy-start | bytes 393220
  11.5 0.9 %copy-start.11 = (bf16[512,128]{1,0:T(8,128)(2,1)S(1)}, bf16[512,128]{1,0:T(8,128)(2,1)}, u32[]{:S(2)}) copy-start(bf16[512,128]{1,0:T(8,128)(2,1)} %copy-done.10) | copy-start | bytes 393220
  12.4 0.7 copy-start.18
  13.1 4.1 %copy-start.2 = (bf16[1024,1024]{1,0:T(8,128)(2,1)S(1)}, bf16[1024,1024]{1,0:T(8,128)(2,1)}, u32[]{:S(2)}) copy-start(bf16[1024,1024]{1,0:T(8,128)(2,1)} %weight_ref.1) | copy-start | bytes 6291460
  13.1 4.1 %copy-start.14 = (bf16[96,512]{1,0:T(8,128)(2,1)S(1)}, bf16[96,512]{1,0:T(8,128)(2,1)}, u32[]{:S(2)}) copy-start(bf16[96,512]{1,0:T(8,128)(2,1)} %copy-done.13) | copy-start | bytes 294916
  15.8 35.8 %copy-start.3 = (bf16[1,2048,256]{2,1,0:T(8,128)(2,1)S(1)}, bf16[1,2048,256]{2,1,0:T(8,128)(2,1)}, u32[]{:S(2)}) copy-start(bf16[1,2048,256]{2,1,0:T(8,128)(2,1)} %param.33) | copy-start | bytes 3145732
  15.8 35.8 %copy-start.4 = (bf16[1,2048,256]{2,1,0:T(8,128)(2,1)S(1)}, bf16[1,2048,256]{2,1,0:T(8,128)(2,1)}, u32[]{:S(2)}) copy-start(bf16[1,2048,256]{2,1,0:T(8,128)(2,1)} %param.34) | copy-start | bytes 3145732
  15.8 35.8 %copy-start.5 = (bf16[1,256,2048]{2,1,0:T(8,128)(2,1)S(1)}, bf16[1,256,2048]{2,1,0:T(8,128)(2,1)}, u32[]{:S(2)}) copy-start(bf16[1,256,2048]{2,1,0:T(8,128)(2,1)} %param.35) | copy-start | bytes 3145732
  15.8 35.8 %copy-start.17 = (f32[2048]{0:T(1024)S(1)}, f32[2048]{0:T(1024)}, u32[]{:S(2)}) copy-start(f32[2048]{0:T(1024)} %param.29) | copy-start | bytes 24580
  15.8 1.4 %collective-permute-start.1 = (bf16[48,512]{1,0:T(8,128)(2,1)S(1)}, bf16[48,512]{1,0:T(8,128)(2,1)S(1)}, u32[]{:S(2)}, u32[]{:S(2)}) collective-permute-start(bf16[48,512]{1,0:T(8,128)(2,1)S(1)} %get-tuple-element.16.own_ref), channel_id=1, source_target_pairs={{0,1},{1,0},{2,3},{3,2},{4,5},{5,4},{6,7},{7,6},{8,9},{9,8},{10,11... | collective-permute-start | bytes 147464 | tf_op jit(solution)/shard_map/ppermute | solution.py:15

commit v6 on v5

--- a/solution.py
+++ b/solution.py
@@ -27,9 +27,12 @@
     places = {"s": pltpu.SMEM, "v": pltpu.VMEM, "V": pltpu.VMEM, "h": pltpu.HBM}
     run = pl.pallas_call(
         body,
-        out_shape=tuple(jax.ShapeDtypeStruct(shape, kind) for shape, kind in outs),
+        out_shape=tuple(
+            places[space](shape, kind) if space in "Vh" else jax.ShapeDtypeStruct(shape, kind)
+            for shape, kind, space in outs
+        ),
         in_specs=[pl.BlockSpec(memory_space=places[space]) for space in spaces],
-        out_specs=tuple(pl.BlockSpec(memory_space=pltpu.VMEM) for _ in outs),
+        out_specs=tuple(pl.BlockSpec(memory_space=places[space]) for _, _, space in outs),
         scratch_shapes=getattr(body, "scratch", ()),
         compiler_params=pltpu.CompilerParams(vmem_limit_bytes=body.room << 20),
         cost_estimate=pl.CostEstimate(flops=body.flops, bytes_accessed=0, transcendentals=0),
@@ -72,7 +75,7 @@
 
 def route(ids_ref, prob_ref, logit_ref, place_ref, pick_ref):
     top_count, sequences = ids_ref.shape
-    columns = place_ref.shape[1]
+    columns = place_ref.shape[0]
     experts = columns // 4
     rows = [ids_ref[k : k + 1, :].astype(F32) for k in range(top_count)]
     ids = [as_column(row).astype(jnp.int32) for row in rows]
@@ -84,6 +87,7 @@
     logit_exp = [jnp.exp(logit_ref[k : k + 1, :]) for k in range(top_count)]
     weights = [as_column(prob_ref[...] * one / sum(logit_exp)) for one in logit_exp]
     column = iota((sequences, columns), 1)
+    places = []
     for half in range(2):
         place = jnp.zeros((sequences, columns), F32)
         pick = jnp.zeros((sequences, columns), F32)
@@ -92,11 +96,12 @@
             place = jnp.where(here, 1.0, place)
             pick = jnp.where(here, weights[k], pick)
         span = slice(half * sequences, (half + 1) * sequences)
-        place_ref[span, :] = place.astype(BF16)
+        places.append(place)
         high = pick.astype(BF16)
         pick_ref[span, :] = high
         low_span = slice((2 + half) * sequences, (3 + half) * sequences)
         pick_ref[low_span, :] = (pick - high.astype(F32)).astype(BF16)
+    place_ref[...] = jnp.concatenate(places, axis=0).T.astype(BF16)
 
 
 def begin(
@@ -180,8 +185,13 @@
     mixed_ref[...] = (new_hidden * jax.nn.gelu(gelu_input.astype(F32), approximate=True)).astype(BF16)
 
 
-def project(core_ref, tokens_ref, own_ref, other_ref, weight_ref, place_ref, residual_ref, out_ref):
+def project(
+    core_ref, tokens_ref, own_ref, other_ref, weight_ref, place_ref, fresh_ref, residual_ref, out_ref,
+    new_hbm, sem,
+):
     core = core_ref[0]
+    copy = pltpu.make_async_copy(fresh_ref, new_hbm, sem)
+    copy.start()
     half = own_ref.shape[1]
     own_rows = pl.ds(pl.multiple_of(core * half, half), half)
     other_rows = pl.ds(pl.multiple_of((1 - core) * half, half), half)
@@ -190,10 +200,11 @@
     residual_ref[...] = residual
     width = residual.shape[1] // 2
     stacked = jnp.concatenate([residual[:, :width], residual[:, width:]], axis=0)
-    outgoing = lax.dot_general(
-        place_ref[...], stacked, (((0,), (0,)), ((), ())), preferred_element_type=F32
-    )
-    out_ref[...] = outgoing.astype(BF16).reshape(out_ref.shape)
+    out_ref[...] = mm(place_ref[...], stacked).astype(BF16).reshape(out_ref.shape)
+    copy.wait()
+
+
+project.scratch = (pltpu.SemaphoreType.DMA,)
 
 
 def experts_of(
@@ -290,24 +301,32 @@
     recur_pairs, input_pairs, place, pick = call(
         begin,
         (
-            ((channels, 128), BF16),
-            ((channels, 128), BF16),
-            ((2 * sequences, messages), BF16),
-            ((4 * sequences, messages), BF16),
+            ((channels, 128), BF16, "v"),
+            ((channels, 128), BF16, "v"),
+            ((messages, 2 * sequences), BF16, "v"),
+            ((4 * sequences, messages), BF16, "v"),
         ),
         "h" * 5,
     )(recur_blocks, input_blocks, expert_ids.T, group_prob[None, :], expert_logit.T)
-    new_hidden, mixed = call(
-        mixer, (((sequences, channels), F32), ((sequences, channels), BF16)), "s" + "V" * 11
+    fresh, mixed = call(
+        mixer,
+        (((sequences, channels), F32, "V"), ((sequences, channels), BF16, "v")),
+        "s" + "V" * 11,
     )(
         core, tokens, other_tokens, mixer_gain[None, :], branch_weight, gelu_weight,
         jnp.transpose(conv_state, (1, 0, 2)), conv_kernel, hidden_state, decay_rate[None, :],
         recur_pairs, input_pairs,
     )
     other_mixed = swap(mixed)
-    residual, outgoing = call(
-        project, (((sequences, half), BF16), ((messages // 2, 2, width), BF16)), "s" + "v" * 5
-    )(core, tokens, mixed, other_mixed, output_weight, place)
+    residual, outgoing, new_hidden = call(
+        project,
+        (
+            ((sequences, half), BF16, "v"),
+            ((messages // 2, 2, width), BF16, "v"),
+            ((sequences, channels), F32, "h"),
+        ),
+        "s" + "v" * 5 + "V",
+    )(core, tokens, mixed, other_mixed, output_weight, place, fresh)
     other_gate = swap(expert_gate[0])
     other_up = swap(expert_up[0])
     other_down = swap(expert_down[0])
@@ -315,12 +334,12 @@
         (outgoing, other_gate, other_up, other_down)
     )
     received = exchange(outgoing)
-    (answers,) = call(experts_of, (((messages // 2, 2, width), BF16),), "VvVVVVVV")(
+    (answers,) = call(experts_of, (((messages // 2, 2, width), BF16, "v"),), "VvVVVVVV")(
         received, expert_gain[None, :], expert_gate[0], expert_up[0], expert_down[0], other_gate,
         other_up, other_down,
     )
     returned = exchange(answers)
-    (layer_out,) = call(combine, (((sequences, half), BF16),), "vvv")(returned, pick, residual)
+    (layer_out,) = call(combine, (((sequences, half), BF16, "v"),), "vvv")(returned, pick, residual)
     return (layer_out, new_hidden)
 
 

time: 82.4 us -> 81.8 us (level)
  transfers between devices with their start and end apart: 5 -> 5, of which waited for: 1 -> 1; matrix products, arithmetic and copies ran while one was open for 0% -> 0% of each run, Pallas kernels for 6% -> 5%
where the time goes in v6:
time: 81.8 us; the launch traced here: 81.5 us
  blocking collectives  59.8 us (73%)
  Pallas kernels  8.69 us (11%)
  local copies, waits for them, and re-layouts  6.99 us (9%)
  starting transfers between devices  4.4 us (5%)
  waiting for transfers between devices  0.89 us (1%)
    all_to_all x2, blocking collectives, exchange(): lax.all_to_all(messages, ('tp', 'ep'), split_axis=0, concat_axis=0, tiled...  59.8 us
    pallas_call x5, Pallas kernels, placed(): run(*(pltpu.with_memory_space_constraint(operand, places[space]) if space...  8.69 us
    unnamed x38, local copies, waits for them, and re-layouts  6.99 us
    ppermute x5, starting transfers between devices, swap(): return lax.ppermute(array, 'tp', [(0, 1), (1, 0)])  4.4 us
  transfers between devices with their start and end apart: 5, of which 1 were waited for; matrix products, arithmetic and copies ran while one was open for 0% of the time, Pallas kernels for 5%

profile of v6, /device:TPU:1, one launch (start us, length us, event | category | flops | bytes accessed | tf_op | source)
XLA Modules:
  0.0 81.5 jit_solution(919876447401514650)
XLA Ops:
  0.6 3.3 %collective-permute-start = (bf16[48,1024]{1,0:T(8,128)(2,1)}, bf16[48,1024]{1,0:T(8,128)(2,1)}, u32[]{:S(2)}, u32[]{:S(2)}) collective-permute-start(bf16[48,1024]{1,0:T(8,128)(2,1)} %tokens_ref.1), channel_id=1, source_target_pairs={{0,1},{1,0},{2,3},{3,2},{4,5},{5,4},{6,7},{7,6},{8,9},{9,8},{10,11... | collective-permute-start | bytes 294920 | tf_op jit(solution)/shard_map/ppermute | solution.py:15
  3.9 0.1 collective-permute-start.2
  4.0 0.4 collective-permute-start.3
  4.4 0.1 collective-permute-start.4
  4.5 0.0 copy-start
  4.5 0.0 copy-start.6
  4.5 0.0 copy-start.14
  4.5 0.0 copy-start.15
  4.5 0.0 copy-start.16
  4.6 1.6 %shard_map.185 = (bf16[512,128]{1,0:T(8,128)(2,1)S(1)}, bf16[512,128]{1,0:T(8,128)(2,1)S(1)}, bf16[512,96]{1,0:T(8,128)(2,1)S(1)}, bf16[192,512]{1,0:T(8,128)(2,1)S(1)}) custom-call(bf16[8,64,64]{2,1,0:T(8,128)(2,1)} %recur_hbm.1, bf16[8,64,64]{2,1,0:T(8,128)(2,1)} %input_hbm.1, s32[2,48]{1,0:T(2,128)} %bitcast.21, f32[1,48]{1,0:T(1,128)} %bitcast.23, ...), custom_call_target="tpu_custom_call" | custom-call | flops 20000000000 | tf_op jit(solution)/shard_map/pallas_call | solution.py:42
  6.1 0.0 copy-start.8
  6.1 0.6 copy-done.8
  6.8 0.0 copy-start.10
  6.8 0.7 copy-done.10
  7.4 0.7 copy-done.12
  8.1 0.0 collective-permute-done.other_ref
  8.1 0.0 copy-done
  8.1 0.0 copy-done.6
  8.1 0.0 copy-done.14
  8.1 0.0 copy-done.15
  8.1 0.0 copy-done.16
  8.1 0.0 copy-start.1
  8.1 1.6 %copy-done.1 = bf16[2048,512]{1,0:T(8,128)(2,1)S(1)} copy-done((bf16[2048,512]{1,0:T(8,128)(2,1)S(1)}, bf16[2048,512]{1,0:T(8,128)(2,1)}, u32[]{:S(2)}) %copy-start.1) | copy-done | bytes 2097176
  9.7 0.9 %copy-done.7 = bf16[48,3,512]{2,0,1:T(8,128)(2,1)S(1)} copy-done((bf16[48,3,512]{2,0,1:T(8,128)(2,1)S(1)}, bf16[48,3,512]{2,0,1:T(8,128)(2,1)}, u32[]{:S(2)}) %copy-start.7) | copy-done | bytes 147480
  10.6 0.9 %copy-done.11 = bf16[512,128]{1,0:T(8,128)(2,1)S(1)} copy-done((bf16[512,128]{1,0:T(8,128)(2,1)S(1)}, bf16[512,128]{1,0:T(8,128)(2,1)}, u32[]{:S(2)}) %copy-start.11) | copy-done | bytes 131096
  11.5 0.9 %copy-done.13 = bf16[512,128]{1,0:T(8,128)(2,1)S(1)} copy-done((bf16[512,128]{1,0:T(8,128)(2,1)S(1)}, bf16[512,128]{1,0:T(8,128)(2,1)}, u32[]{:S(2)}) %copy-start.13) | copy-done | bytes 131096
  12.4 0.7 copy-done.18
  13.1 2.1 %shard_map.186 = (f32[48,512]{1,0:T(8,128)S(1)}, bf16[48,512]{1,0:T(8,128)(2,1)S(1)}) custom-call(s32[1]{0:T(128)} %bitcast.core_ref, bf16[48,1024]{1,0:T(8,128)(2,1)S(1)} %copy-done.6, bf16[48,1024]{1,0:T(8,128)(2,1)} %collective-permute-done.other_ref, f32[1,2048]{1,0:T(1,128)S(1)} %bitcast.18, bf16[2048,512]{1,0:T(8,128)(2,1)S(1)} %copy-done, ...), custom_call_target="tpu_custom_call" | custom-call | flops 210000000 | tf_op jit(solution)/shard_map/pallas_call | solution.py:42
  15.2 0.0 copy-start.3
  15.2 0.0 copy-start.4
  15.2 0.0 copy-start.5
  15.3 0.0 copy-start.17
  15.3 0.5 collective-permute-start.1
  15.8 0.9 %collective-permute-done.1.other_ref = bf16[48,512]{1,0:T(8,128)(2,1)S(1)} collective-permute-done((bf16[48,512]{1,0:T(8,128)(2,1)S(1)}, bf16[48,512]{1,0:T(8,128)(2,1)S(1)}, u32[]{:S(2)}, u32[]{:S(2)}) %collective-permute-start.1) | collective-permute-done | bytes 49184 | tf_op jit(solution)/shard_map/ppermute | solution.py:15
  16.6 0.0 copy-done.2
  16.6 0.0 copy-done.9
  16.7 0.8 shard_map.187
  17.4 0.0 collective-permute-done.2.gate_b
  17.4 0.0 collective-permute-done.3.up_b
  17.4 0.0 collective-permute-done.4.down_b
  17.4 33.6 %all_to_all.10.rows_ref = bf16[256,2,512]{2,1,0:T(2,128)(2,1)S(1)} all-to-all(bf16[256,2,512]{2,1,0:T(2,128)(2,1)S(1)} %get-tuple-element.21), channel_id=1, replica_groups=mesh['ep'=128,'tp'=2] {'tp','ep'}, dimensions={0} | all-to-all | bytes 1048576 | tf_op jit(solution)/shard_map/all_to_all | solution.py:271
  51.1 0.0 copy-done.3
  51.1 0.0 copy-done.4
  51.1 0.0 copy-done.5
  51.1 0.0 copy-done.17
  51.1 3.4 %shard_map.188 = bf16[256,2,512]{2,1,0:T(2,128)(2,1)S(1)} custom-call(bf16[256,2,512]{2,1,0:T(2,128)(2,1)S(1)} %all_to_all.10.rows_ref, f32[1,2048]{1,0:T(1,128)S(1)} %bitcast.19, bf16[2048,256]{1,0:T(8,128)(2,1)S(1)} %bitcast.12, bf16[2048,256]{1,0:T(8,128)(2,1)S(1)} %bitcast.14, bf16[256,2048]{1,0:T(8,128)(2,1)S(1)} %bitcast.16, ...), custom_call_target="tpu_custom_call" | custom-call | flops 810000000 | tf_op jit(solution)/shard_map/pallas_call | solution.py:42
  54.5 26.2 %all_to_all.11.returned_ref = bf16[256,2,512]{2,1,0:T(2,128)(2,1)S(1)} all-to-all(bf16[256,2,512]{2,1,0:T(2,128)(2,1)S(1)} %shard_map.188), channel_id=1, replica_groups=mesh['ep'=128,'tp'=2] {'tp','ep'}, dimensions={0} | all-to-all | bytes 1048576 | tf_op jit(solution)/shard_map/all_to_all | solution.py:271
  80.6 0.9 %shard_map.189 = bf16[48,1024]{1,0:T(8,128)(2,1)} custom-call(bf16[256,2,512]{2,1,0:T(2,128)(2,1)S(1)} %all_to_all.11.returned_ref, bf16[192,512]{1,0:T(8,128)(2,1)S(1)} %get-tuple-element.25.pick_ref, bf16[48,1024]{1,0:T(8,128)(2,1)S(1)} %get-tuple-element.26.residual_ref), custom_call_target="tpu_custom_call" | custom-call | flops 100000000 | tf_op jit(solution)/shard_map/pallas_call | solution.py:42
  (7 shorter events, 0.0 us)
Async XLA Ops:
  0.6 7.5 %collective-permute-start = (bf16[48,1024]{1,0:T(8,128)(2,1)}, bf16[48,1024]{1,0:T(8,128)(2,1)}, u32[]{:S(2)}, u32[]{:S(2)}) collective-permute-start(bf16[48,1024]{1,0:T(8,128)(2,1)} %tokens_ref.1), channel_id=1, source_target_pairs={{0,1},{1,0},{2,3},{3,2},{4,5},{5,4},{6,7},{7,6},{8,9},{9,8},{10,11... | collective-permute-start | bytes 294920 | tf_op jit(solution)/shard_map/ppermute | solution.py:15
  3.9 13.5 %collective-permute-start.2 = (bf16[2048,256]{1,0:T(8,128)(2,1)}, bf16[2048,256]{1,0:T(8,128)(2,1)S(1)}, u32[]{:S(2)}, u32[]{:S(2)}) collective-permute-start(bf16[2048,256]{1,0:T(8,128)(2,1)} %bitcast.11), channel_id=1, source_target_pairs={{0,1},{1,0},{2,3},{3,2},{4,5},{5,4},{6,7},{7,6},{8,9},{9,8},{10,11... | collective-permute-start | bytes 3145736 | tf_op jit(solution)/shard_map/ppermute | solution.py:15
  4.0 13.4 %collective-permute-start.3 = (bf16[2048,256]{1,0:T(8,128)(2,1)}, bf16[2048,256]{1,0:T(8,128)(2,1)}, u32[]{:S(2)}, u32[]{:S(2)}) collective-permute-start(bf16[2048,256]{1,0:T(8,128)(2,1)} %bitcast.13), channel_id=1, source_target_pairs={{0,1},{1,0},{2,3},{3,2},{4,5},{5,4},{6,7},{7,6},{8,9},{9,8},{10,11... | collective-permute-start | bytes 3145736 | tf_op jit(solution)/shard_map/ppermute | solution.py:15
  4.4 13.0 %collective-permute-start.4 = (bf16[256,2048]{1,0:T(8,128)(2,1)}, bf16[256,2048]{1,0:T(8,128)(2,1)}, u32[]{:S(2)}, u32[]{:S(2)}) collective-permute-start(bf16[256,2048]{1,0:T(8,128)(2,1)} %bitcast.15), channel_id=1, source_target_pairs={{0,1},{1,0},{2,3},{3,2},{4,5},{5,4},{6,7},{7,6},{8,9},{9,8},{10,11... | collective-permute-start | bytes 3145736 | tf_op jit(solution)/shard_map/ppermute | solution.py:15
  4.5 3.6 %copy-start = (bf16[2048,512]{1,0:T(8,128)(2,1)S(1)}, bf16[2048,512]{1,0:T(8,128)(2,1)}, u32[]{:S(2)}) copy-start(bf16[2048,512]{1,0:T(8,128)(2,1)} %branch_ref.1) | copy-start | bytes 6291460
  4.5 3.6 %copy-start.6 = (bf16[48,1024]{1,0:T(8,128)(2,1)S(1)}, bf16[48,1024]{1,0:T(8,128)(2,1)}, u32[]{:S(2)}) copy-start(bf16[48,1024]{1,0:T(8,128)(2,1)} %tokens_ref.1) | copy-start | bytes 294916
  4.5 3.6 %copy-start.14 = (f32[48,512]{1,0:T(8,128)S(1)}, f32[48,512]{1,0:T(8,128)}, u32[]{:S(2)}) copy-start(f32[48,512]{1,0:T(8,128)} %hidden_ref.1) | copy-start | bytes 294916
  4.5 3.6 %copy-start.15 = (f32[2048]{0:T(1024)S(1)}, f32[2048]{0:T(1024)}, u32[]{:S(2)}) copy-start(f32[2048]{0:T(1024)} %param.21) | copy-start | bytes 24580
  4.5 3.6 %copy-start.16 = (f32[4,512]{1,0:T(4,128)S(1)}, f32[4,512]{1,0:T(4,128)}, u32[]{:S(2)}) copy-start(f32[4,512]{1,0:T(4,128)} %taps_ref.1) | copy-start | bytes 24580
  6.1 0.7 copy-start.8
  6.8 0.7 copy-start.10
  7.4 0.7 copy-start.12
  8.1 1.6 %copy-start.1 = (bf16[2048,512]{1,0:T(8,128)(2,1)S(1)}, bf16[2048,512]{1,0:T(8,128)(2,1)}, u32[]{:S(2)}) copy-start(bf16[2048,512]{1,0:T(8,128)(2,1)} %gelu_ref.1) | copy-start | bytes 6291460
  9.7 0.9 %copy-start.7 = (bf16[48,3,512]{2,0,1:T(8,128)(2,1)S(1)}, bf16[48,3,512]{2,0,1:T(8,128)(2,1)}, u32[]{:S(2)}) copy-start(bf16[48,3,512]{2,0,1:T(8,128)(2,1)} %param.19) | copy-start | bytes 442372
  10.6 0.9 %copy-start.11 = (bf16[512,128]{1,0:T(8,128)(2,1)S(1)}, bf16[512,128]{1,0:T(8,128)(2,1)}, u32[]{:S(2)}) copy-start(bf16[512,128]{1,0:T(8,128)(2,1)} %copy-done.10) | copy-start | bytes 393220
  11.5 0.9 %copy-start.13 = (bf16[512,128]{1,0:T(8,128)(2,1)S(1)}, bf16[512,128]{1,0:T(8,128)(2,1)}, u32[]{:S(2)}) copy-start(bf16[512,128]{1,0:T(8,128)(2,1)} %copy-done.12) | copy-start | bytes 393220
  12.4 0.7 copy-start.18
  13.1 3.5 %copy-start.2 = (bf16[1024,1024]{1,0:T(8,128)(2,1)S(1)}, bf16[1024,1024]{1,0:T(8,128)(2,1)}, u32[]{:S(2)}) copy-start(bf16[1024,1024]{1,0:T(8,128)(2,1)} %weight_ref.1) | copy-start | bytes 6291460
  13.1 3.5 %copy-start.9 = (bf16[512,96]{1,0:T(8,128)(2,1)S(1)}, bf16[512,96]{1,0:T(8,128)(2,1)}, u32[]{:S(2)}) copy-start(bf16[512,96]{1,0:T(8,128)(2,1)} %copy-done.8) | copy-start | bytes 294916
  15.2 35.8 %copy-start.3 = (bf16[1,2048,256]{2,1,0:T(8,128)(2,1)S(1)}, bf16[1,2048,256]{2,1,0:T(8,128)(2,1)}, u32[]{:S(2)}) copy-start(bf16[1,2048,256]{2,1,0:T(8,128)(2,1)} %param.33) | copy-start | bytes 3145732
  15.2 35.8 %copy-start.4 = (bf16[1,2048,256]{2,1,0:T(8,128)(2,1)S(1)}, bf16[1,2048,256]{2,1,0:T(8,128)(2,1)}, u32[]{:S(2)}) copy-start(bf16[1,2048,256]{2,1,0:T(8,128)(2,1)} %param.34) | copy-start | bytes 3145732
  15.2 35.8 %copy-start.5 = (bf16[1,256,2048]{2,1,0:T(8,128)(2,1)S(1)}, bf16[1,256,2048]{2,1,0:T(8,128)(2,1)}, u32[]{:S(2)}) copy-start(bf16[1,256,2048]{2,1,0:T(8,128)(2,1)} %param.35) | copy-start | bytes 3145732
  15.3 35.8 %copy-start.17 = (f32[2048]{0:T(1024)S(1)}, f32[2048]{0:T(1024)}, u32[]{:S(2)}) copy-start(f32[2048]{0:T(1024)} %param.29) | copy-start | bytes 24580
  15.3 1.4 %collective-permute-start.1 = (bf16[48,512]{1,0:T(8,128)(2,1)S(1)}, bf16[48,512]{1,0:T(8,128)(2,1)S(1)}, u32[]{:S(2)}, u32[]{:S(2)}) collective-permute-start(bf16[48,512]{1,0:T(8,128)(2,1)S(1)} %get-tuple-element.17.own_ref), channel_id=1, source_target_pairs={{0,1},{1,0},{2,3},{3,2},{4,5},{5,4},{6,7},{7,6},{8,9},{9,8},{10,11... | collective-permute-start | bytes 147464 | tf_op jit(solution)/shard_map/ppermute | solution.py:15

commit v7 on v6

--- a/solution.py
+++ b/solution.py
@@ -220,21 +220,20 @@
     def of_quarter(q):
         return pl.ds((q // 2) * 2 * slots + q % 2, slots, 2)
 
-    quarters = [
-        jnp.concatenate([scratch_ref[piece, of_quarter(q), :] for piece in range(pieces)], axis=1)
-        for q in range(4)
-    ]
-    squares = sum(jnp.sum(part * part, axis=1, keepdims=True) for part in quarters)
-    scaling = lax.rsqrt(squares / (4 * width) + EPSILON)
-    quarters = [
-        (part * scaling * gain_ref[:, q * width : (q + 1) * width]).astype(BF16)
-        for q, part in enumerate(quarters)
-    ]
-    rows = jnp.concatenate(quarters, axis=1)
-    hidden = [
-        (jax.nn.silu(mm(rows, gate[...])) * mm(rows, up[...])).astype(BF16)
-        for gate, up in ((gate_a, up_a), (gate_b, up_b))
-    ]
+    squares = jnp.zeros((slots, 128), F32)
+    parts = []
+    for q in range(4):
+        for piece in range(pieces):
+            part = scratch_ref[piece, of_quarter(q), :]
+            start = q * width + piece * 128
+            squares = squares + part * part
+            parts.append((part * gain_ref[:, start : start + 128]).astype(BF16))
+    scaling = lax.rsqrt(jnp.sum(squares, axis=1, keepdims=True) / (4 * width) + EPSILON)
+    rows = jnp.concatenate(parts, axis=1)
+    hidden = []
+    for gate_ref, up_ref in ((gate_a, up_a), (gate_b, up_b)):
+        gate = mm(rows, gate_ref[...]) * scaling
+        hidden.append((jax.nn.silu(gate) * (mm(rows, up_ref[...]) * scaling)).astype(BF16))
     for q in range(4):
         span = slice(q * width, (q + 1) * width)
         answer = mm(hidden[0], down_a[:, span]) + mm(hidden[1], down_b[:, span])

time: 81.8 us -> 81.6 us (level)
  no operation moved by 1% of the time
where the time goes in v7:
time: 81.6 us; the launch traced here: 81.3 us
  blocking collectives  59.8 us (73%)
  Pallas kernels  8.48 us (10%)
  local copies, waits for them, and re-layouts  6.99 us (9%)
  starting transfers between devices  4.4 us (5%)
  waiting for transfers between devices  0.89 us (1%)
    all_to_all x2, blocking collectives, exchange(): lax.all_to_all(messages, ('tp', 'ep'), split_axis=0, concat_axis=0, tiled...  59.8 us
    pallas_call x5, Pallas kernels, placed(): run(*(pltpu.with_memory_space_constraint(operand, places[space]) if space...  8.48 us
    unnamed x38, local copies, waits for them, and re-layouts  6.99 us
    ppermute x5, starting transfers between devices, swap(): return lax.ppermute(array, 'tp', [(0, 1), (1, 0)])  4.4 us
  transfers between devices with their start and end apart: 5, of which 1 were waited for; matrix products, arithmetic and copies ran while one was open for 0% of the time, Pallas kernels for 5%

profile of v7, /device:TPU:1, one launch (start us, length us, event | category | flops | bytes accessed | tf_op | source)
XLA Modules:
  0.0 81.3 jit_solution(11386268225246934103)
XLA Ops:
  0.6 3.3 %collective-permute-start = (bf16[48,1024]{1,0:T(8,128)(2,1)}, bf16[48,1024]{1,0:T(8,128)(2,1)}, u32[]{:S(2)}, u32[]{:S(2)}) collective-permute-start(bf16[48,1024]{1,0:T(8,128)(2,1)} %tokens_ref.1), channel_id=1, source_target_pairs={{0,1},{1,0},{2,3},{3,2},{4,5},{5,4},{6,7},{7,6},{8,9},{9,8},{10,11... | collective-permute-start | bytes 294920 | tf_op jit(solution)/shard_map/ppermute | solution.py:15
  3.9 0.1 collective-permute-start.2
  4.0 0.4 collective-permute-start.3
  4.4 0.1 collective-permute-start.4
  4.5 0.0 copy-start
  4.5 0.0 copy-start.6
  4.5 0.0 copy-start.14
  4.5 0.0 copy-start.15
  4.5 0.0 copy-start.16
  4.6 1.6 %shard_map.185 = (bf16[512,128]{1,0:T(8,128)(2,1)S(1)}, bf16[512,128]{1,0:T(8,128)(2,1)S(1)}, bf16[512,96]{1,0:T(8,128)(2,1)S(1)}, bf16[192,512]{1,0:T(8,128)(2,1)S(1)}) custom-call(bf16[8,64,64]{2,1,0:T(8,128)(2,1)} %recur_hbm.1, bf16[8,64,64]{2,1,0:T(8,128)(2,1)} %input_hbm.1, s32[2,48]{1,0:T(2,128)} %bitcast.21, f32[1,48]{1,0:T(1,128)} %bitcast.23, ...), custom_call_target="tpu_custom_call" | custom-call | flops 20000000000 | tf_op jit(solution)/shard_map/pallas_call | solution.py:42
  6.1 0.0 copy-start.8
  6.1 0.6 copy-done.8
  6.8 0.0 copy-start.10
  6.8 0.7 copy-done.10
  7.4 0.7 copy-done.12
  8.1 0.0 collective-permute-done.other_ref
  8.1 0.0 copy-done
  8.1 0.0 copy-done.6
  8.1 0.0 copy-done.14
  8.1 0.0 copy-done.15
  8.1 0.0 copy-done.16
  8.1 0.0 copy-start.1
  8.1 1.6 %copy-done.1 = bf16[2048,512]{1,0:T(8,128)(2,1)S(1)} copy-done((bf16[2048,512]{1,0:T(8,128)(2,1)S(1)}, bf16[2048,512]{1,0:T(8,128)(2,1)}, u32[]{:S(2)}) %copy-start.1) | copy-done | bytes 2097176
  9.7 0.9 %copy-done.7 = bf16[48,3,512]{2,0,1:T(8,128)(2,1)S(1)} copy-done((bf16[48,3,512]{2,0,1:T(8,128)(2,1)S(1)}, bf16[48,3,512]{2,0,1:T(8,128)(2,1)}, u32[]{:S(2)}) %copy-start.7) | copy-done | bytes 147480
  10.6 0.9 %copy-done.11 = bf16[512,128]{1,0:T(8,128)(2,1)S(1)} copy-done((bf16[512,128]{1,0:T(8,128)(2,1)S(1)}, bf16[512,128]{1,0:T(8,128)(2,1)}, u32[]{:S(2)}) %copy-start.11) | copy-done | bytes 131096
  11.5 0.9 %copy-done.13 = bf16[512,128]{1,0:T(8,128)(2,1)S(1)} copy-done((bf16[512,128]{1,0:T(8,128)(2,1)S(1)}, bf16[512,128]{1,0:T(8,128)(2,1)}, u32[]{:S(2)}) %copy-start.13) | copy-done | bytes 131096
  12.4 0.7 copy-done.18
  13.1 2.1 %shard_map.186 = (f32[48,512]{1,0:T(8,128)S(1)}, bf16[48,512]{1,0:T(8,128)(2,1)S(1)}) custom-call(s32[1]{0:T(128)} %bitcast.core_ref, bf16[48,1024]{1,0:T(8,128)(2,1)S(1)} %copy-done.6, bf16[48,1024]{1,0:T(8,128)(2,1)} %collective-permute-done.other_ref, f32[1,2048]{1,0:T(1,128)S(1)} %bitcast.18, bf16[2048,512]{1,0:T(8,128)(2,1)S(1)} %copy-done, ...), custom_call_target="tpu_custom_call" | custom-call | flops 210000000 | tf_op jit(solution)/shard_map/pallas_call | solution.py:42
  15.2 0.0 copy-start.3
  15.2 0.0 copy-start.4
  15.2 0.0 copy-start.5
  15.3 0.0 copy-start.17
  15.3 0.5 collective-permute-start.1
  15.8 0.9 %collective-permute-done.1.other_ref = bf16[48,512]{1,0:T(8,128)(2,1)S(1)} collective-permute-done((bf16[48,512]{1,0:T(8,128)(2,1)S(1)}, bf16[48,512]{1,0:T(8,128)(2,1)S(1)}, u32[]{:S(2)}, u32[]{:S(2)}) %collective-permute-start.1) | collective-permute-done | bytes 49184 | tf_op jit(solution)/shard_map/ppermute | solution.py:15
  16.6 0.0 copy-done.2
  16.6 0.0 copy-done.9
  16.7 0.8 shard_map.187
  17.4 0.0 collective-permute-done.2.gate_b
  17.4 0.0 collective-permute-done.3.up_b
  17.4 0.0 collective-permute-done.4.down_b
  17.4 33.6 %all_to_all.10.rows_ref = bf16[256,2,512]{2,1,0:T(2,128)(2,1)S(1)} all-to-all(bf16[256,2,512]{2,1,0:T(2,128)(2,1)S(1)} %get-tuple-element.21), channel_id=1, replica_groups=mesh['ep'=128,'tp'=2] {'tp','ep'}, dimensions={0} | all-to-all | bytes 1048576 | tf_op jit(solution)/shard_map/all_to_all | solution.py:270
  51.1 0.0 copy-done.3
  51.1 0.0 copy-done.4
  51.1 0.0 copy-done.5
  51.1 0.0 copy-done.17
  51.1 3.2 %shard_map.188 = bf16[256,2,512]{2,1,0:T(2,128)(2,1)S(1)} custom-call(bf16[256,2,512]{2,1,0:T(2,128)(2,1)S(1)} %all_to_all.10.rows_ref, f32[1,2048]{1,0:T(1,128)S(1)} %bitcast.19, bf16[2048,256]{1,0:T(8,128)(2,1)S(1)} %bitcast.12, bf16[2048,256]{1,0:T(8,128)(2,1)S(1)} %bitcast.14, bf16[256,2048]{1,0:T(8,128)(2,1)S(1)} %bitcast.16, ...), custom_call_target="tpu_custom_call" | custom-call | flops 810000000 | tf_op jit(solution)/shard_map/pallas_call | solution.py:42
  54.2 26.2 %all_to_all.11.returned_ref = bf16[256,2,512]{2,1,0:T(2,128)(2,1)S(1)} all-to-all(bf16[256,2,512]{2,1,0:T(2,128)(2,1)S(1)} %shard_map.188), channel_id=1, replica_groups=mesh['ep'=128,'tp'=2] {'tp','ep'}, dimensions={0} | all-to-all | bytes 1048576 | tf_op jit(solution)/shard_map/all_to_all | solution.py:270
  80.4 0.9 %shard_map.189 = bf16[48,1024]{1,0:T(8,128)(2,1)} custom-call(bf16[256,2,512]{2,1,0:T(2,128)(2,1)S(1)} %all_to_all.11.returned_ref, bf16[192,512]{1,0:T(8,128)(2,1)S(1)} %get-tuple-element.25.pick_ref, bf16[48,1024]{1,0:T(8,128)(2,1)S(1)} %get-tuple-element.26.residual_ref), custom_call_target="tpu_custom_call" | custom-call | flops 100000000 | tf_op jit(solution)/shard_map/pallas_call | solution.py:42
  (7 shorter events, 0.0 us)
Async XLA Ops:
  0.6 7.5 %collective-permute-start = (bf16[48,1024]{1,0:T(8,128)(2,1)}, bf16[48,1024]{1,0:T(8,128)(2,1)}, u32[]{:S(2)}, u32[]{:S(2)}) collective-permute-start(bf16[48,1024]{1,0:T(8,128)(2,1)} %tokens_ref.1), channel_id=1, source_target_pairs={{0,1},{1,0},{2,3},{3,2},{4,5},{5,4},{6,7},{7,6},{8,9},{9,8},{10,11... | collective-permute-start | bytes 294920 | tf_op jit(solution)/shard_map/ppermute | solution.py:15
  3.9 13.5 %collective-permute-start.2 = (bf16[2048,256]{1,0:T(8,128)(2,1)}, bf16[2048,256]{1,0:T(8,128)(2,1)S(1)}, u32[]{:S(2)}, u32[]{:S(2)}) collective-permute-start(bf16[2048,256]{1,0:T(8,128)(2,1)} %bitcast.11), channel_id=1, source_target_pairs={{0,1},{1,0},{2,3},{3,2},{4,5},{5,4},{6,7},{7,6},{8,9},{9,8},{10,11... | collective-permute-start | bytes 3145736 | tf_op jit(solution)/shard_map/ppermute | solution.py:15
  4.0 13.4 %collective-permute-start.3 = (bf16[2048,256]{1,0:T(8,128)(2,1)}, bf16[2048,256]{1,0:T(8,128)(2,1)}, u32[]{:S(2)}, u32[]{:S(2)}) collective-permute-start(bf16[2048,256]{1,0:T(8,128)(2,1)} %bitcast.13), channel_id=1, source_target_pairs={{0,1},{1,0},{2,3},{3,2},{4,5},{5,4},{6,7},{7,6},{8,9},{9,8},{10,11... | collective-permute-start | bytes 3145736 | tf_op jit(solution)/shard_map/ppermute | solution.py:15
  4.4 13.0 %collective-permute-start.4 = (bf16[256,2048]{1,0:T(8,128)(2,1)}, bf16[256,2048]{1,0:T(8,128)(2,1)}, u32[]{:S(2)}, u32[]{:S(2)}) collective-permute-start(bf16[256,2048]{1,0:T(8,128)(2,1)} %bitcast.15), channel_id=1, source_target_pairs={{0,1},{1,0},{2,3},{3,2},{4,5},{5,4},{6,7},{7,6},{8,9},{9,8},{10,11... | collective-permute-start | bytes 3145736 | tf_op jit(solution)/shard_map/ppermute | solution.py:15
  4.5 3.6 %copy-start = (bf16[2048,512]{1,0:T(8,128)(2,1)S(1)}, bf16[2048,512]{1,0:T(8,128)(2,1)}, u32[]{:S(2)}) copy-start(bf16[2048,512]{1,0:T(8,128)(2,1)} %branch_ref.1) | copy-start | bytes 6291460
  4.5 3.6 %copy-start.6 = (bf16[48,1024]{1,0:T(8,128)(2,1)S(1)}, bf16[48,1024]{1,0:T(8,128)(2,1)}, u32[]{:S(2)}) copy-start(bf16[48,1024]{1,0:T(8,128)(2,1)} %tokens_ref.1) | copy-start | bytes 294916
  4.5 3.6 %copy-start.14 = (f32[48,512]{1,0:T(8,128)S(1)}, f32[48,512]{1,0:T(8,128)}, u32[]{:S(2)}) copy-start(f32[48,512]{1,0:T(8,128)} %hidden_ref.1) | copy-start | bytes 294916
  4.5 3.6 %copy-start.15 = (f32[2048]{0:T(1024)S(1)}, f32[2048]{0:T(1024)}, u32[]{:S(2)}) copy-start(f32[2048]{0:T(1024)} %param.21) | copy-start | bytes 24580
  4.5 3.6 %copy-start.16 = (f32[4,512]{1,0:T(4,128)S(1)}, f32[4,512]{1,0:T(4,128)}, u32[]{:S(2)}) copy-start(f32[4,512]{1,0:T(4,128)} %taps_ref.1) | copy-start | bytes 24580
  6.1 0.7 copy-start.8
  6.8 0.7 copy-start.10
  7.4 0.7 copy-start.12
  8.1 1.6 %copy-start.1 = (bf16[2048,512]{1,0:T(8,128)(2,1)S(1)}, bf16[2048,512]{1,0:T(8,128)(2,1)}, u32[]{:S(2)}) copy-start(bf16[2048,512]{1,0:T(8,128)(2,1)} %gelu_ref.1) | copy-start | bytes 6291460
  9.7 0.9 %copy-start.7 = (bf16[48,3,512]{2,0,1:T(8,128)(2,1)S(1)}, bf16[48,3,512]{2,0,1:T(8,128)(2,1)}, u32[]{:S(2)}) copy-start(bf16[48,3,512]{2,0,1:T(8,128)(2,1)} %param.19) | copy-start | bytes 442372
  10.6 0.9 %copy-start.11 = (bf16[512,128]{1,0:T(8,128)(2,1)S(1)}, bf16[512,128]{1,0:T(8,128)(2,1)}, u32[]{:S(2)}) copy-start(bf16[512,128]{1,0:T(8,128)(2,1)} %copy-done.10) | copy-start | bytes 393220
  11.5 0.9 %copy-start.13 = (bf16[512,128]{1,0:T(8,128)(2,1)S(1)}, bf16[512,128]{1,0:T(8,128)(2,1)}, u32[]{:S(2)}) copy-start(bf16[512,128]{1,0:T(8,128)(2,1)} %copy-done.12) | copy-start | bytes 393220
  12.4 0.7 copy-start.18
  13.1 3.5 %copy-start.2 = (bf16[1024,1024]{1,0:T(8,128)(2,1)S(1)}, bf16[1024,1024]{1,0:T(8,128)(2,1)}, u32[]{:S(2)}) copy-start(bf16[1024,1024]{1,0:T(8,128)(2,1)} %weight_ref.1) | copy-start | bytes 6291460
  13.1 3.5 %copy-start.9 = (bf16[512,96]{1,0:T(8,128)(2,1)S(1)}, bf16[512,96]{1,0:T(8,128)(2,1)}, u32[]{:S(2)}) copy-start(bf16[512,96]{1,0:T(8,128)(2,1)} %copy-done.8) | copy-start | bytes 294916
  15.2 35.8 %copy-start.3 = (bf16[1,2048,256]{2,1,0:T(8,128)(2,1)S(1)}, bf16[1,2048,256]{2,1,0:T(8,128)(2,1)}, u32[]{:S(2)}) copy-start(bf16[1,2048,256]{2,1,0:T(8,128)(2,1)} %param.33) | copy-start | bytes 3145732
  15.2 35.8 %copy-start.4 = (bf16[1,2048,256]{2,1,0:T(8,128)(2,1)S(1)}, bf16[1,2048,256]{2,1,0:T(8,128)(2,1)}, u32[]{:S(2)}) copy-start(bf16[1,2048,256]{2,1,0:T(8,128)(2,1)} %param.34) | copy-start | bytes 3145732
  15.2 35.8 %copy-start.5 = (bf16[1,256,2048]{2,1,0:T(8,128)(2,1)S(1)}, bf16[1,256,2048]{2,1,0:T(8,128)(2,1)}, u32[]{:S(2)}) copy-start(bf16[1,256,2048]{2,1,0:T(8,128)(2,1)} %param.35) | copy-start | bytes 3145732
  15.3 35.8 %copy-start.17 = (f32[2048]{0:T(1024)S(1)}, f32[2048]{0:T(1024)}, u32[]{:S(2)}) copy-start(f32[2048]{0:T(1024)} %param.29) | copy-start | bytes 24580
  15.3 1.4 %collective-permute-start.1 = (bf16[48,512]{1,0:T(8,128)(2,1)S(1)}, bf16[48,512]{1,0:T(8,128)(2,1)S(1)}, u32[]{:S(2)}, u32[]{:S(2)}) collective-permute-start(bf16[48,512]{1,0:T(8,128)(2,1)S(1)} %get-tuple-element.17.own_ref), channel_id=1, source_target_pairs={{0,1},{1,0},{2,3},{3,2},{4,5},{5,4},{6,7},{7,6},{8,9},{9,8},{10,11... | collective-permute-start | bytes 147464 | tf_op jit(solution)/shard_map/ppermute | solution.py:15

commit v8 on v7

--- a/solution.py
+++ b/solution.py
@@ -215,7 +215,7 @@
     pieces = width // 128
     flat = rows_ref[...].reshape(2 * messages, width)
     for piece in range(pieces):
-        scratch_ref[piece] = flat[:, piece * 128 : (piece + 1) * 128].astype(F32)
+        scratch_ref[piece, : 2 * messages, :] = flat[:, piece * 128 : (piece + 1) * 128].astype(F32)
 
     def of_quarter(q):
         return pl.ds((q // 2) * 2 * slots + q % 2, slots, 2)
@@ -239,11 +239,11 @@
         answer = mm(hidden[0], down_a[:, span]) + mm(hidden[1], down_b[:, span])
         for piece in range(pieces):
             scratch_ref[piece, of_quarter(q), :] = answer[:, piece * 128 : (piece + 1) * 128]
-    answers = jnp.concatenate([scratch_ref[piece].astype(BF16) for piece in range(pieces)], axis=1)
+    answers = jnp.concatenate([scratch_ref[piece, : 2 * messages, :].astype(BF16) for piece in range(pieces)], axis=1)
     out_ref[...] = answers.reshape(out_ref.shape)
 
 
-experts_of.scratch = (pltpu.VMEM((4, 512, 128), F32),)
+experts_of.scratch = (pltpu.VMEM((4, 528, 128), F32),)
 
 
 def combine(returned_ref, pick_ref, residual_ref, out_ref):

time: 81.6 us -> 81.6 us (level)
  no operation moved by 1% of the time
where the time goes in v8:
time: 81.6 us; the launch traced here: 81.3 us
  blocking collectives  59.8 us (73%)
  Pallas kernels  8.47 us (10%)
  local copies, waits for them, and re-layouts  6.99 us (9%)
  starting transfers between devices  4.4 us (5%)
  waiting for transfers between devices  0.89 us (1%)
    all_to_all x2, blocking collectives, exchange(): lax.all_to_all(messages, ('tp', 'ep'), split_axis=0, concat_axis=0, tiled...  59.8 us
    pallas_call x5, Pallas kernels, placed(): run(*(pltpu.with_memory_space_constraint(operand, places[space]) if space...  8.47 us
    unnamed x38, local copies, waits for them, and re-layouts  6.99 us
    ppermute x5, starting transfers between devices, swap(): return lax.ppermute(array, 'tp', [(0, 1), (1, 0)])  4.4 us
  transfers between devices with their start and end apart: 5, of which 1 were waited for; matrix products, arithmetic and copies ran while one was open for 0% of the time, Pallas kernels for 5%

profile of v8, /device:TPU:1, one launch (start us, length us, event | category | flops | bytes accessed | tf_op | source)
XLA Modules:
  0.0 81.3 jit_solution(7700341293418358437)
XLA Ops:
  0.6 3.3 %collective-permute-start = (bf16[48,1024]{1,0:T(8,128)(2,1)}, bf16[48,1024]{1,0:T(8,128)(2,1)}, u32[]{:S(2)}, u32[]{:S(2)}) collective-permute-start(bf16[48,1024]{1,0:T(8,128)(2,1)} %tokens_ref.1), channel_id=1, source_target_pairs={{0,1},{1,0},{2,3},{3,2},{4,5},{5,4},{6,7},{7,6},{8,9},{9,8},{10,11... | collective-permute-start | bytes 294920 | tf_op jit(solution)/shard_map/ppermute | solution.py:15
  3.9 0.1 collective-permute-start.2
  4.0 0.4 collective-permute-start.3
  4.4 0.1 collective-permute-start.4
  4.5 0.0 copy-start
  4.5 0.0 copy-start.6
  4.5 0.0 copy-start.14
  4.5 0.0 copy-start.15
  4.5 0.0 copy-start.16
  4.6 1.6 %shard_map.185 = (bf16[512,128]{1,0:T(8,128)(2,1)S(1)}, bf16[512,128]{1,0:T(8,128)(2,1)S(1)}, bf16[512,96]{1,0:T(8,128)(2,1)S(1)}, bf16[192,512]{1,0:T(8,128)(2,1)S(1)}) custom-call(bf16[8,64,64]{2,1,0:T(8,128)(2,1)} %recur_hbm.1, bf16[8,64,64]{2,1,0:T(8,128)(2,1)} %input_hbm.1, s32[2,48]{1,0:T(2,128)} %bitcast.21, f32[1,48]{1,0:T(1,128)} %bitcast.23, ...), custom_call_target="tpu_custom_call" | custom-call | flops 20000000000 | tf_op jit(solution)/shard_map/pallas_call | solution.py:42
  6.1 0.0 copy-start.8
  6.1 0.6 copy-done.8
  6.8 0.0 copy-start.10
  6.8 0.7 copy-done.10
  7.4 0.7 copy-done.12
  8.1 0.0 collective-permute-done.other_ref
  8.1 0.0 copy-done
  8.1 0.0 copy-done.6
  8.1 0.0 copy-done.14
  8.1 0.0 copy-done.15
  8.1 0.0 copy-done.16
  8.1 0.0 copy-start.1
  8.1 1.6 %copy-done.1 = bf16[2048,512]{1,0:T(8,128)(2,1)S(1)} copy-done((bf16[2048,512]{1,0:T(8,128)(2,1)S(1)}, bf16[2048,512]{1,0:T(8,128)(2,1)}, u32[]{:S(2)}) %copy-start.1) | copy-done | bytes 2097176
  9.7 0.9 %copy-done.7 = bf16[48,3,512]{2,0,1:T(8,128)(2,1)S(1)} copy-done((bf16[48,3,512]{2,0,1:T(8,128)(2,1)S(1)}, bf16[48,3,512]{2,0,1:T(8,128)(2,1)}, u32[]{:S(2)}) %copy-start.7) | copy-done | bytes 147480
  10.6 0.9 %copy-done.11 = bf16[512,128]{1,0:T(8,128)(2,1)S(1)} copy-done((bf16[512,128]{1,0:T(8,128)(2,1)S(1)}, bf16[512,128]{1,0:T(8,128)(2,1)}, u32[]{:S(2)}) %copy-start.11) | copy-done | bytes 131096
  11.5 0.9 %copy-done.13 = bf16[512,128]{1,0:T(8,128)(2,1)S(1)} copy-done((bf16[512,128]{1,0:T(8,128)(2,1)S(1)}, bf16[512,128]{1,0:T(8,128)(2,1)}, u32[]{:S(2)}) %copy-start.13) | copy-done | bytes 131096
  12.4 0.7 copy-done.18
  13.1 2.1 %shard_map.186 = (f32[48,512]{1,0:T(8,128)S(1)}, bf16[48,512]{1,0:T(8,128)(2,1)S(1)}) custom-call(s32[1]{0:T(128)} %bitcast.core_ref, bf16[48,1024]{1,0:T(8,128)(2,1)S(1)} %copy-done.6, bf16[48,1024]{1,0:T(8,128)(2,1)} %collective-permute-done.other_ref, f32[1,2048]{1,0:T(1,128)S(1)} %bitcast.18, bf16[2048,512]{1,0:T(8,128)(2,1)S(1)} %copy-done, ...), custom_call_target="tpu_custom_call" | custom-call | flops 210000000 | tf_op jit(solution)/shard_map/pallas_call | solution.py:42
  15.2 0.0 copy-start.3
  15.2 0.0 copy-start.4
  15.2 0.0 copy-start.5
  15.3 0.0 copy-start.17
  15.3 0.5 collective-permute-start.1
  15.8 0.9 %collective-permute-done.1.other_ref = bf16[48,512]{1,0:T(8,128)(2,1)S(1)} collective-permute-done((bf16[48,512]{1,0:T(8,128)(2,1)S(1)}, bf16[48,512]{1,0:T(8,128)(2,1)S(1)}, u32[]{:S(2)}, u32[]{:S(2)}) %collective-permute-start.1) | collective-permute-done | bytes 49184 | tf_op jit(solution)/shard_map/ppermute | solution.py:15
  16.6 0.0 copy-done.2
  16.6 0.0 copy-done.9
  16.7 0.8 shard_map.187
  17.4 0.0 collective-permute-done.2.gate_b
  17.4 0.0 collective-permute-done.3.up_b
  17.4 0.0 collective-permute-done.4.down_b
  17.4 33.6 %all_to_all.10.rows_ref = bf16[256,2,512]{2,1,0:T(2,128)(2,1)S(1)} all-to-all(bf16[256,2,512]{2,1,0:T(2,128)(2,1)S(1)} %get-tuple-element.21), channel_id=1, replica_groups=mesh['ep'=128,'tp'=2] {'tp','ep'}, dimensions={0} | all-to-all | bytes 1048576 | tf_op jit(solution)/shard_map/all_to_all | solution.py:270
  51.1 0.0 copy-done.3
  51.1 0.0 copy-done.4
  51.1 0.0 copy-done.5
  51.1 0.0 copy-done.17
  51.1 3.2 %shard_map.188 = bf16[256,2,512]{2,1,0:T(2,128)(2,1)S(1)} custom-call(bf16[256,2,512]{2,1,0:T(2,128)(2,1)S(1)} %all_to_all.10.rows_ref, f32[1,2048]{1,0:T(1,128)S(1)} %bitcast.19, bf16[2048,256]{1,0:T(8,128)(2,1)S(1)} %bitcast.12, bf16[2048,256]{1,0:T(8,128)(2,1)S(1)} %bitcast.14, bf16[256,2048]{1,0:T(8,128)(2,1)S(1)} %bitcast.16, ...), custom_call_target="tpu_custom_call" | custom-call | flops 810000000 | tf_op jit(solution)/shard_map/pallas_call | solution.py:42
  54.2 26.2 %all_to_all.11.returned_ref = bf16[256,2,512]{2,1,0:T(2,128)(2,1)S(1)} all-to-all(bf16[256,2,512]{2,1,0:T(2,128)(2,1)S(1)} %shard_map.188), channel_id=1, replica_groups=mesh['ep'=128,'tp'=2] {'tp','ep'}, dimensions={0} | all-to-all | bytes 1048576 | tf_op jit(solution)/shard_map/all_to_all | solution.py:270
  80.4 0.9 %shard_map.189 = bf16[48,1024]{1,0:T(8,128)(2,1)} custom-call(bf16[256,2,512]{2,1,0:T(2,128)(2,1)S(1)} %all_to_all.11.returned_ref, bf16[192,512]{1,0:T(8,128)(2,1)S(1)} %get-tuple-element.25.pick_ref, bf16[48,1024]{1,0:T(8,128)(2,1)S(1)} %get-tuple-element.26.residual_ref), custom_call_target="tpu_custom_call" | custom-call | flops 100000000 | tf_op jit(solution)/shard_map/pallas_call | solution.py:42
  (7 shorter events, 0.0 us)
Async XLA Ops:
  0.6 7.5 %collective-permute-start = (bf16[48,1024]{1,0:T(8,128)(2,1)}, bf16[48,1024]{1,0:T(8,128)(2,1)}, u32[]{:S(2)}, u32[]{:S(2)}) collective-permute-start(bf16[48,1024]{1,0:T(8,128)(2,1)} %tokens_ref.1), channel_id=1, source_target_pairs={{0,1},{1,0},{2,3},{3,2},{4,5},{5,4},{6,7},{7,6},{8,9},{9,8},{10,11... | collective-permute-start | bytes 294920 | tf_op jit(solution)/shard_map/ppermute | solution.py:15
  3.9 13.5 %collective-permute-start.2 = (bf16[2048,256]{1,0:T(8,128)(2,1)}, bf16[2048,256]{1,0:T(8,128)(2,1)S(1)}, u32[]{:S(2)}, u32[]{:S(2)}) collective-permute-start(bf16[2048,256]{1,0:T(8,128)(2,1)} %bitcast.11), channel_id=1, source_target_pairs={{0,1},{1,0},{2,3},{3,2},{4,5},{5,4},{6,7},{7,6},{8,9},{9,8},{10,11... | collective-permute-start | bytes 3145736 | tf_op jit(solution)/shard_map/ppermute | solution.py:15
  4.0 13.4 %collective-permute-start.3 = (bf16[2048,256]{1,0:T(8,128)(2,1)}, bf16[2048,256]{1,0:T(8,128)(2,1)}, u32[]{:S(2)}, u32[]{:S(2)}) collective-permute-start(bf16[2048,256]{1,0:T(8,128)(2,1)} %bitcast.13), channel_id=1, source_target_pairs={{0,1},{1,0},{2,3},{3,2},{4,5},{5,4},{6,7},{7,6},{8,9},{9,8},{10,11... | collective-permute-start | bytes 3145736 | tf_op jit(solution)/shard_map/ppermute | solution.py:15
  4.4 13.0 %collective-permute-start.4 = (bf16[256,2048]{1,0:T(8,128)(2,1)}, bf16[256,2048]{1,0:T(8,128)(2,1)}, u32[]{:S(2)}, u32[]{:S(2)}) collective-permute-start(bf16[256,2048]{1,0:T(8,128)(2,1)} %bitcast.15), channel_id=1, source_target_pairs={{0,1},{1,0},{2,3},{3,2},{4,5},{5,4},{6,7},{7,6},{8,9},{9,8},{10,11... | collective-permute-start | bytes 3145736 | tf_op jit(solution)/shard_map/ppermute | solution.py:15
  4.5 3.6 %copy-start = (bf16[2048,512]{1,0:T(8,128)(2,1)S(1)}, bf16[2048,512]{1,0:T(8,128)(2,1)}, u32[]{:S(2)}) copy-start(bf16[2048,512]{1,0:T(8,128)(2,1)} %branch_ref.1) | copy-start | bytes 6291460
  4.5 3.6 %copy-start.6 = (bf16[48,1024]{1,0:T(8,128)(2,1)S(1)}, bf16[48,1024]{1,0:T(8,128)(2,1)}, u32[]{:S(2)}) copy-start(bf16[48,1024]{1,0:T(8,128)(2,1)} %tokens_ref.1) | copy-start | bytes 294916
  4.5 3.6 %copy-start.14 = (f32[48,512]{1,0:T(8,128)S(1)}, f32[48,512]{1,0:T(8,128)}, u32[]{:S(2)}) copy-start(f32[48,512]{1,0:T(8,128)} %hidden_ref.1) | copy-start | bytes 294916
  4.5 3.6 %copy-start.15 = (f32[2048]{0:T(1024)S(1)}, f32[2048]{0:T(1024)}, u32[]{:S(2)}) copy-start(f32[2048]{0:T(1024)} %param.21) | copy-start | bytes 24580
  4.5 3.6 %copy-start.16 = (f32[4,512]{1,0:T(4,128)S(1)}, f32[4,512]{1,0:T(4,128)}, u32[]{:S(2)}) copy-start(f32[4,512]{1,0:T(4,128)} %taps_ref.1) | copy-start | bytes 24580
  6.1 0.7 copy-start.8
  6.8 0.7 copy-start.10
  7.4 0.7 copy-start.12
  8.1 1.6 %copy-start.1 = (bf16[2048,512]{1,0:T(8,128)(2,1)S(1)}, bf16[2048,512]{1,0:T(8,128)(2,1)}, u32[]{:S(2)}) copy-start(bf16[2048,512]{1,0:T(8,128)(2,1)} %gelu_ref.1) | copy-start | bytes 6291460
  9.7 0.9 %copy-start.7 = (bf16[48,3,512]{2,0,1:T(8,128)(2,1)S(1)}, bf16[48,3,512]{2,0,1:T(8,128)(2,1)}, u32[]{:S(2)}) copy-start(bf16[48,3,512]{2,0,1:T(8,128)(2,1)} %param.19) | copy-start | bytes 442372
  10.6 0.9 %copy-start.11 = (bf16[512,128]{1,0:T(8,128)(2,1)S(1)}, bf16[512,128]{1,0:T(8,128)(2,1)}, u32[]{:S(2)}) copy-start(bf16[512,128]{1,0:T(8,128)(2,1)} %copy-done.10) | copy-start | bytes 393220
  11.5 0.9 %copy-start.13 = (bf16[512,128]{1,0:T(8,128)(2,1)S(1)}, bf16[512,128]{1,0:T(8,128)(2,1)}, u32[]{:S(2)}) copy-start(bf16[512,128]{1,0:T(8,128)(2,1)} %copy-done.12) | copy-start | bytes 393220
  12.4 0.7 copy-start.18
  13.1 3.5 %copy-start.2 = (bf16[1024,1024]{1,0:T(8,128)(2,1)S(1)}, bf16[1024,1024]{1,0:T(8,128)(2,1)}, u32[]{:S(2)}) copy-start(bf16[1024,1024]{1,0:T(8,128)(2,1)} %weight_ref.1) | copy-start | bytes 6291460
  13.1 3.5 %copy-start.9 = (bf16[512,96]{1,0:T(8,128)(2,1)S(1)}, bf16[512,96]{1,0:T(8,128)(2,1)}, u32[]{:S(2)}) copy-start(bf16[512,96]{1,0:T(8,128)(2,1)} %copy-done.8) | copy-start | bytes 294916
  15.2 35.8 %copy-start.3 = (bf16[1,2048,256]{2,1,0:T(8,128)(2,1)S(1)}, bf16[1,2048,256]{2,1,0:T(8,128)(2,1)}, u32[]{:S(2)}) copy-start(bf16[1,2048,256]{2,1,0:T(8,128)(2,1)} %param.33) | copy-start | bytes 3145732
  15.2 35.8 %copy-start.4 = (bf16[1,2048,256]{2,1,0:T(8,128)(2,1)S(1)}, bf16[1,2048,256]{2,1,0:T(8,128)(2,1)}, u32[]{:S(2)}) copy-start(bf16[1,2048,256]{2,1,0:T(8,128)(2,1)} %param.34) | copy-start | bytes 3145732
  15.2 35.8 %copy-start.5 = (bf16[1,256,2048]{2,1,0:T(8,128)(2,1)S(1)}, bf16[1,256,2048]{2,1,0:T(8,128)(2,1)}, u32[]{:S(2)}) copy-start(bf16[1,256,2048]{2,1,0:T(8,128)(2,1)} %param.35) | copy-start | bytes 3145732
  15.3 35.8 %copy-start.17 = (f32[2048]{0:T(1024)S(1)}, f32[2048]{0:T(1024)}, u32[]{:S(2)}) copy-start(f32[2048]{0:T(1024)} %param.29) | copy-start | bytes 24580
  15.3 1.4 %collective-permute-start.1 = (bf16[48,512]{1,0:T(8,128)(2,1)S(1)}, bf16[48,512]{1,0:T(8,128)(2,1)S(1)}, u32[]{:S(2)}, u32[]{:S(2)}) collective-permute-start(bf16[48,512]{1,0:T(8,128)(2,1)S(1)} %get-tuple-element.17.own_ref), channel_id=1, source_target_pairs={{0,1},{1,0},{2,3},{3,2},{4,5},{5,4},{6,7},{7,6},{8,9},{9,8},{10,11... | collective-permute-start | bytes 147464 | tf_op jit(solution)/shard_map/ppermute | solution.py:15
